TPU v7x, 32 devices: a whole 2x2x4 slice. The times are simulated.
32 devices in a mesh: sp: 16 (over z, y, x), tp: 2 (over core).
Axes of the slice: x: 2, y: 2, z: 4, core: 2. Of those that a mesh axis runs over, the one named last changes fastest.
Arguments:
- queries: bfloat16 [4096, 2048], P('sp', 'tp'), may hold values from -6 to 6
- keys: bfloat16 [4096, 2048], P('sp', 'tp'), may hold values from -6 to 6
- hidden: bfloat16 [4096, 2048], P('sp'), may hold values from -6 to 6
- value_weight: bfloat16 [2048, 2048], P(None, 'tp'), may hold values from -0.125 to 0.125
- beta_pre: float32 [4096, 16], P('sp', 'tp'), may hold values from -9 to 3
- decay_pre: float32 [4096, 16], P('sp', 'tp'), may hold values from -5 to 4
- decay_rate: float32 [16], P('tp'), may hold values from 0 to 0.06
- out_grad: bfloat16 [4096, 2048], P('sp', 'tp'), may hold values from -6 to 6
Outputs:
- d_queries: bfloat16 [4096, 2048], P('sp', 'tp')
- d_keys: bfloat16 [4096, 2048], P('sp', 'tp')
- d_beta: float32 [4096, 16], P('sp', 'tp')
- d_decay: float32 [4096, 16], P('sp', 'tp')
- d_hidden: bfloat16 [4096, 2048], P(('sp', 'tp'))
- d_weight: float32 [2048, 2048], P('sp', 'tp')
All inputs are finite; a program needn't handle non-finite values.
Results may differ from a plain program's by a relative error of at most 0.022.
Values may be sent and summed in bfloat16 or wider, within the bound.
No kernel may reach another device: no remote copies, remote signals or barrier semaphores. Data moves between devices by JAX's collectives and lax.ppermute only.
A program may use at most 256 MiB of HBM per device.

v0:
```python
import jax
import jax.numpy as jnp
from jax import lax
from jax.sharding import PartitionSpec as P

BLOCK = 64


highest = lax.Precision.HIGHEST
norm_floor = 16.0


def prefix(value, axis, join, neutral, backward):
    count = lax.axis_size(axis)
    place = lax.axis_index(axis)
    ahead = count - 1 - place if backward else place
    gathered = jax.tree.map(
        lambda a, kind: lax.all_gather(a.astype(kind), axis),
        value,
        jax.tree.map(lambda a: jnp.bfloat16 if a.dtype == jnp.float32 else a.dtype, value),
    )
    state = jax.tree.map(lambda a, e: jnp.zeros_like(a) + jnp.asarray(e, a.dtype), value, neutral)

    def one(step, state):
        source = count - 1 - step if backward else step
        return join(
            state,
            jax.tree.map(
                lambda a, own: lax.dynamic_index_in_dim(a, source, 0, False).astype(own.dtype),
                gathered,
                value,
            ),
        )

    return lax.fori_loop(0, ahead, one, state)


def to_blocks(tensor, blocks):
    shaped = tensor.reshape((blocks, BLOCK) + tensor.shape[1:])
    return jnp.moveaxis(shaped, 1, 2)


def block_setup(key_raw, beta_pre, decay_pre, rate):
    blocks = key_raw.shape[0] // BLOCK
    key_unit = key_raw * lax.rsqrt(jnp.sum(key_raw * key_raw, axis=-1, keepdims=True) + norm_floor)
    write_rate = jax.nn.sigmoid(beta_pre)
    log_decay = -rate[None, :] * jax.nn.softplus(decay_pre)
    key_blocks = to_blocks(key_unit, blocks)
    rate_blocks = to_blocks(write_rate, blocks)
    log_sums = jnp.cumsum(to_blocks(log_decay, blocks), axis=-1)
    position = jnp.arange(BLOCK)
    inclusive = position[:, None] >= position[None, :]
    strict = position[:, None] > position[None, :]
    spread = log_sums[..., :, None] - log_sums[..., None, :]
    decay_mask = jnp.where(inclusive, jnp.exp(jnp.where(inclusive, spread, 0.0)), 0.0)
    key_gram = jnp.einsum("nhid,nhjd->nhij", key_blocks, key_blocks, precision=highest)
    lower_part = jnp.where(strict, rate_blocks[..., :, None] * key_gram * decay_mask, 0.0)
    system = jnp.eye(BLOCK, dtype=jnp.float32) + lower_part
    return (key_blocks, rate_blocks, log_sums, decay_mask, system)


def span_pieces(query_raw, key_raw, values, beta_pre, decay_pre, rate):
    key_blocks, rate_blocks, log_sums, decay_mask, system = block_setup(
        key_raw, beta_pre, decay_pre, rate
    )
    blocks = key_blocks.shape[0]
    query_unit = query_raw * lax.rsqrt(
        jnp.sum(query_raw * query_raw, axis=-1, keepdims=True) + norm_floor
    )
    query_unit = query_unit * query_raw.shape[-1] ** (-0.5)
    query_blocks = to_blocks(query_unit, blocks)
    value_blocks = to_blocks(values, blocks)
    block_gain = jnp.exp(log_sums)
    right_side = jnp.concatenate(
        [rate_blocks[..., None] * value_blocks, (rate_blocks * block_gain)[..., None] * key_blocks],
        axis=-1,
    )
    solved = jax.scipy.linalg.solve_triangular(system, right_side, lower=True, unit_diagonal=True)
    value_size = values.shape[-1]
    query_key = (
        jnp.einsum("nhid,nhjd->nhij", query_blocks, key_blocks, precision=highest) * decay_mask
    )
    query_decayed = query_blocks * block_gain[..., None]
    key_decayed = key_blocks * jnp.exp(log_sums[..., -1:] - log_sums)[..., None]
    pieces = (
        solved[..., :value_size],
        solved[..., value_size:],
        query_key,
        query_decayed,
        key_decayed,
        block_gain[..., -1],
    )
    return (pieces, (system, rate_blocks))


def sweep_pieces(pieces, carry_state):

    def sweep_advance(current, inputs):
        new_values, key_sweep, query_key, query_decayed, key_decayed, end_gain = inputs
        written = new_values - jnp.einsum("hcd,hde->hce", key_sweep, current, precision=highest)
        output = jnp.einsum("hcd,hde->hce", query_decayed, current, precision=highest)
        output = output + jnp.einsum("hij,hje->hie", query_key, written, precision=highest)
        current = end_gain[:, None, None] * current + jnp.einsum(
            "hcd,hce->hde", key_decayed, written, precision=highest
        )
        return (current, output)

    final, outputs = lax.scan(sweep_advance, carry_state, pieces)
    outputs = jnp.moveaxis(outputs, 2, 1)
    return (
        outputs.reshape(outputs.shape[0] * outputs.shape[1], outputs.shape[2], outputs.shape[3]),
        final,
    )


def span_transition(pieces):
    key_sweep, key_decayed, end_gain = (pieces[1], pieces[4], pieces[5])
    head_count, key_size = (key_sweep.shape[1], key_sweep.shape[3])

    def span_advance(transition, inputs):
        sweep, decayed, gain = inputs
        mixed = jnp.einsum("hce,hef->hcf", sweep, transition, precision=highest)
        updated = gain[:, None, None] * transition - jnp.einsum(
            "hcd,hcf->hdf", decayed, mixed, precision=highest
        )
        return (updated, None)

    identity = jnp.broadcast_to(
        jnp.eye(key_size, dtype=jnp.float32), (head_count, key_size, key_size)
    )
    final, _ = lax.scan(span_advance, identity, (key_sweep, key_decayed, end_gain))
    return final


def chain_forward(earlier, later):
    product = jnp.einsum("hde,hef->hdf", later[0], earlier[0], precision=highest)
    offset = jnp.einsum("hde,hef->hdf", later[0], earlier[1], precision=highest) + later[1]
    return (product, offset)


def chain_backward(earlier, later):
    product = jnp.einsum("hde,hef->hdf", later[0], earlier[0], precision=highest)
    offset = later[1] + jnp.einsum("hde,hef->hdf", later[0], earlier[1], precision=highest)
    return (product, offset)


def weight_term(hidden, grad_list):
    total = lax.dot_general(
        hidden, grad_list[0], (((0,), (0,)), ((), ())), preferred_element_type=jnp.float32
    )
    for extra in grad_list[1:]:
        total = total + lax.dot_general(
            hidden, extra, (((0,), (0,)), ((), ())), preferred_element_type=jnp.float32
        )
    return total


def per_device(queries, keys, hidden, value_weight, beta_pre, decay_pre, decay_rate, out_grad):
    head_count = decay_rate.shape[0]
    key_size = queries.shape[1] // head_count
    value_size = value_weight.shape[1] // head_count
    length = queries.shape[0]
    blocks = length // BLOCK
    values = jnp.dot(hidden, value_weight, preferred_element_type=jnp.float32).astype(jnp.bfloat16)
    query_raw = queries.astype(jnp.float32).reshape(length, head_count, key_size)
    key_raw = keys.astype(jnp.float32).reshape(length, head_count, key_size)
    value_heads = values.astype(jnp.float32).reshape(length, head_count, value_size)
    grad_heads = out_grad.astype(jnp.float32).reshape(length, head_count, value_size)
    zero_state = jnp.zeros((head_count, key_size, value_size), jnp.float32)

    def make_pieces(query_in, key_in, value_in, beta_in, decay_in):
        return span_pieces(query_in, key_in, value_in, beta_in, decay_in, decay_rate)

    primal = (query_raw, key_raw, value_heads, beta_pre, decay_pre)
    pieces, pull_pieces, extras = jax.vjp(make_pieces, *primal, has_aux=True)
    system, rate_blocks = extras

    def value_solve(value_in):
        scaled = rate_blocks[..., None] * to_blocks(value_in, blocks)
        return jax.scipy.linalg.solve_triangular(system, scaled, lower=True, unit_diagonal=True)

    _, pull_values = jax.vjp(value_solve, value_heads)
    (_, span_offset), pull_zero = jax.vjp(sweep_pieces, pieces, zero_state)
    local_cot, own_state_grad = pull_zero((grad_heads, zero_state))
    value_local = pull_values(local_cot[0])[0]
    local_grad = value_local.reshape(length, head_count * value_size).astype(jnp.bfloat16)
    transition = span_transition(pieces)
    identity = jnp.broadcast_to(jnp.eye(key_size, dtype=jnp.float32), transition.shape)
    earlier_maps = prefix(
        (transition, span_offset), "sp", chain_forward, (identity, zero_state), False
    )
    start_state = earlier_maps[1]
    later_maps = prefix(
        (jnp.swapaxes(transition, 1, 2), own_state_grad),
        "sp",
        chain_backward,
        (identity, zero_state),
        True,
    )
    end_grad = later_maps[1]
    _, pull_full = jax.vjp(sweep_pieces, pieces, start_state)
    total_cot = pull_full((grad_heads, end_grad))[0]
    carried_cot = jax.tree.map(lambda first, second: first - second, total_cot, local_cot)
    grad_query, grad_key, _, grad_beta, grad_decay = pull_pieces(total_cot)
    value_carried = pull_values(carried_cot[0])[0]
    carried_grad = value_carried.reshape(length, head_count * value_size).astype(jnp.bfloat16)
    d_weight = lax.psum_scatter(
        weight_term(hidden, [local_grad, carried_grad]), "sp", scatter_dimension=0, tiled=True
    )
    total = lax.dot_general(
        local_grad, value_weight, (((1,), (1,)), ((), ())), preferred_element_type=jnp.float32
    )
    d_hidden = lax.psum_scatter(
        (
            total
            + lax.dot_general(
                carried_grad,
                value_weight,
                (((1,), (1,)), ((), ())),
                preferred_element_type=jnp.float32,
            )
        ).astype(jnp.bfloat16),
        "tp",
        scatter_dimension=0,
        tiled=True,
    )
    d_queries = grad_query.reshape(length, head_count * key_size).astype(jnp.bfloat16)
    d_keys = grad_key.reshape(length, head_count * key_size).astype(jnp.bfloat16)
    return (d_queries, d_keys, grad_beta, grad_decay, d_hidden, d_weight)


def solution(mesh):
    return jax.shard_map(
        per_device,
        mesh=mesh,
        in_specs=(
            P("sp", "tp"),
            P("sp", "tp"),
            P("sp", None),
            P(None, "tp"),
            P("sp", "tp"),
            P("sp", "tp"),
            P("tp"),
            P("sp", "tp"),
        ),
        out_specs=(
            P("sp", "tp"),
            P("sp", "tp"),
            P("sp", "tp"),
            P("sp", "tp"),
            P(("sp", "tp"), None),
            P("sp", "tp"),
        ),
        check_vma=False,
    )
```

profile of v0, /device:TPU:0, one launch (start us, length us, event | category | flops | bytes accessed | tf_op | source)
XLA Modules:
  0.0 823.7 jit_solution(2084794772031629973)
XLA Ops:
  19.0 158.0 %custom-call.13 = f32[4,8,1,64,64]{3,4,2,1,0:T(8,128)S(1)} custom-call(f32[4,8,1,64,64]{4,3,2,1,0:T(8,128)} %get-tuple-element.1072), custom_call_target="InvertDiagBlocksLowerTriangular" | custom-call | tf_op jit(solution)/shard_map/jvp(jit(_solve_triangular))/vmap(vmap())/triangular_solve | solution.py:78
  177.1 3.7 fusion.111
  187.9 17.2 %while.108 = (s32[]{:T(128)}, f32[8,128,128]{2,1,0:T(8,128)S(1)}, f32[4,8]{1,0:T(4,128)}, f32[4,8,64,128]{3,2,1,0:T(8,128)}, f32[4,8,64,128]{3,2,1,0:T(8,128)}, /*index=5*/s32[]{:T(128)}) while((s32[]{:T(128)}, f32[8,128,128]{2,1,0:T(8,128)S(1)}, f32[4,8]{1,0:T(4,128)}, f32[4,8,64,128]{3,2,1,0:T(8,128)}, f32[4,8,64,128]{3,2,1,0:T(8,128)}, ...), condition=%wide.region_3.4_spmd, body=%wide.region_2.3_spmd.sunk | while | flops 201588736 | bytes 2622633 | solution.py:131
  207.2 22.1 %while.113 = (s32[]{:T(128)}, f32[8,128,128]{2,1,0:T(8,128)S(1)}, f32[4,8,1,1]{1,3,2,0:T(1,128)}, f32[4,8]{1,0:T(4,128)}, f32[4,8,64,128]{3,2,1,0:T(8,128)}, /*i...) while((s32[]{:T(128)}, f32[8,128,128]{2,1,0:T(8,128)S(1)}, ...), condition=%wide.region_6.7_spmd.clone, body=%wide.region_5.6_spmd.clone.sunk | while | flops 201916416 | bytes 2886860 | solution.py:108
  237.0 36.7 %while.114 = (s32[]{:T(128)}, f32[8,128,128]{2,1,0:T(8,128)}, f32[4,8,64,128]{3,2,1,0:T(8,128)}, f32[4,8,1,1]{1,3,2,0:T(1,128)}, f32[4,8,64,128]{3,2,1,0:T(8,128...) while((s32[]{:T(128)}, f32[8,128,128]{2,1,0:T(8,128)}, ...), condition=%wide.region_8.9_spmd.clone, body=%wide.region_7.8_spmd.clone.sunk | while | flops 353107968 | bytes 7606003 | solution.py:108
  270.9 2.8 convolution_add_fusion.30
  280.4 5.6 fusion.146
  286.0 75.6 %all-gather.15.cloned.1.call-done = bf16[128,128,128]{2,1,0:T(8,128)(2,1)} async-done(((bf16[8,128,128]{2,1,0:T(8,128)(2,1)}), bf16[128,128,128]{2,1,0:T(8,128)(2,1)}) %all-gather.15.cloned.1.call-update) | async-done | bytes 4194320 | tf_op jit(solution)/shard_map/all_gather | solution.py:18
  362.8 26.2 %while.111 = (s32[]{:T(128)}, f32[8,128,128]{2,1,0:T(8,128)S(1)}, f32[4,8,128,128]{3,2,1,0:T(8,128)}, f32[4,8,64,128]{3,2,1,0:T(8,128)}, f32[4,8,1,1]{1,3,2,0:T(...) while((s32[]{:T(128)}, f32[8,128,128]{2,1,0:T(8,128)S(1)}, ...), condition=%wide.region_14.15_spmd, body=%wide.region_13.14_spmd.sunk | while | flops 201654272 | bytes 4197101 | solution.py:108
  389.0 50.2 %all-gather.9.cloned.1.call-done = bf16[128,128,128]{2,1,0:T(8,128)(2,1)} async-done(((bf16[8,128,128]{2,1,0:T(8,128)(2,1)}), bf16[128,128,128]{2,1,0:T(8,128)(2,1)}) %all-gather.9.cloned.1.call-update) | async-done | bytes 4194320 | tf_op jit(solution)/shard_map/all_gather | solution.py:18
  439.2 77.4 %all-gather.11.cloned.1.call-done = bf16[128,128,128]{2,1,0:T(8,128)(2,1)} async-done(((bf16[8,128,128]{2,1,0:T(8,128)(2,1)}), bf16[128,128,128]{2,1,0:T(8,128)(2,1)}) %all-gather.11.cloned.1.call-update) | async-done | bytes 4194320 | tf_op jit(solution)/shard_map/all_gather | solution.py:18
  516.6 23.0 %while.109 = (s32[]{:T(128)}, f32[8,128,128]{2,1,0:T(8,128)S(1)}, s32[]{:T(128)}, bf16[16,8,128,128]{3,2,1,0:T(8,128)(2,1)}, bf16[16,8,128,128]{3,2,1,0:T(8,128)...) while((s32[]{:T(128)}, f32[8,128,128]{2,1,0:T(8,128)S(1)}, s32[]{:T(128)}, ...), condition=%wide.region_10.11_spmd, body=%wide.region_9.10_spmd.sunk | while | flops 201588736 | bytes 2622603 | solution.py:35
  545.2 71.6 %while.112 = (s32[]{:T(128)}, f32[8,128,128]{2,1,0:T(8,128)S(1)}, f32[4,8,64,128]{3,2,1,0:T(8,128)}, f32[4,8,64,128]{3,2,1,0:T(8,128)}, f32[4,8,64,64]{3,2,1,0:T...) while((s32[]{:T(128)}, f32[8,128,128]{2,1,0:T(8,128)S(1)}, ...), condition=%wide.region_17.18_spmd, body=%wide.region_15.17_spmd.sunk | while | flops 705495040 | bytes 18882472 | solution.py:108
  551.2 2.8 fusion.287
  557.8 2.9 fusion.286
  569.1 2.8 fusion.287
  575.7 2.9 fusion.286
  587.0 2.8 fusion.287
  593.6 3.0 fusion.286
  604.9 2.8 fusion.287
  611.6 3.0 fusion.286
  616.8 3.1 fusion.112
  621.0 8.0 add_bitcast_fusion
  629.8 5.5 fusion.148
  639.4 4.2 fusion.101
  643.6 3.4 multiply_select_fusion
  652.9 4.8 fusion.104
  657.7 2.8 convolution_add_fusion.12
  664.2 5.4 fusion.96
  669.7 4.2 broadcast_multiply_fusion
  683.3 119.6 %reduce-scatter.5.cloned.1.call-done = f32[128,1024]{0,1:T(8,128)} async-done(((f32[2048,1024]{0,1:T(8,128)}), f32[128,1024]{0,1:T(8,128)}) %reduce-scatter.5.cloned.1.call-update) | async-done | bytes 524304 | tf_op jit(solution)/shard_map/reduce_scatter | solution.py:207
  804.9 11.5 %reduce-scatter.3.cloned.1.call-done = bf16[128,2048]{1,0:T(8,128)(2,1)} async-done(((bf16[256,2048]{1,0:T(8,128)(2,1)}), bf16[128,2048]{1,0:T(8,128)(2,1)}) %reduce-scatter.3.cloned.1.call-update) | async-done | bytes 524304 | tf_op jit(solution)/shard_map/reduce_scatter | solution.py:213
  (364 shorter events, 238.5 us)
Async XLA Ops:
  7.2 169.9 %copy-start = (bf16[256,2048]{1,0:T(8,128)(2,1)S(1)}, bf16[256,2048]{1,0:T(8,128)(2,1)}, u32[]{:S(2)}) copy-start(bf16[256,2048]{1,0:T(8,128)(2,1)} %param.26) | copy-start | bytes 3145732
  7.2 278.8 %all-gather.13.cloned.1.call-start = ((), (), s32[]{:S(2)}) async-start(), calls=%async_computation.6 | async-start | bytes 4456448 | tf_op jit(solution)/shard_map/all_gather | solution.py:18
  7.2 10.0 %copy-start.36 = (pred[64,64]{1,0:T(8,128)(4,1)}, pred[64,64]{1,0:T(8,128)(4,1)S(1)}, u32[]{:S(2)}) copy-start(pred[64,64]{1,0:T(8,128)(4,1)S(1)} %get-tuple-element.1082) | copy-start | bytes 12292
  9.9 7.3 copy-start.3
  11.1 6.1 copy-start.48
  11.4 5.8 copy-start.38
  14.8 4.2 copy-start.22
  177.0 6.2 copy-start.7
  206.1 155.5 %all-gather.15.cloned.1.call-start = ((), (), s32[]{:S(2)}) async-start(), calls=%async_computation.7 | async-start | bytes 4456448 | tf_op jit(solution)/shard_map/all_gather | solution.py:18
  230.1 209.1 %all-gather.9.cloned.1.call-start = ((), (), s32[]{:S(2)}) async-start(), calls=%async_computation.4 | async-start | bytes 4456448 | tf_op jit(solution)/shard_map/all_gather | solution.py:18
  237.0 4.3 copy-start.2
  246.1 4.5 copy-start.2
  255.3 4.5 copy-start.2
  264.5 4.5 copy-start.2
  273.7 6.7 copy-start.1
  275.9 240.7 %all-gather.11.cloned.1.call-start = ((), (), s32[]{:S(2)}) async-start(), calls=%async_computation.5 | async-start | bytes 4456448 | tf_op jit(solution)/shard_map/all_gather | solution.py:18
  276.4 526.4 %reduce-scatter.5.cloned.1.call-start = ((), (), s32[]{:S(2)}) async-start(), calls=%async_computation.3 | async-start | bytes 8912896 | tf_op jit(solution)/shard_map/reduce_scatter | solution.py:207
  545.2 5.9 copy-start.6
  563.1 5.9 copy-start.6
  580.9 5.9 copy-start.6
  598.9 5.9 copy-start.6
  629.0 187.4 %reduce-scatter.3.cloned.1.call-start = ((), (), s32[]{:S(2)}) async-start(), calls=%async_computation.2 | async-start | bytes 1572864 | tf_op jit(solution)/shard_map/reduce_scatter | solution.py:213
  629.8 5.6 copy-start.8
  629.8 5.6 copy-start.11
  629.8 5.6 copy-start.14
  639.3 4.2 copy-start.9
  639.3 4.2 copy-start.12
  639.3 4.2 copy-start.16
  639.3 4.3 copy-start.23
  639.3 4.3 copy-start.37
  639.4 4.3 copy-start.39
  652.9 4.8 copy-start.25
  (31 other events, 61.7 us)
Sparse Core Ops, SparseCore 0:
  206.3 78.3 all-gather.12
  287.4 74.1 all-gather.14
  364.9 74.1 all-gather.8
  442.4 74.1 all-gather.10
  629.1 173.7 reduce-scatter.4
  805.5 10.8 reduce-scatter.2
where the time goes:
time: 835 us; the launch traced here: 824 us
  waiting for transfers between devices  335 us (40%)
  matrix products  236 us (28%)
  other arithmetic  181 us (22%)
  local copies, waits for them, and re-layouts  53.3 us (6%)
  between operations  15.5 us (2%)
    all_gather x4, waiting for transfers between devices, prefix(): lax.all_gather(a.astype(kind), axis)  203 us
    another operation x4, other arithmetic, span_pieces(): jax.scipy.linalg.solve_triangular(system, right_side, lower=True, unit_di...  158 us
    reduce_scatter x1, waiting for transfers between devices, per_device(): lax.psum_scatter(weight_term(hidden, [local_grad, carried_grad]), 'sp', s...  120 us
    dot_general x20, matrix products, sweep_advance(): jnp.einsum('hcd,hde->hce', key_sweep, current, precision=highest)  41.9 us
    dot_general x20, matrix products, sweep_advance(): jnp.einsum('hcd,hce->hde', key_decayed, written, precision=highest)  41.1 us
    dot_general x12, matrix products, sweep_advance(): jnp.einsum('hcd,hde->hce', query_decayed, current, precision=highest)  27.8 us
    dot_general x12, matrix products, sweep_advance(): jnp.einsum('hij,hje->hie', query_key, written, precision=highest)  25.8 us
    dot_general x15, matrix products, chain_backward(): jnp.einsum('hde,hef->hdf', later[0], earlier[1], precision=highest)  21.7 us
  transfers between devices with their start and end apart: 6, of which 5 were waited for; matrix products, arithmetic and copies ran while one was open for 19% of the time, Pallas kernels for 0%

commit v1 on v0

v1 whole, which is shorter than its diff:
```python
import functools

import jax
import jax.numpy as jnp
from jax import lax
from jax.experimental import pallas as pl
from jax.experimental.pallas import tpu as pltpu
from jax.sharding import PartitionSpec as P

NORM_FLOOR = 16.0
F32 = jnp.float32
BF16 = jnp.bfloat16
HIGHEST = lax.Precision.HIGHEST
VMEM_LIMIT = 56 * 1024 * 1024


def dot(a, b, ca=1, cb=0, precision=None):
    return lax.dot_general(
        a, b, (((ca,), (cb,)), ((), ())), precision=precision, preferred_element_type=F32
    )


def low(x):
    return x.astype(BF16)


def iotas(n):
    rows = lax.broadcasted_iota(jnp.int32, (n, n), 0)
    cols = lax.broadcasted_iota(jnp.int32, (n, n), 1)
    return rows, cols


def head_columns(beta_pre, decay_pre, rate, g_ref, b_ref, gt_ref):
    n, heads = beta_pre.shape
    rows, cols = iotas(n)
    log_decay = -rate * (jnp.maximum(decay_pre, 0.0) + jnp.log1p(jnp.exp(-jnp.abs(decay_pre))))
    sums = dot((rows >= cols).astype(F32), log_decay, precision=HIGHEST)
    g_ref[...] = jnp.zeros_like(g_ref)
    b_ref[...] = jnp.zeros_like(b_ref)
    g_ref[:, 0:heads] = sums
    b_ref[:, 0:heads] = 1.0 / (1.0 + jnp.exp(-beta_pre))
    gt_ref[...] = jnp.transpose(g_ref[...])


def lane_column(ref, head):
    full = ref[...]
    width = full.shape[1]
    rolled = pltpu.roll(full, lax.rem(width - head, width), 1)
    return jnp.broadcast_to(rolled[:, 0:1], full.shape)


def head_common(q16, k16, head, g_ref, b_ref, gt_ref):
    n, size = k16.shape
    k32, q32 = k16.astype(F32), q16.astype(F32)
    g = lane_column(g_ref, head)
    beta = lane_column(b_ref, head)
    rk = jnp.broadcast_to(
        lax.rsqrt(jnp.sum(k32 * k32, axis=1, keepdims=True) + NORM_FLOOR), (n, size)
    )
    rq = jnp.broadcast_to(
        lax.rsqrt(jnp.sum(q32 * q32, axis=1, keepdims=True) + NORM_FLOOR), (n, size)
    )
    g_row = gt_ref[pl.ds(head, 1), :]
    rk_row = jnp.transpose(rk)[0:1, :]
    rows, cols = iotas(n)
    wide = jnp.concatenate([g] * (n // size), axis=1)
    gamma = jnp.where(rows >= cols, jnp.exp(jnp.minimum(wide - g_row, 0.0)), 0.0)
    gamma_rk = gamma * rk_row
    gram = dot(jnp.concatenate([k16, q16], axis=0), k16, 1, 1)
    scale = size**-0.5
    tile = lambda x: jnp.concatenate([x] * (n // size), axis=1)
    a0 = jnp.where(rows > cols, gram[:n] * gamma_rk * tile(rk), 0.0)
    p = gram[n:] * gamma_rk * tile(rq * scale)
    g_end = g[n - 1 : n, :]
    return dict(
        g=g, beta=beta, rk=rk, rq=rq, k_hat=k32 * rk, q_hat=q32 * (rq * scale), gain=jnp.exp(g),
        tail=jnp.exp(g_end - g), gain_end=jnp.exp(g_end), gamma_rk=gamma_rk, a0=a0, p=p,
        rows=rows, cols=cols, tile=tile, scale=scale,
    )


def unit_lower_inverse(a, rows, cols):
    n = a.shape[0]
    differ = rows ^ cols
    eye = (rows == cols).astype(F32)
    x = eye - jnp.where(differ == 1, a, 0.0)
    size = 2
    while size < n:
        part = jnp.where((differ >= size) & (differ < 2 * size), a, 0.0)
        if 2 * size == n:
            x11, x22 = low(x[:size, :size]), low(x[size:, size:])
            x21 = -dot(x22, low(dot(low(a[size:, :size]), x11)))
            top = x[:size]
            bottom = jnp.concatenate([x21, x[size:, size:]], axis=1)
            x = jnp.concatenate([top, bottom], axis=0)
        else:
            x16 = low(x)
            x = x - dot(x16, low(dot(low(part), x16)))
        size *= 2
    ah = low(a)
    al = low(a - ah.astype(F32))
    xh = low(x)
    xl = low(x - xh.astype(F32))
    product = dot(jnp.concatenate([ah, al, ah], axis=1), jnp.concatenate([xh, xh, xl], axis=0))
    return x + dot(xh, low(eye - x - product))


def local_kernel(pack, q_ref, k_ref, do_ref, bp_ref, dp_ref, rate_ref,
                 tg_ref, inv_ref, dr_ref, y_ref, g_ref, b_ref, gt_ref):
    step = pl.program_id(0)

    @pl.when(step == 0)
    def _():
        head_columns(bp_ref[...], dp_ref[...], rate_ref[...], g_ref, b_ref, gt_ref)

    size = q_ref.shape[1] // pack
    for p in range(pack):
        lanes = slice(p * size, (p + 1) * size)
        h = head_common(q_ref[:, lanes], k_ref[:, lanes], step * pack + p, g_ref, b_ref, gt_ref)
        inv = low(unit_lower_inverse(h["a0"] * h["tile"](h["beta"]), h["rows"], h["cols"]))
        inv_ref[p] = inv
        do16 = do_ref[:, lanes]
        d_written = dot(low(h["p"]), do16, 0, 0)
        k_tail = low(h["k_hat"] * h["tail"])
        both = dot(inv, jnp.concatenate([low(d_written), k_tail], axis=1), 0, 0)
        dr16, y16 = low(both[:, :size]), low(both[:, size:])
        dr_ref[:, lanes] = dr16
        y_ref[:, lanes] = y16
        k_in = low(h["k_hat"] * h["beta"] * h["gain"])
        eye = lax.broadcasted_iota(jnp.int32, (size, size), 0) == lax.broadcasted_iota(
            jnp.int32, (size, size), 1
        )
        transition = jnp.where(eye, h["gain_end"], 0.0) - dot(y16, k_in, 0, 0)
        own = dot(
            jnp.concatenate([low(h["q_hat"] * h["gain"]), -k_in], axis=0),
            jnp.concatenate([do16, dr16], axis=0),
            0,
            0,
        )
        tg_ref[0, p] = low(transition)
        tg_ref[1, p] = low(own)


def offset_kernel(pack, y_ref, v_ref, bp_ref, o_ref, b_ref):
    step = pl.program_id(0)

    @pl.when(step == 0)
    def _():
        b_ref[...] = jnp.zeros_like(b_ref)
        b_ref[:, 0 : bp_ref.shape[1]] = 1.0 / (1.0 + jnp.exp(-bp_ref[...]))

    size = y_ref.shape[1] // pack
    for p in range(pack):
        lanes = slice(p * size, (p + 1) * size)
        beta = lane_column(b_ref, step * pack + p)
        o_ref[p] = low(dot(y_ref[:, lanes], low(v_ref[:, lanes].astype(F32) * beta), 0, 0))


def values_kernel(pack, dr_ref, y_ref, e_ref, bp_ref, dv_ref, b_ref):
    step = pl.program_id(0)

    @pl.when(step == 0)
    def _():
        b_ref[...] = jnp.zeros_like(b_ref)
        b_ref[:, 0 : bp_ref.shape[1]] = 1.0 / (1.0 + jnp.exp(-bp_ref[...]))

    size = y_ref.shape[1] // pack
    for p in range(pack):
        lanes = slice(p * size, (p + 1) * size)
        beta = lane_column(b_ref, step * pack + p)
        dr = dr_ref[:, lanes].astype(F32) + dot(y_ref[:, lanes], e_ref[p])
        dv_ref[:, lanes] = low(dr * beta)


def grads_kernel(pack, q_ref, k_ref, v_ref, do_ref, bp_ref, dp_ref, rate_ref, inv_ref, dr_ref, y_ref, s_ref, e_ref,
                 dq_ref, dk_ref, db_ref, dd_ref, g_ref, b_ref, gt_ref, dg_acc, db_acc):
    step = pl.program_id(0)

    @pl.when(step == 0)
    def _():
        head_columns(bp_ref[...], dp_ref[...], rate_ref[...], g_ref, b_ref, gt_ref)
        dg_acc[...] = jnp.zeros_like(dg_acc)
        db_acc[...] = jnp.zeros_like(db_acc)

    size = q_ref.shape[1] // pack
    n = q_ref.shape[0]
    lane = lax.broadcasted_iota(jnp.int32, (n, size), 1)
    row = lax.broadcasted_iota(jnp.int32, (n, size), 0)
    for p in range(pack):
        lanes = slice(p * size, (p + 1) * size)
        head = step * pack + p
        k16, q16, do16 = k_ref[:, lanes], q_ref[:, lanes], do_ref[:, lanes]
        h = head_common(q16, k16, head, g_ref, b_ref, gt_ref)
        beta, rk, k_hat, q_hat, gain, tail = (
            h["beta"], h["rk"], h["k_hat"], h["q_hat"], h["gain"], h["tail"]
        )
        s16, e16 = s_ref[p], e_ref[p]
        inner = v_ref[:, lanes].astype(F32) - gain * (rk * dot(k16, s16))
        written = dot(inv_ref[p], low(beta * inner))
        w16 = low(written)
        dr = dr_ref[:, lanes].astype(F32) + dot(y_ref[:, lanes], e16)
        dr16 = low(dr)
        pair = dot(jnp.concatenate([dr16, do16], axis=0), w16, 1, 1)
        d_a, d_p = -pair[:n], pair[n:]
        weights = d_a * h["a0"] * h["tile"](beta) + d_p * h["p"]
        x1 = low(jnp.where(h["rows"] > h["cols"], d_a * h["gamma_rk"], 0.0))
        x2 = low(d_p * h["gamma_rk"])
        xs = jnp.concatenate([x1, x2], axis=0)
        row_side = dot(xs, k16)
        col_side = dot(xs, jnp.concatenate([low(beta * k_hat), low(q_hat)], axis=0), 0, 0)
        at_s = dot(jnp.concatenate([do16, dr16], axis=0), s16, 1, 1)
        d_qd, dr_s = at_s[:n], at_s[n:]
        d_kt = dot(w16, e16, 1, 1)
        d_q = row_side[n:] + gain * d_qd
        in_term = beta * gain * dr_s
        d_k = rk * (beta * row_side[:n] - in_term + tail * d_kt) + col_side
        unit = q_ref[:, lanes].astype(F32) * h["rq"]
        d_q = h["rq"] * h["scale"] * (d_q - unit * jnp.sum(unit * d_q, axis=1, keepdims=True))
        d_k = d_k - k_hat * jnp.sum(k_hat * d_k, axis=1, keepdims=True)
        dq_ref[:, lanes] = low(d_q)
        dk_ref[:, lanes] = low(d_k)
        tail_term = d_kt * k_hat * tail
        direct = gain * d_qd * q_hat - in_term * k_hat - tail_term
        row_sum = jnp.sum(weights, axis=1, keepdims=True) + jnp.sum(direct, axis=1, keepdims=True)
        col_sum = jnp.sum(weights, axis=0, keepdims=True)
        col_sum = jnp.transpose(jnp.broadcast_to(col_sum, (size, n)))
        end = jnp.sum(tail_term, axis=(0, 1), keepdims=True) + jnp.sum(
            h["gain_end"] * (s16.astype(F32) * e16.astype(F32)), axis=(0, 1), keepdims=True
        )
        dg = row_sum - col_sum + jnp.where(row == n - 1, end, 0.0)
        dg_acc[...] = jnp.where(lane == head, dg, dg_acc[...])
        d_beta = jnp.sum(dr * written, axis=1, keepdims=True)
        db_acc[...] = jnp.where(lane == head, (1.0 - beta) * d_beta, db_acc[...])

    @pl.when(step == pl.num_programs(0) - 1)
    def _():
        heads = bp_ref.shape[1]
        rows, cols = iotas(n)
        d_log = dot((rows <= cols).astype(F32), dg_acc[...], precision=HIGHEST)
        slope = -rate_ref[...] / (1.0 + jnp.exp(-dp_ref[...]))
        dd_ref[...] = d_log[:, 0:heads] * slope
        db_ref[...] = db_acc[:, 0:heads]


def call(body, grid, ins, outs, scratch, name, flops):
    specs = lambda items: [pl.BlockSpec(block, index) for _, block, index in items]
    return pl.pallas_call(
        body,
        grid=(grid,),
        in_specs=specs(ins),
        out_specs=specs(outs),
        out_shape=[a for a, _, _ in outs],
        scratch_shapes=scratch,
        compiler_params=pltpu.CompilerParams(
            dimension_semantics=("arbitrary",), vmem_limit_bytes=VMEM_LIMIT
        ),
        cost_estimate=pl.CostEstimate(flops=flops, bytes_accessed=1 << 20, transcendentals=0),
        name=name,
    )(*[a for a, _, _ in ins])


def shape(dims, dtype):
    return jax.ShapeDtypeStruct(dims, dtype)


def group_total_kernel(group, pos_ref, tg_ref, total_ref):
    pos = pos_ref[0]
    heads = tg_ref.shape[2]
    for i in range(heads):
        slot = pos ^ (group - 1)
        t, g = tg_ref[slot, 0, i].astype(F32), tg_ref[slot, 1, i].astype(F32)
        for j in range(group - 2, -1, -1):
            slot = pos ^ j
            tj = tg_ref[slot, 0, i]
            g = tg_ref[slot, 1, i].astype(F32) + dot(tj, low(g), 0, 0)
            t = dot(low(t), tj)
        total_ref[0, i] = low(t)
        total_ref[1, i] = low(g)


def group_total_forward_kernel(group, pos_ref, tg_ref, o_ref, total_ref):
    pos = pos_ref[0]
    heads = tg_ref.shape[2]
    for i in range(heads):
        t, o = tg_ref[pos, 0, i].astype(F32), o_ref[pos, i].astype(F32)
        for j in range(1, group):
            slot = pos ^ j
            tj = tg_ref[slot, 0, i]
            o = o_ref[slot, i].astype(F32) + dot(tj, low(o))
            t = dot(tj, low(t))
        total_ref[0, i] = low(t)
        total_ref[1, i] = low(o)


def join_kernel(backward, own_ref, far_ref, out_ref):
    for i in range(own_ref.shape[1]):
        near, far = own_ref[0, i], far_ref[0, i]
        if backward:
            out_ref[1, i] = low(own_ref[1, i].astype(F32) + dot(near, far_ref[1, i], 0, 0))
            out_ref[0, i] = low(dot(far, near))
        else:
            out_ref[1, i] = low(own_ref[1, i].astype(F32) + dot(near, far_ref[1, i]))
            out_ref[0, i] = low(dot(near, far))


def spread_back_kernel(group, pos_ref, tg_ref, near_ref, far_ref, out_ref):
    pos = pos_ref[0]
    for i in range(tg_ref.shape[2]):
        e = near_ref[1, i].astype(F32) + dot(near_ref[0, i], far_ref[i], 0, 0)
        for j in range(group - 1, -1, -1):
            slot = pos ^ j
            out_ref[slot, i] = low(e)
            if j:
                e = tg_ref[slot, 1, i].astype(F32) + dot(tg_ref[slot, 0, i], low(e), 0, 0)


def spread_forward_kernel(group, pos_ref, tg_ref, o_ref, near_ref, far_ref, out_ref):
    pos = pos_ref[0]
    for i in range(tg_ref.shape[2]):
        s = near_ref[1, i].astype(F32) + dot(near_ref[0, i], far_ref[i])
        for j in range(group):
            slot = pos ^ j
            out_ref[slot, i] = low(s)
            if j < group - 1:
                s = o_ref[slot, i].astype(F32) + dot(tg_ref[slot, 0, i], low(s))


def small_call(body, name, out_shape, args, flops):
    specs = [
        pl.BlockSpec(memory_space=pltpu.SMEM if a.dtype == jnp.int32 else pltpu.VMEM) for a in args
    ]
    return pl.pallas_call(
        body,
        in_specs=specs,
        out_specs=pl.BlockSpec(memory_space=pltpu.VMEM),
        out_shape=out_shape,
        cost_estimate=pl.CostEstimate(flops=flops, bytes_accessed=1 << 20, transcendentals=0),
        name=name,
    )(*args)


def group_size(count, heads):
    size = 1
    while size * size < count and count % (2 * size) == 0 and heads % (2 * size) == 0:
        size *= 2
    return size


def per_device(queries, keys, hidden, value_weight, beta_pre, decay_pre, decay_rate, out_grad):
    heads = decay_rate.shape[0]
    n, width = queries.shape
    dk = width // heads
    dv = value_weight.shape[1] // heads
    model = hidden.shape[1]
    spans = lax.axis_size("sp")
    group = group_size(spans, heads)
    outer = spans // group
    place = lax.axis_index("sp")
    pos = lax.rem(place, group)
    lead = lax.div(place, group)
    pos_arr = jnp.full((1,), pos, jnp.int32)
    share = heads // group
    pack = 2
    steps = heads // pack
    rate = decay_rate.reshape(1, heads)
    full = lambda a: (a, a.shape, lambda i: (0,) * a.ndim)
    cols = lambda a, w: (a, (n, pack * w), lambda i: (0, i))
    first = lambda a: (a, (pack,) + a.shape[1:], lambda i: (i,) + (0,) * (a.ndim - 1))
    big = heads * n * n * 256

    def near(x, d):
        return lax.ppermute(x, "sp", [(s, s ^ d) for s in range(spans)])

    def along(x, d):
        return lax.ppermute(
            x, "sp", [(s, s + d * group) for s in range(spans) if 0 <= s + d * group < spans]
        )

    rows = model // spans
    by_owner = hidden.reshape(n, outer, group, rows)

    def hidden_part(d):
        return lax.dynamic_index_in_dim(by_owner, pos ^ d, 2, False).reshape(n, outer * rows)

    hidden_parts = [hidden_part(0)] + [near(hidden_part(d), d) for d in range(1, group)]

    tg_shape = shape((2, heads, dk, dk), BF16)
    col_scratch = [pltpu.VMEM((n, 128), F32), pltpu.VMEM((n, 128), F32), pltpu.VMEM((128, n), F32)]
    tg, inv, dr, y = call(
        functools.partial(local_kernel, pack),
        steps,
        [cols(queries, dk), cols(keys, dk), cols(out_grad, dv), full(beta_pre), full(decay_pre), full(rate)],
        [
            (tg_shape, (2, pack, dk, dk), lambda i: (0, i, 0, 0)),
            first(shape((heads, n, n), BF16)),
            cols(shape((n, width), BF16), dv),
            cols(shape((n, width), BF16), dk),
        ],
        col_scratch,
        "local",
        big,
    )

    def to_shares(x, axis):
        parts = []
        for d in range(group):
            piece = lax.dynamic_slice_in_dim(x, (pos ^ d) * share, share, axis)
            parts.append(near(piece, d) if d else piece)
        return jnp.stack(parts)

    def from_shares(x):
        parts = [near(x[d], d) if d else x[d] for d in range(group)]
        ordered = lax.dynamic_update_slice_in_dim
        out = jnp.zeros((heads,) + x.shape[2:], x.dtype)
        for d in range(group):
            out = ordered(out, parts[d], (pos ^ d) * share, 0)
        return out

    small = group * share * dk * dk * dk * 4

    def scan_outer(total, backward):
        sign = -1 if backward else 1
        reach = 1
        inclusive, nearest = total, None
        while True:
            last = 2 * reach >= outer
            if nearest is None:
                nearest = along(inclusive, sign * reach)
                if last:
                    return nearest, jnp.zeros_like(nearest[1])
                inclusive = small_call(
                    functools.partial(join_kernel, backward), "join",
                    shape(total.shape, BF16), [inclusive, nearest], small,
                )
            elif last:
                return nearest, along(inclusive[1], sign * reach)
            else:
                far = along(inclusive, sign * reach)
                join = lambda a, b: small_call(
                    functools.partial(join_kernel, backward), "join",
                    shape(total.shape, BF16), [a, b], small,
                )
                nearest, inclusive = join(nearest, far), join(inclusive, far)
            reach *= 2

    share_shape = shape((2, share, dk, dv), BF16)
    spread_shape = shape((group, share, dk, dv), BF16)

    tg_shared = to_shares(tg, 1)
    back_total = small_call(
        functools.partial(group_total_kernel, group), "total_back", share_shape, [pos_arr, tg_shared], small
    )
    b_near, b_far = scan_outer(back_total, True)
    ends = small_call(
        functools.partial(spread_back_kernel, group), "spread_back", spread_shape,
        [pos_arr, tg_shared, b_near, b_far], small,
    )
    end_grad = from_shares(ends)

    (d_values,) = call(
        functools.partial(values_kernel, pack),
        steps,
        [cols(dr, dv), cols(y, dk), first(end_grad), full(beta_pre)],
        [cols(shape((n, width), BF16), dv)],
        [pltpu.VMEM((n, 128), F32)],
        "values",
        heads * n * dk * dv * 2,
    )
    grad_parts = [d_values] + [near(d_values, d) for d in range(1, group)]
    partial = sum(
        lax.dot_general(a, b, (((0,), (0,)), ((), ())), preferred_element_type=F32)
        for a, b in zip(hidden_parts, grad_parts)
    ).reshape(outer, rows, width)
    d_weight = lax.dynamic_index_in_dim(partial, lead, 0, False)
    for e in range(1, outer):
        target = lax.rem(lead + e, outer)
        piece = lax.dynamic_index_in_dim(partial, target, 0, False).astype(BF16)
        moved = lax.ppermute(
            piece, "sp", [(s, (s + e * group) % spans) for s in range(spans)]
        )
        d_weight = d_weight + moved.astype(F32)

    values = jnp.dot(hidden, value_weight, preferred_element_type=F32).astype(BF16)
    (offset,) = call(
        functools.partial(offset_kernel, pack),
        steps,
        [cols(y, dk), cols(values, dv), full(beta_pre)],
        [first(shape((heads, dk, dv), BF16))],
        [pltpu.VMEM((n, 128), F32)],
        "offset",
        heads * n * dk * dv * 2,
    )
    offset_shared = to_shares(offset, 0)
    forward_total = small_call(
        functools.partial(group_total_forward_kernel, group), "total_forward", share_shape,
        [pos_arr, tg_shared, offset_shared], small,
    )
    f_near, f_far = scan_outer(forward_total, False)
    starts = small_call(
        functools.partial(spread_forward_kernel, group), "spread_forward", spread_shape,
        [pos_arr, tg_shared, offset_shared, f_near, f_far], small,
    )
    start_state = from_shares(starts)

    core = lax.axis_index("tp")
    cores = lax.axis_size("tp")
    own_rows = n // cores

    def input_grad(which):
        piece = lax.dynamic_slice_in_dim(d_values, which * own_rows, own_rows, 0)
        return lax.dot_general(
            piece, value_weight, (((1,), (1,)), ((), ())), preferred_element_type=F32
        )

    d_hidden = input_grad(core)
    for d in range(1, cores):
        moved = lax.ppermute(
            input_grad(lax.rem(core + d, cores)).astype(BF16),
            "tp",
            [(c, (c + d) % cores) for c in range(cores)],
        )
        d_hidden = d_hidden + moved.astype(F32)
    d_hidden = d_hidden.astype(BF16)

    d_queries, d_keys, d_beta, d_decay = call(
        functools.partial(grads_kernel, pack),
        steps,
        [
            cols(queries, dk), cols(keys, dk), cols(values, dv), cols(out_grad, dv), full(beta_pre), full(decay_pre),
            full(rate), first(inv), cols(dr, dv), cols(y, dk), first(start_state), first(end_grad),
        ],
        [
            cols(shape((n, width), BF16), dk),
            cols(shape((n, width), BF16), dk),
            full(shape((n, heads), F32)),
            full(shape((n, heads), F32)),
        ],
        col_scratch + [pltpu.VMEM((n, dk), F32), pltpu.VMEM((n, dk), F32)],
        "grads",
        big,
    )
    return (d_queries, d_keys, d_beta, d_decay, d_hidden, d_weight)


def solution(mesh):
    return jax.shard_map(
        per_device,
        mesh=mesh,
        in_specs=(
            P("sp", "tp"),
            P("sp", "tp"),
            P("sp", None),
            P(None, "tp"),
            P("sp", "tp"),
            P("sp", "tp"),
            P("tp"),
            P("sp", "tp"),
        ),
        out_specs=(
            P("sp", "tp"),
            P("sp", "tp"),
            P("sp", "tp"),
            P("sp", "tp"),
            P(("sp", "tp"), None),
            P("sp", "tp"),
        ),
        check_vma=False,
    )
```

time: 835 us -> 180 us (0.22); the launches traced: 824 us -> 179 us
  waiting for transfers between devices: 335 us -> 36.8 us
  matrix products: 236 us -> 14.2 us
  other arithmetic: 181 us -> 2.53 us
  Pallas kernels: 0 us -> 66.9 us
  starting transfers between devices: 0.92 us -> 40.2 us
  local copies, waits for them, and re-layouts: 53.3 us -> 17.2 us
  between operations: 15.5 us -> 0.96 us
    dot_general x99 -> x7, matrix products: 223 us -> 14.2 us  [the longest x2 5.99 us: input_grad(): lax.dot_general(piece, value_weight, (((1,), (1,)), ((), ())), preferred_...]
    all_gather x4 -> x0, waiting for transfers between devices: 203 us -> none  [prefix(): lax.all_gather(a.astype(kind), axis)]
    another operation x6 -> x2, other arithmetic: 162 us -> 1.6 us  [to_shares(): return jnp.stack(parts)]
    reduce_scatter x2 -> x0, waiting for transfers between devices: 131 us -> none  [the longest x1 120 us: per_device(): lax.psum_scatter(weight_term(hidden, [local_grad, carried_grad]), 'sp', s...]
    pallas_call x0 -> x10, Pallas kernels: none -> 66.9 us  [the longest x4 53 us: call(): pl.pallas_call(body, grid=(grid,), in_specs=specs(ins), out_specs=specs(o...]
    ppermute x0 -> x26, starting transfers between devices: none -> 40.2 us  [the longest x18 22.9 us: near(): return lax.ppermute(x, 'sp', [(s, s ^ d) for s in range(spans)])]
    ppermute x0 -> x26, waiting for transfers between devices: none -> 36.8 us  [the longest x18 22.4 us: near(): return lax.ppermute(x, 'sp', [(s, s ^ d) for s in range(spans)])]
    another operation x5 -> x0, matrix products: 13.1 us -> none  [the longest x3 7.27 us: span_pieces(): jax.scipy.linalg.solve_triangular(system, right_side, lower=True, unit_di...]
  transfers between devices with their start and end apart: 6 -> 26, of which waited for: 5 -> 11; matrix products, arithmetic and copies ran while one was open for 19% -> 11% of each run, Pallas kernels for 0% -> 15%
where the time goes in v1:
time: 180 us; the launch traced here: 179 us
  Pallas kernels  66.9 us (37%)
  starting transfers between devices  40.2 us (22%)
  waiting for transfers between devices  36.8 us (20%)
  local copies, waits for them, and re-layouts  17.2 us (10%)
  matrix products  14.2 us (8%)
  other arithmetic  2.53 us (1%)
    pallas_call x4, Pallas kernels, call(): pl.pallas_call(body, grid=(grid,), in_specs=specs(ins), out_specs=specs(o...  53 us
    ppermute x18, starting transfers between devices, near(): return lax.ppermute(x, 'sp', [(s, s ^ d) for s in range(spans)])  22.9 us
    ppermute x18, waiting for transfers between devices, near(): return lax.ppermute(x, 'sp', [(s, s ^ d) for s in range(spans)])  22.4 us
    ppermute x3, waiting for transfers between devices, per_device(): lax.ppermute(piece, 'sp', [(s, (s + e * group) % spans) for s in range(sp...  14.3 us
    pallas_call x6, Pallas kernels, small_call(): pl.pallas_call(body, in_specs=specs, out_specs=pl.BlockSpec(memory_space=...  13.9 us
    ppermute x4, starting transfers between devices, along(): lax.ppermute(x, 'sp', [(s, s + d * group) for s in range(spans) if 0 <= s...  11.8 us
    unnamed x27, local copies, waits for them, and re-layouts  10.6 us
    dot_general x2, matrix products, input_grad(): lax.dot_general(piece, value_weight, (((1,), (1,)), ((), ())), preferred_...  5.99 us
  transfers between devices with their start and end apart: 26, of which 11 were waited for; matrix products, arithmetic and copies ran while one was open for 11% of the time, Pallas kernels for 15%

profile of v1, /device:TPU:0, one launch (start us, length us, event | category | flops | bytes accessed | tf_op | source)
XLA Modules:
  0.0 178.8 jit_solution(15472430447473404917)
XLA Ops:
  2.1 1.5 copy.34.dp_ref
  3.6 4.6 %convolution_convert_fusion.1.v_ref = bf16[256,1024]{1,0:T(8,128)(2,1)} fusion(bf16[256,2048]{1,0:T(8,128)(2,1)} %param.10, bf16[2048,1024]{1,0:T(8,128)(2,1)} %param.11), kind=kOutput, calls=%fused_computation.4 | convolution fusion | flops 1074003968 | bytes 5767168 | tf_op jit(solution)/shard_map/dot_general | solution.py:483
  8.2 32.6 %local.1 = (bf16[2,8,128,128]{3,2,1,0:T(8,128)(2,1)}, bf16[8,256,256]{2,1,0:T(8,128)(2,1)}, bf16[256,1024]{1,0:T(8,128)(2,1)}, bf16[256,1024]{1,0:T(8,128)(2,1)}) custom-call(bf16[256,1024]{1,0:T(8,128)(2,1)} %q_ref.3, bf16[256,1024]{1,0:T(8,128)(2,1)} %k_ref.3, bf16[256,1024]{1,0:T(8,128)(2,1)} %do_ref.3, f32[256,8]{1,0:T(8,128)} %copy.33.bp_ref, ...), custom_call_target="tpu_custom_call" | custom-call | flops 134217728 | bytes 1048576 | tf_op jit(solution)/shard_map/local/pallas_call | solution.py:247
  40.7 4.3 %offset.1 = bf16[8,128,128]{2,1,0:T(8,128)(2,1)} custom-call(bf16[256,1024]{1,0:T(8,128)(2,1)} %get-tuple-element.16.y_ref, bf16[256,1024]{1,0:T(8,128)(2,1)} %convolution_convert_fusion.1.v_ref, f32[256,8]{1,0:T(8,128)} %copy.33.bp_ref), custom_call_target="tpu_custom_call" | custom-call | flops 67108864 | bytes 1048576 | tf_op jit(solution)/shard_map/offset/pallas_call | solution.py:247
  46.0 4.0 %collective-permute-start.5 = (bf16[2,128,128]{2,1,0:T(8,128)(2,1)S(1)}, bf16[2,128,128]{2,1,0:T(8,128)(2,1)S(1)}, u32[]{:S(2)}, u32[]{:S(2)}) collective-permute-start(bf16[2,128,128]{2,1,0:T(8,128)(2,1)S(1)} %get-tuple-element.58), channel_id=1, source_target_pairs={{0,6},{2,4},{4,2},{6,0},{8,14},{10,12},{12,10},{14,8},{16,22},{18,... | collective-permute-start | bytes 196616 | tf_op jit(solution)/shard_map/ppermute | solution.py:372
  50.6 2.9 %collective-permute-start.2 = (bf16[2,2,128,128]{3,2,1,0:T(8,128)(2,1)S(1)}, bf16[2,2,128,128]{3,2,1,0:T(8,128)(2,1)S(1)}, u32[]{:S(2)}, u32[]{:S(2)}) collective-permute-start(bf16[2,2,128,128]{3,2,1,0:T(8,128)(2,1)S(1)} %get-tuple-element.48), channel_id=1, source_target_pairs={{0,6},{2,4},{4,2},{6,0},{8,14},{10,12},{12,10},{14,8},{16,22},{18,... | collective-permute-start | bytes 393224 | tf_op jit(solution)/shard_map/ppermute | solution.py:372
  56.4 2.6 %collective-permute-done.2 = bf16[2,2,128,128]{3,2,1,0:T(8,128)(2,1)S(1)} collective-permute-done((bf16[2,2,128,128]{3,2,1,0:T(8,128)(2,1)S(1)}, bf16[2,2,128,128]{3,2,1,0:T(8,128)(2,1)S(1)}, u32[]{:S(2)}, u32[]{:S(2)}) %collective-permute-start.2) | collective-permute-done | bytes 131104 | tf_op jit(solution)/shard_map/ppermute | solution.py:372
  60.8 2.5 %total_forward.1.own_ref = bf16[2,2,128,128]{3,2,1,0:T(8,128)(2,1)} custom-call(s32[1]{0:T(128)} %bitcast.1.pos_ref, bf16[4,2,2,128,128]{4,3,2,1,0:T(8,128)(2,1)} %pad_maximum_fusion.tg_ref, bf16[4,2,128,128]{3,2,1,0:T(8,128)(2,1)} %pad_maximum_fusion.1.o_ref), custom_call_target="tpu_custom_call" | custom-call | flops 67108864 | bytes 1048576 | tf_op jit(solution)/shard_map/total_forward/pallas_call | solution.py:332
  63.3 3.5 %collective-permute-start.6 = (bf16[2,2,128,128]{3,2,1,0:T(8,128)(2,1)}, bf16[2,2,128,128]{3,2,1,0:T(8,128)(2,1)S(1)}, u32[]{:S(2)}, u32[]{:S(2)}) collective-permute-start(bf16[2,2,128,128]{3,2,1,0:T(8,128)(2,1)} %total_forward.1.own_ref), channel_id=1, source_target_pairs={{0,8},{2,10},{4,12},{6,14},{8,16},{10,18},{12,20},{14,22},{16,24},... | collective-permute-start | bytes 393224 | tf_op jit(solution)/shard_map/ppermute | solution.py:375
  69.0 1.5 collective-permute-start.21
  70.5 2.4 %total_back.1.own_ref = bf16[2,2,128,128]{3,2,1,0:T(8,128)(2,1)} custom-call(s32[1]{0:T(128)} %bitcast.1.pos_ref, bf16[4,2,2,128,128]{4,3,2,1,0:T(8,128)(2,1)} %pad_maximum_fusion.tg_ref), custom_call_target="tpu_custom_call" | custom-call | flops 67108864 | bytes 1048576 | tf_op jit(solution)/shard_map/total_back/pallas_call | solution.py:332
  74.9 1.8 %join.2 = bf16[2,2,128,128]{3,2,1,0:T(8,128)(2,1)} custom-call(bf16[2,2,128,128]{3,2,1,0:T(8,128)(2,1)} %total_forward.1.own_ref, bf16[2,2,128,128]{3,2,1,0:T(8,128)(2,1)} %copy-done.5), custom_call_target="tpu_custom_call" | custom-call | flops 67108864 | bytes 1048576 | tf_op jit(solution)/shard_map/join/pallas_call | solution.py:332
  77.5 5.5 %collective-permute-start.7 = (bf16[2,128,128]{2,1,0:T(8,128)(2,1)S(1)}, bf16[2,128,128]{2,1,0:T(8,128)(2,1)S(1)}, u32[]{:S(2)}, u32[]{:S(2)}) collective-permute-start(bf16[2,128,128]{2,1,0:T(8,128)(2,1)S(1)} %slice_bitcast_fusion.9), channel_id=1, source_target_pairs={{0,16},{2,18},{4,20},{6,22},{8,24},{10,26},{12,28},{14,30},{1,17},... | collective-permute-start | bytes 196616 | tf_op jit(solution)/shard_map/ppermute | solution.py:375
  83.7 1.8 %join.3 = bf16[2,2,128,128]{3,2,1,0:T(8,128)(2,1)} custom-call(bf16[2,2,128,128]{3,2,1,0:T(8,128)(2,1)} %total_back.1.own_ref, bf16[2,2,128,128]{3,2,1,0:T(8,128)(2,1)} %copy-done.6), custom_call_target="tpu_custom_call" | custom-call | flops 67108864 | bytes 1048576 | tf_op jit(solution)/shard_map/join/pallas_call | solution.py:332
  88.5 2.7 %spread_forward.1 = bf16[4,2,128,128]{3,2,1,0:T(8,128)(2,1)} custom-call(s32[1]{0:T(128)} %bitcast.1.pos_ref, bf16[4,2,2,128,128]{4,3,2,1,0:T(8,128)(2,1)} %pad_maximum_fusion.tg_ref, bf16[4,2,128,128]{3,2,1,0:T(8,128)(2,1)} %pad_maximum_fusion.1.o_ref, bf16[2,2,128,128]{3,2,1,0:T(8,128)(2,1)} %copy-done.5, bf16[2,128,128]{2,1,0:T(8,128)(2,1)} %copy-done.10), custom_call_target="tpu_custom_call" | custom-call | flops 67108864 | bytes 1048576 | tf_op jit(solution)/shard_map/spread_forward/pallas_call | solution.py:332
  94.7 2.7 %spread_back.1 = bf16[4,2,128,128]{3,2,1,0:T(8,128)(2,1)} custom-call(s32[1]{0:T(128)} %bitcast.1.pos_ref, bf16[4,2,2,128,128]{4,3,2,1,0:T(8,128)(2,1)} %pad_maximum_fusion.tg_ref, bf16[2,2,128,128]{3,2,1,0:T(8,128)(2,1)} %copy-done.6, bf16[2,128,128]{2,1,0:T(8,128)(2,1)} %copy-done.9), custom_call_target="tpu_custom_call" | custom-call | flops 67108864 | bytes 1048576 | tf_op jit(solution)/shard_map/spread_back/pallas_call | solution.py:332
  100.3 2.3 %collective-permute-done.13 = bf16[2,128,128]{2,1,0:T(8,128)(2,1)S(1)} collective-permute-done((bf16[2,128,128]{2,1,0:T(8,128)(2,1)S(1)}, bf16[2,128,128]{2,1,0:T(8,128)(2,1)S(1)}, u32[]{:S(2)}, u32[]{:S(2)}) %collective-permute-start.13) | collective-permute-done | bytes 65568 | tf_op jit(solution)/shard_map/ppermute | solution.py:372
  103.7 3.3 %collective-permute-done.14 = bf16[2,128,128]{2,1,0:T(8,128)(2,1)S(1)} collective-permute-done((bf16[2,128,128]{2,1,0:T(8,128)(2,1)S(1)}, bf16[2,128,128]{2,1,0:T(8,128)(2,1)S(1)}, u32[]{:S(2)}, u32[]{:S(2)}) %collective-permute-start.14) | collective-permute-done | bytes 65568 | tf_op jit(solution)/shard_map/ppermute | solution.py:372
  106.9 1.5 collective-permute-start.15
  108.5 3.6 %collective-permute-done.15 = bf16[2,128,128]{2,1,0:T(8,128)(2,1)S(1)} collective-permute-done((bf16[2,128,128]{2,1,0:T(8,128)(2,1)S(1)}, bf16[2,128,128]{2,1,0:T(8,128)(2,1)S(1)}, u32[]{:S(2)}, u32[]{:S(2)}) %collective-permute-start.15) | collective-permute-done | bytes 65568 | tf_op jit(solution)/shard_map/ppermute | solution.py:372
  113.8 4.1 %values.1 = bf16[256,1024]{1,0:T(8,128)(2,1)} custom-call(bf16[256,1024]{1,0:T(8,128)(2,1)} %get-tuple-element.15.dr_ref, bf16[256,1024]{1,0:T(8,128)(2,1)} %get-tuple-element.16.y_ref, bf16[8,128,128]{2,1,0:T(8,128)(2,1)} %copy-done.2, f32[256,8]{1,0:T(8,128)} %copy.33.bp_ref), custom_call_target="tpu_custom_call" | custom-call | flops 67108864 | bytes 1048576 | tf_op jit(solution)/shard_map/values/pallas_call | solution.py:247
  117.9 1.5 collective-permute-start.10
  120.6 3.2 %collective-permute-done.10 = bf16[2,128,128]{2,1,0:T(8,128)(2,1)S(1)} collective-permute-done((bf16[2,128,128]{2,1,0:T(8,128)(2,1)S(1)}, bf16[2,128,128]{2,1,0:T(8,128)(2,1)S(1)}, u32[]{:S(2)}, u32[]{:S(2)}) %collective-permute-start.10) | collective-permute-done | bytes 65568 | tf_op jit(solution)/shard_map/ppermute | solution.py:372
  125.7 12.0 %grads.1 = (bf16[256,1024]{1,0:T(8,128)(2,1)}, bf16[256,1024]{1,0:T(8,128)(2,1)}, f32[256,8]{1,0:T(8,128)}, f32[256,8]{1,0:T(8,128)}) custom-call(bf16[256,1024]{1,0:T(8,128)(2,1)} %q_ref.3, bf16[256,1024]{1,0:T(8,128)(2,1)} %k_ref.3, bf16[256,1024]{1,0:T(8,128)(2,1)} %convolution_convert_fusion.1.v_ref, bf16[256,1024]{1,0:T(8,128)(2,1)} %do_ref.3, ...), custom_call_target="tpu_custom_call" | custom-call | flops 134217728 | bytes 1048576 | tf_op jit(solution)/shard_map/grads/pallas_call | solution.py:247
  137.7 1.6 copy.37
  139.2 1.6 copy.38
  140.8 3.7 %convolution_convert_fusion = bf16[128,2048]{1,0:T(8,128)(2,1)S(1)} fusion(bf16[2048,1024]{1,0:T(8,128)(2,1)} %param.11, bf16[256,1024]{1,0:T(8,128)(2,1)S(1)} %copy-done.1, s32[]{:T(128)S(6)} %select_n.61), kind=kOutput, calls=%fused_computation.2 | convolution fusion | flops 537133056 | bytes 4980740 | tf_op jit(solution)/shard_map/dot_general | solution.py:511
  149.3 5.8 %collective-permute-done.22 = bf16[256,1024]{1,0:T(8,128)(2,1)S(1)} collective-permute-done((bf16[256,1024]{1,0:T(8,128)(2,1)S(1)}, bf16[256,1024]{1,0:T(8,128)(2,1)S(1)}, u32[]{:S(2)}, u32[]{:S(2)}) %collective-permute-start.22) | collective-permute-done | bytes 524320 | tf_op jit(solution)/shard_map/ppermute | solution.py:372
  155.7 4.5 %collective-permute-start.25 = (bf16[128,1024]{1,0:T(8,128)(2,1)S(1)}, bf16[128,1024]{1,0:T(8,128)(2,1)S(1)}, u32[]{:S(2)}, u32[]{:S(2)}) collective-permute-start(bf16[128,1024]{1,0:T(8,128)(2,1)S(1)} %get-tuple-element.41), channel_id=1, source_target_pairs={{0,24},{2,26},{4,28},{6,30},{8,0},{10,2},{12,4},{14,6},{16,8},{18,... | collective-permute-start | bytes 786440 | tf_op jit(solution)/shard_map/ppermute | solution.py:478
  161.2 2.3 %fusion = bf16[128,2048]{1,0:T(8,128)(2,1)} fusion(bf16[2048,1024]{1,0:T(8,128)(2,1)S(1)} %copy-done, bf16[128,2048]{1,0:T(8,128)(2,1)S(1)} %collective-permute-done.16, bf16[256,1024]{1,0:T(8,128)(2,1)S(1)} %copy-done.1, s32[]{:T(128)S(6)} %select_n.60), kind=kOutput, calls=%fused_computation.1 | convolution fusion | flops 537657344 | bytes 5505028 | tf_op jit(solution)/shard_map/dot_general | solution.py:511
  163.5 2.9 %collective-permute-done.25 = bf16[128,1024]{1,0:T(8,128)(2,1)S(1)} collective-permute-done((bf16[128,1024]{1,0:T(8,128)(2,1)S(1)}, bf16[128,1024]{1,0:T(8,128)(2,1)S(1)}, u32[]{:S(2)}, u32[]{:S(2)}) %collective-permute-start.25) | collective-permute-done | bytes 262176 | tf_op jit(solution)/shard_map/ppermute | solution.py:478
  166.4 11.4 %collective-permute-done.24 = bf16[128,1024]{1,0:T(8,128)(2,1)S(1)} collective-permute-done((bf16[128,1024]{1,0:T(8,128)(2,1)S(1)}, bf16[128,1024]{1,0:T(8,128)(2,1)S(1)}, u32[]{:S(2)}, u32[]{:S(2)}) %collective-permute-start.24) | collective-permute-done | bytes 262176 | tf_op jit(solution)/shard_map/ppermute | solution.py:478
  (85 shorter events, 35.7 us)
Async XLA Ops:
  8.2 46.3 %copy-start.4 = (bf16[256,2048]{1,0:T(8,128)(2,1)S(1)}, bf16[256,2048]{1,0:T(8,128)(2,1)}, u32[]{:S(2)}) copy-start(bf16[256,2048]{1,0:T(8,128)(2,1)} %param.10) | copy-start | bytes 3145732
  40.7 9.9 %copy-start.7 = (bf16[2,8,128,128]{3,2,1,0:T(8,128)(2,1)S(1)}, bf16[2,8,128,128]{3,2,1,0:T(8,128)(2,1)}, u32[]{:S(2)}) copy-start(bf16[2,8,128,128]{3,2,1,0:T(8,128)(2,1)} %get-tuple-element.17) | copy-start | bytes 1572868
  46.0 8.1 %collective-permute-start.5 = (bf16[2,128,128]{2,1,0:T(8,128)(2,1)S(1)}, bf16[2,128,128]{2,1,0:T(8,128)(2,1)S(1)}, u32[]{:S(2)}, u32[]{:S(2)}) collective-permute-start(bf16[2,128,128]{2,1,0:T(8,128)(2,1)S(1)} %get-tuple-element.58), channel_id=1, source_target_pairs={{0,6},{2,4},{4,2},{6,0},{8,14},{10,12},{12,10},{14,8},{16,22},{18,... | collective-permute-start | bytes 196616 | tf_op jit(solution)/shard_map/ppermute | solution.py:372
  50.0 5.7 %collective-permute-start.4 = (bf16[2,128,128]{2,1,0:T(8,128)(2,1)S(1)}, bf16[2,128,128]{2,1,0:T(8,128)(2,1)S(1)}, u32[]{:S(2)}, u32[]{:S(2)}) collective-permute-start(bf16[2,128,128]{2,1,0:T(8,128)(2,1)S(1)} %get-tuple-element.59), channel_id=1, source_target_pairs={{0,4},{2,6},{4,0},{6,2},{8,12},{10,14},{12,8},{14,10},{16,20},{18,... | collective-permute-start | bytes 196616 | tf_op jit(solution)/shard_map/ppermute | solution.py:372
  50.5 5.2 %collective-permute-start.3 = (bf16[2,128,128]{2,1,0:T(8,128)(2,1)S(1)}, bf16[2,128,128]{2,1,0:T(8,128)(2,1)S(1)}, u32[]{:S(2)}, u32[]{:S(2)}) collective-permute-start(bf16[2,128,128]{2,1,0:T(8,128)(2,1)S(1)} %get-tuple-element.60), channel_id=1, source_target_pairs={{0,2},{2,0},{4,6},{6,4},{8,10},{10,8},{12,14},{14,12},{16,18},{18,... | collective-permute-start | bytes 196616 | tf_op jit(solution)/shard_map/ppermute | solution.py:372
  50.6 8.3 %collective-permute-start.2 = (bf16[2,2,128,128]{3,2,1,0:T(8,128)(2,1)S(1)}, bf16[2,2,128,128]{3,2,1,0:T(8,128)(2,1)S(1)}, u32[]{:S(2)}, u32[]{:S(2)}) collective-permute-start(bf16[2,2,128,128]{3,2,1,0:T(8,128)(2,1)S(1)} %get-tuple-element.48), channel_id=1, source_target_pairs={{0,6},{2,4},{4,2},{6,0},{8,14},{10,12},{12,10},{14,8},{16,22},{18,... | collective-permute-start | bytes 393224 | tf_op jit(solution)/shard_map/ppermute | solution.py:372
  53.6 6.3 %collective-permute-start.1 = (bf16[2,2,128,128]{3,2,1,0:T(8,128)(2,1)S(1)}, bf16[2,2,128,128]{3,2,1,0:T(8,128)(2,1)S(1)}, u32[]{:S(2)}, u32[]{:S(2)}) collective-permute-start(bf16[2,2,128,128]{3,2,1,0:T(8,128)(2,1)S(1)} %get-tuple-element.49), channel_id=1, source_target_pairs={{0,4},{2,6},{4,0},{6,2},{8,12},{10,14},{12,8},{14,10},{16,20},{18,... | collective-permute-start | bytes 393224 | tf_op jit(solution)/shard_map/ppermute | solution.py:372
  54.1 5.9 %collective-permute-start = (bf16[2,2,128,128]{3,2,1,0:T(8,128)(2,1)S(1)}, bf16[2,2,128,128]{3,2,1,0:T(8,128)(2,1)S(1)}, u32[]{:S(2)}, u32[]{:S(2)}) collective-permute-start(bf16[2,2,128,128]{3,2,1,0:T(8,128)(2,1)S(1)} %get-tuple-element.50), channel_id=1, source_target_pairs={{0,2},{2,0},{4,6},{6,4},{8,10},{10,8},{12,14},{14,12},{16,18},{18,... | collective-permute-start | bytes 393224 | tf_op jit(solution)/shard_map/ppermute | solution.py:372
  63.3 10.9 %collective-permute-start.6 = (bf16[2,2,128,128]{3,2,1,0:T(8,128)(2,1)}, bf16[2,2,128,128]{3,2,1,0:T(8,128)(2,1)S(1)}, u32[]{:S(2)}, u32[]{:S(2)}) collective-permute-start(bf16[2,2,128,128]{3,2,1,0:T(8,128)(2,1)} %total_forward.1.own_ref), channel_id=1, source_target_pairs={{0,8},{2,10},{4,12},{6,14},{8,16},{10,18},{12,20},{14,22},{16,24},... | collective-permute-start | bytes 393224 | tf_op jit(solution)/shard_map/ppermute | solution.py:375
  66.9 78.0 %collective-permute-start.19 = (bf16[256,512]{0,1:T(8,128)(2,1)S(1)}, bf16[256,512]{0,1:T(8,128)(2,1)S(1)}, u32[]{:S(2)}, u32[]{:S(2)}) collective-permute-start(bf16[256,512]{0,1:T(8,128)(2,1)S(1)} %bitcast.72), channel_id=1, source_target_pairs={{0,4},{2,6},{4,0},{6,2},{8,12},{10,14},{12,8},{14,10},{16,20},{18,... | collective-permute-start | bytes 786440 | tf_op jit(solution)/shard_map/ppermute | solution.py:372
  67.9 79.9 %collective-permute-start.17 = (bf16[256,512]{0,1:T(8,128)(2,1)S(1)}, bf16[256,512]{0,1:T(8,128)(2,1)}, u32[]{:S(2)}, u32[]{:S(2)}) collective-permute-start(bf16[256,512]{0,1:T(8,128)(2,1)S(1)} %bitcast.71), channel_id=1, source_target_pairs={{0,2},{2,0},{4,6},{6,4},{8,10},{10,8},{12,14},{14,12},{16,18},{18,... | collective-permute-start | bytes 786440 | tf_op jit(solution)/shard_map/ppermute | solution.py:372
  69.0 80.3 %collective-permute-start.21 = (bf16[256,512]{0,1:T(8,128)(2,1)S(1)}, bf16[256,512]{0,1:T(8,128)(2,1)S(1)}, u32[]{:S(2)}, u32[]{:S(2)}) collective-permute-start(bf16[256,512]{0,1:T(8,128)(2,1)S(1)} %bitcast.70), channel_id=1, source_target_pairs={{0,6},{2,4},{4,2},{6,0},{8,14},{10,12},{12,10},{14,8},{16,22},{18,... | collective-permute-start | bytes 786440 | tf_op jit(solution)/shard_map/ppermute | solution.py:372
  72.9 10.2 %collective-permute-start.11 = (bf16[2,2,128,128]{3,2,1,0:T(8,128)(2,1)}, bf16[2,2,128,128]{3,2,1,0:T(8,128)(2,1)S(1)}, u32[]{:S(2)}, u32[]{:S(2)}) collective-permute-start(bf16[2,2,128,128]{3,2,1,0:T(8,128)(2,1)} %total_back.1.own_ref), channel_id=1, source_target_pairs={{8,0},{10,2},{12,4},{14,6},{16,8},{18,10},{20,12},{22,14},{24,16},... | collective-permute-start | bytes 393224 | tf_op jit(solution)/shard_map/ppermute | solution.py:375
  77.5 10.3 %collective-permute-start.7 = (bf16[2,128,128]{2,1,0:T(8,128)(2,1)S(1)}, bf16[2,128,128]{2,1,0:T(8,128)(2,1)S(1)}, u32[]{:S(2)}, u32[]{:S(2)}) collective-permute-start(bf16[2,128,128]{2,1,0:T(8,128)(2,1)S(1)} %slice_bitcast_fusion.9), channel_id=1, source_target_pairs={{0,16},{2,18},{4,20},{6,22},{8,24},{10,26},{12,28},{14,30},{1,17},... | collective-permute-start | bytes 196616 | tf_op jit(solution)/shard_map/ppermute | solution.py:375
  86.4 7.6 %collective-permute-start.12 = (bf16[2,128,128]{2,1,0:T(8,128)(2,1)S(1)}, bf16[2,128,128]{2,1,0:T(8,128)(2,1)S(1)}, u32[]{:S(2)}, u32[]{:S(2)}) collective-permute-start(bf16[2,128,128]{2,1,0:T(8,128)(2,1)S(1)} %slice_bitcast_fusion.4), channel_id=1, source_target_pairs={{16,0},{18,2},{20,4},{22,6},{24,8},{26,10},{28,12},{30,14},{17,1},... | collective-permute-start | bytes 196616 | tf_op jit(solution)/shard_map/ppermute | solution.py:375
  93.0 24.9 %collective-permute-start.8 = (bf16[2,128,128]{2,1,0:T(8,128)(2,1)S(1)}, bf16[2,128,128]{2,1,0:T(8,128)(2,1)S(1)}, u32[]{:S(2)}, u32[]{:S(2)}) collective-permute-start(bf16[2,128,128]{2,1,0:T(8,128)(2,1)S(1)} %get-tuple-element.56), channel_id=1, source_target_pairs={{0,2},{2,0},{4,6},{6,4},{8,10},{10,8},{12,14},{14,12},{16,18},{18,... | collective-permute-start | bytes 196616 | tf_op jit(solution)/shard_map/ppermute | solution.py:372
  98.3 4.3 %collective-permute-start.13 = (bf16[2,128,128]{2,1,0:T(8,128)(2,1)S(1)}, bf16[2,128,128]{2,1,0:T(8,128)(2,1)S(1)}, u32[]{:S(2)}, u32[]{:S(2)}) collective-permute-start(bf16[2,128,128]{2,1,0:T(8,128)(2,1)S(1)} %get-tuple-element.53), channel_id=1, source_target_pairs={{0,2},{2,0},{4,6},{6,4},{8,10},{10,8},{12,14},{14,12},{16,18},{18,... | collective-permute-start | bytes 196616 | tf_op jit(solution)/shard_map/ppermute | solution.py:372
  102.6 4.3 %collective-permute-start.14 = (bf16[2,128,128]{2,1,0:T(8,128)(2,1)S(1)}, bf16[2,128,128]{2,1,0:T(8,128)(2,1)S(1)}, u32[]{:S(2)}, u32[]{:S(2)}) collective-permute-start(bf16[2,128,128]{2,1,0:T(8,128)(2,1)S(1)} %get-tuple-element.52), channel_id=1, source_target_pairs={{0,4},{2,6},{4,0},{6,2},{8,12},{10,14},{12,8},{14,10},{16,20},{18,... | collective-permute-start | bytes 196616 | tf_op jit(solution)/shard_map/ppermute | solution.py:372
  106.9 5.2 %collective-permute-start.15 = (bf16[2,128,128]{2,1,0:T(8,128)(2,1)S(1)}, bf16[2,128,128]{2,1,0:T(8,128)(2,1)S(1)}, u32[]{:S(2)}, u32[]{:S(2)}) collective-permute-start(bf16[2,128,128]{2,1,0:T(8,128)(2,1)S(1)} %get-tuple-element.51), channel_id=1, source_target_pairs={{0,6},{2,4},{4,2},{6,0},{8,14},{10,12},{12,10},{14,8},{16,22},{18,... | collective-permute-start | bytes 196616 | tf_op jit(solution)/shard_map/ppermute | solution.py:372
  112.1 7.3 %collective-permute-start.9 = (bf16[2,128,128]{2,1,0:T(8,128)(2,1)S(1)}, bf16[2,128,128]{2,1,0:T(8,128)(2,1)S(1)}, u32[]{:S(2)}, u32[]{:S(2)}) collective-permute-start(bf16[2,128,128]{2,1,0:T(8,128)(2,1)S(1)} %get-tuple-element.55), channel_id=1, source_target_pairs={{0,4},{2,6},{4,0},{6,2},{8,12},{10,14},{12,8},{14,10},{16,20},{18,... | collective-permute-start | bytes 196616 | tf_op jit(solution)/shard_map/ppermute | solution.py:372
  117.9 5.9 %collective-permute-start.10 = (bf16[2,128,128]{2,1,0:T(8,128)(2,1)S(1)}, bf16[2,128,128]{2,1,0:T(8,128)(2,1)S(1)}, u32[]{:S(2)}, u32[]{:S(2)}) collective-permute-start(bf16[2,128,128]{2,1,0:T(8,128)(2,1)S(1)} %get-tuple-element.54), channel_id=1, source_target_pairs={{0,6},{2,4},{4,2},{6,0},{8,14},{10,12},{12,10},{14,8},{16,22},{18,... | collective-permute-start | bytes 196616 | tf_op jit(solution)/shard_map/ppermute | solution.py:372
  119.5 27.0 %collective-permute-start.20 = (bf16[256,1024]{1,0:T(8,128)(2,1)}, bf16[256,1024]{1,0:T(8,128)(2,1)S(1)}, u32[]{:S(2)}, u32[]{:S(2)}) collective-permute-start(bf16[256,1024]{1,0:T(8,128)(2,1)} %values.1), channel_id=1, source_target_pairs={{0,4},{2,6},{4,0},{6,2},{8,12},{10,14},{12,8},{14,10},{16,20},{18,... | collective-permute-start | bytes 1572872 | tf_op jit(solution)/shard_map/ppermute | solution.py:372
  123.8 24.1 %collective-permute-start.18 = (bf16[256,1024]{1,0:T(8,128)(2,1)}, bf16[256,1024]{1,0:T(8,128)(2,1)S(1)}, u32[]{:S(2)}, u32[]{:S(2)}) collective-permute-start(bf16[256,1024]{1,0:T(8,128)(2,1)} %values.1), channel_id=1, source_target_pairs={{0,2},{2,0},{4,6},{6,4},{8,10},{10,8},{12,14},{14,12},{16,18},{18,... | collective-permute-start | bytes 1572872 | tf_op jit(solution)/shard_map/ppermute | solution.py:372
  124.9 0.7 copy-start.3
  125.7 15.1 %copy-start.1 = (bf16[256,1024]{1,0:T(8,128)(2,1)S(1)}, bf16[256,1024]{1,0:T(8,128)(2,1)}, u32[]{:S(2)}) copy-start(bf16[256,1024]{1,0:T(8,128)(2,1)} %values.1) | copy-start | bytes 1572868
  145.0 1.5 copy-start.8
  145.0 10.1 %collective-permute-start.22 = (bf16[256,1024]{1,0:T(8,128)(2,1)S(1)}, bf16[256,1024]{1,0:T(8,128)(2,1)S(1)}, u32[]{:S(2)}, u32[]{:S(2)}) collective-permute-start(bf16[256,1024]{1,0:T(8,128)(2,1)S(1)} %copy-done.1), channel_id=1, source_target_pairs={{0,6},{2,4},{4,2},{6,0},{8,14},{10,12},{12,10},{14,8},{16,22},{18,... | collective-permute-start | bytes 1572872 | tf_op jit(solution)/shard_map/ppermute | solution.py:372
  146.5 14.8 %collective-permute-start.16 = (bf16[128,2048]{1,0:T(8,128)(2,1)S(1)}, bf16[128,2048]{1,0:T(8,128)(2,1)S(1)}, u32[]{:S(2)}, u32[]{:S(2)}) collective-permute-start(bf16[128,2048]{1,0:T(8,128)(2,1)S(1)} %convolution_convert_fusion), channel_id=1, source_target_pairs={{0,1},{1,0},{2,3},{3,2},{4,5},{5,4},{6,7},{7,6},{8,9},{9,8},{10,11... | collective-permute-start | bytes 1572872 | tf_op jit(solution)/shard_map/ppermute | solution.py:517
  155.1 6.1 %copy-start = (bf16[2048,1024]{1,0:T(8,128)(2,1)S(1)}, bf16[2048,1024]{1,0:T(8,128)(2,1)}, u32[]{:S(2)}) copy-start(bf16[2048,1024]{1,0:T(8,128)(2,1)} %param.11) | copy-start | bytes 12582916
  155.7 10.7 %collective-permute-start.25 = (bf16[128,1024]{1,0:T(8,128)(2,1)S(1)}, bf16[128,1024]{1,0:T(8,128)(2,1)S(1)}, u32[]{:S(2)}, u32[]{:S(2)}) collective-permute-start(bf16[128,1024]{1,0:T(8,128)(2,1)S(1)} %get-tuple-element.41), channel_id=1, source_target_pairs={{0,24},{2,26},{4,28},{6,30},{8,0},{10,2},{12,4},{14,6},{16,8},{18,... | collective-permute-start | bytes 786440 | tf_op jit(solution)/shard_map/ppermute | solution.py:478
  160.2 17.6 %collective-permute-start.24 = (bf16[128,1024]{1,0:T(8,128)(2,1)S(1)}, bf16[128,1024]{1,0:T(8,128)(2,1)S(1)}, u32[]{:S(2)}, u32[]{:S(2)}) collective-permute-start(bf16[128,1024]{1,0:T(8,128)(2,1)S(1)} %get-tuple-element.42), channel_id=1, source_target_pairs={{0,16},{2,18},{4,20},{6,22},{8,24},{10,26},{12,28},{14,30},{16,0},... | collective-permute-start | bytes 786440 | tf_op jit(solution)/shard_map/ppermute | solution.py:478
  160.2 17.6 %collective-permute-start.23 = (bf16[128,1024]{1,0:T(8,128)(2,1)S(1)}, bf16[128,1024]{1,0:T(8,128)(2,1)S(1)}, u32[]{:S(2)}, u32[]{:S(2)}) collective-permute-start(bf16[128,1024]{1,0:T(8,128)(2,1)S(1)} %get-tuple-element.40), channel_id=1, source_target_pairs={{0,8},{2,10},{4,12},{6,14},{8,16},{10,18},{12,20},{14,22},{16,24},... | collective-permute-start | bytes 786440 | tf_op jit(solution)/shard_map/ppermute | solution.py:478
  (5 other events, 3.3 us)

commit v2 on v0

v2 whole, which is shorter than its diff:
```python
import functools

import jax
import jax.numpy as jnp
from jax import lax
from jax.experimental import pallas as pl
from jax.experimental.pallas import tpu as pltpu
from jax.sharding import PartitionSpec as P

NORM_FLOOR = 16.0
F32 = jnp.float32
BF16 = jnp.bfloat16
HIGHEST = lax.Precision.HIGHEST
VMEM_LIMIT = 56 * 1024 * 1024
PACK = 4
CHUNKS = 2


def dot(a, b, ca=1, cb=0, precision=None):
    return lax.dot_general(
        a, b, (((ca,), (cb,)), ((), ())), precision=precision, preferred_element_type=F32
    )


def low(x):
    return x.astype(BF16)


def iotas(n):
    rows = lax.broadcasted_iota(jnp.int32, (n, n), 0)
    cols = lax.broadcasted_iota(jnp.int32, (n, n), 1)
    return rows, cols


def columns(rows):
    count, n = rows.shape
    return jnp.transpose(jnp.concatenate([rows, jnp.zeros((128 - count, n), F32)], axis=0))


def rate_column(rate_ref):
    count = rate_ref.shape[0]
    row = lax.broadcasted_iota(jnp.int32, (count, 1), 0)
    out = jnp.zeros((count, 1), F32)
    for h in range(count):
        out = jnp.where(row == h, rate_ref[h], out)
    return out


def sigmoid(x):
    return 1.0 / (1.0 + jnp.exp(-x))


def head_columns(beta_ref, decay_ref, rate_ref, g_ref, b_ref, gt_ref):
    decay = decay_ref[...]
    n = decay.shape[1]
    rows, cols = iotas(n)
    log_decay = -rate_column(rate_ref) * (
        jnp.maximum(decay, 0.0) + jnp.log1p(jnp.exp(-jnp.abs(decay)))
    )
    sums = dot(log_decay, (rows <= cols).astype(F32), precision=HIGHEST)
    gt_ref[...] = sums
    g_ref[...] = columns(sums)
    b_ref[...] = columns(sigmoid(beta_ref[...]))


def lane_column(ref, head):
    full = ref[...]
    width = full.shape[1]
    rolled = pltpu.roll(full, lax.rem(width - head, width), 1)
    return jnp.broadcast_to(rolled[:, 0:1], full.shape)


class Head:
    pass


def lanes_of(head, size):
    return pl.ds(pl.multiple_of(head * size, size), size)


def head_common(q_ref, k_ref, head, size, g_ref, b_ref, gt_ref):
    h = Head()
    n = q_ref.shape[0]
    h.head, h.n, h.size = head, n, size
    h.lanes = lanes_of(head, size)
    h.k16, h.q16 = k_ref[:, h.lanes], q_ref[:, h.lanes]
    k32, q32 = h.k16.astype(F32), h.q16.astype(F32)
    h.g = lane_column(g_ref, head)
    h.beta = lane_column(b_ref, head)
    norm = lambda x: jnp.broadcast_to(
        lax.rsqrt(jnp.sum(x * x, axis=1, keepdims=True) + NORM_FLOOR), (n, size)
    )
    h.rk, h.rq = norm(k32), norm(q32)
    g_row = gt_ref[pl.ds(head, 1), :]
    rk_row = jnp.transpose(h.rk)[0:1, :]
    rows, cols = iotas(n)
    h.tile = lambda x: jnp.concatenate([x] * (n // size), axis=1)
    spread = jnp.where(rows >= cols, h.tile(h.g) - g_row, -1e30)
    h.gamma_rk = jnp.exp(spread) * rk_row
    gram = dot(jnp.concatenate([h.k16, h.q16], axis=0), h.k16, 1, 1)
    h.scale = size**-0.5
    h.a0 = jnp.where(rows > cols, gram[:n] * h.gamma_rk * h.tile(h.rk), 0.0)
    h.p = gram[n:] * h.gamma_rk * h.tile(h.rq * h.scale)
    g_end = h.g[n - 1 : n, :]
    h.k_hat, h.q_hat = k32 * h.rk, q32 * (h.rq * h.scale)
    h.gain, h.tail, h.gain_end = jnp.exp(h.g), jnp.exp(g_end - h.g), jnp.exp(g_end)
    return h


def unit_lower_inverses(mats):
    n = mats[0].shape[0]
    rows, cols = iotas(n)
    differ = rows ^ cols
    eye = (rows == cols).astype(F32)
    high = [low(a) for a in mats]
    xs = [low(eye) - a * low((differ == 1).astype(F32)) for a in high]
    size = 2
    while 2 * size < n:
        mask = low(((differ >= size) & (differ < 2 * size)).astype(F32))
        ys = [low(dot(a * mask, x)) for a, x in zip(high, xs)]
        xs = [x - low(dot(x, y)) for x, y in zip(xs, ys)]
        size *= 2
    ys = [low(dot(a[size:, :size], x[:size, :size])) for a, x in zip(high, xs)]
    zs = [low(-dot(x[size:, size:], y)) for x, y in zip(xs, ys)]
    xs = [
        jnp.concatenate([x[:size], jnp.concatenate([z, x[size:, size:]], axis=1)], axis=0)
        for x, z in zip(xs, zs)
    ]
    rest = [low(a - h.astype(F32)) for a, h in zip(mats, high)]
    products = [
        dot(jnp.concatenate([h, l], axis=1), jnp.concatenate([x, x], axis=0))
        for h, l, x in zip(high, rest, xs)
    ]
    return [
        low(x.astype(F32) + dot(x, low(eye - x.astype(F32) - y))) for x, y in zip(xs, products)
    ]


def local_kernel(pack, share, pos_ref, q_ref, k_ref, do_ref, bp_ref, dp_ref, rate_ref, *refs):
    group = q_ref.shape[1] // refs[0].shape[-1] // share
    tg_refs, (inv_ref, dr_ref, y_ref, g_ref, b_ref, gt_ref) = refs[:group], refs[group:]
    pos = pos_ref[0]
    head_columns(bp_ref, dp_ref, rate_ref, g_ref, b_ref, gt_ref)
    size = tg_refs[0].shape[-1]
    for start in range(0, group * share, pack):
        places = range(start, start + pack)
        heads = [
            head_common(q_ref, k_ref, ((p // share) ^ pos) * share + p % share, size, g_ref, b_ref, gt_ref)
            for p in places
        ]
        invs = unit_lower_inverses([h.a0 * h.tile(h.beta) for h in heads])
        outs = [do_ref[:, h.lanes] for h in heads]
        d_written = [low(dot(low(h.p), do16, 0, 0)) for h, do16 in zip(heads, outs)]
        tails = [low(h.k_hat * h.tail) for h in heads]
        both = [
            low(dot(inv, jnp.concatenate([d, t], axis=1), 0, 0))
            for inv, d, t in zip(invs, d_written, tails)
        ]
        eye = lax.broadcasted_iota(jnp.int32, (size, size), 0) == lax.broadcasted_iota(
            jnp.int32, (size, size), 1
        )
        for p, h, inv, do16, b16 in zip(places, heads, invs, outs, both):
            dr16, y16 = b16[:, :size], b16[:, size:]
            inv_ref[p] = inv
            dr_ref[:, h.lanes] = dr16
            y_ref[:, h.lanes] = y16
            k_in = low(h.k_hat * h.beta * h.gain)
            out = tg_refs[p // share]
            out[0, p % share] = low(jnp.where(eye, h.gain_end, 0.0) - dot(y16, k_in, 0, 0))
            own = dot(
                jnp.concatenate([low(h.q_hat * h.gain), -k_in], axis=0),
                jnp.concatenate([do16, dr16], axis=0), 0, 0,
            )
            out[1, p % share] = low(own)


def offset_kernel(share, pos_ref, y_ref, v_ref, bp_ref, *refs):
    o_refs, b_ref = refs[:-1], refs[-1]
    pos = pos_ref[0]
    b_ref[...] = columns(sigmoid(bp_ref[...]))
    size = o_refs[0].shape[-1]
    for p in range(len(o_refs) * share):
        head = ((p // share) ^ pos) * share + p % share
        lanes = lanes_of(head, size)
        beta = lane_column(b_ref, head)
        o_refs[p // share][p % share] = low(
            dot(y_ref[:, lanes], low(v_ref[:, lanes].astype(F32) * beta), 0, 0)
        )


def values_kernel(share, pos_ref, dr_ref, y_ref, bp_ref, *refs):
    e_refs, (dv_ref, b_ref) = refs[:-2], refs[-2:]
    pos = pos_ref[0]
    b_ref[...] = columns(sigmoid(bp_ref[...]))
    size = e_refs[0].shape[-1]
    for p in range(len(e_refs) * share):
        head = ((p // share) ^ pos) * share + p % share
        lanes = lanes_of(head, size)
        beta = lane_column(b_ref, head)
        dr = dr_ref[:, lanes].astype(F32) + dot(y_ref[:, lanes], e_refs[p // share][p % share])
        dv_ref[:, lanes] = low(dr * beta)


def grads_kernel(pack, share, pos_ref, q_ref, k_ref, v_ref, do_ref, bp_ref, dp_ref, rate_ref, inv_ref, dr_ref, y_ref, *refs):
    size = refs[0].shape[-1]
    group = q_ref.shape[1] // size // share
    s_refs, e_refs = refs[:group], refs[group : 2 * group]
    dq_ref, dk_ref, db_ref, dd_ref, g_ref, b_ref, gt_ref, row_acc, col_acc, db_acc = refs[2 * group :]
    pos = pos_ref[0]
    head_columns(bp_ref, dp_ref, rate_ref, g_ref, b_ref, gt_ref)
    count = group * share
    n = q_ref.shape[0]
    rows, cols = iotas(n)
    lane = lax.broadcasted_iota(jnp.int32, (n, size), 1)
    row_acc[...] = jnp.zeros_like(row_acc)
    db_acc[...] = jnp.zeros_like(db_acc)
    for start in range(0, count, pack):
        places = range(start, start + pack)
        heads = [
            head_common(q_ref, k_ref, ((p // share) ^ pos) * share + p % share, size, g_ref, b_ref, gt_ref)
            for p in places
        ]
        for p, h in zip(places, heads):
            h.s16, h.e16 = s_refs[p // share][p % share], e_refs[p // share][p % share]
            h.do16 = do_ref[:, h.lanes]
            inner = v_ref[:, h.lanes].astype(F32) - h.gain * (h.rk * dot(h.k16, h.s16))
            h.right = low(h.beta * inner)
            h.dr = dr_ref[:, h.lanes].astype(F32) + dot(y_ref[:, h.lanes], h.e16)
            h.dr16 = low(h.dr)
        for p, h in zip(places, heads):
            h.written = dot(inv_ref[p], h.right)
            h.w16 = low(h.written)
            at_s = dot(jnp.concatenate([h.do16, h.dr16], axis=0), h.s16, 1, 1)
            h.d_qd, h.dr_s = at_s[:n], at_s[n:]
        for h in heads:
            pair = dot(jnp.concatenate([-h.dr16, h.do16], axis=0), h.w16, 1, 1)
            d_a, d_p = pair[:n], pair[n:]
            h.weights = d_a * h.a0 * h.tile(h.beta) + d_p * h.p
            x1 = low(jnp.where(rows > cols, d_a * h.gamma_rk, 0.0))
            x2 = low(d_p * h.gamma_rk)
            h.xs = jnp.concatenate([x1, x2], axis=0)
            h.d_kt = dot(h.w16, h.e16, 1, 1)
        for h in heads:
            row_side = dot(h.xs, h.k16)
            col_side = dot(
                h.xs, jnp.concatenate([low(h.beta * h.k_hat), low(h.q_hat)], axis=0), 0, 0
            )
            d_q = row_side[n:] + h.gain * h.d_qd
            in_term = h.beta * h.gain * h.dr_s
            d_k = h.rk * (h.beta * row_side[:n] - in_term + h.tail * h.d_kt) + col_side
            unit = h.q16.astype(F32) * h.rq
            d_q = h.rq * h.scale * (d_q - unit * jnp.sum(unit * d_q, axis=1, keepdims=True))
            d_k = d_k - h.k_hat * jnp.sum(h.k_hat * d_k, axis=1, keepdims=True)
            dq_ref[:, h.lanes] = low(d_q)
            dk_ref[:, h.lanes] = low(d_k)
            tail_term = h.d_kt * h.k_hat * h.tail
            direct = h.gain * h.d_qd * h.q_hat - in_term * h.k_hat - tail_term
            folded = sum(h.weights[:, i * size : (i + 1) * size] for i in range(n // size))
            row_sum = jnp.sum(folded + direct, axis=1, keepdims=True)
            end = jnp.sum(
                jnp.sum(tail_term, axis=0, keepdims=True)
                + jnp.sum(h.gain_end * (h.s16.astype(F32) * h.e16.astype(F32)), axis=0, keepdims=True),
                axis=1, keepdims=True,
            )
            last = lax.broadcasted_iota(jnp.int32, (1, n), 1) == n - 1
            col_acc[pl.ds(h.head, 1), :] = jnp.where(last, end, 0.0) - jnp.sum(
                h.weights, axis=0, keepdims=True
            )
            row_acc[...] = jnp.where(lane == h.head, row_sum, row_acc[...])
            d_beta = (1.0 - h.beta) * jnp.sum(h.dr * h.written, axis=1, keepdims=True)
            db_acc[...] = jnp.where(lane == h.head, d_beta, db_acc[...])
    d_sums = jnp.transpose(row_acc[...])[0:count] + col_acc[...]
    d_log = dot(d_sums, (rows >= cols).astype(F32), precision=HIGHEST)
    dd_ref[...] = -rate_column(rate_ref) * sigmoid(dp_ref[...]) * d_log
    db_ref[...] = jnp.transpose(db_acc[...])[0:count]


def call(body, name, args, outs, scratch=(), flops=0):
    place = lambda a: pl.BlockSpec(memory_space=pltpu.SMEM if a.ndim == 1 else pltpu.VMEM)
    return pl.pallas_call(
        body,
        in_specs=[place(a) for a in args],
        out_specs=[pl.BlockSpec(memory_space=pltpu.VMEM) for _ in outs],
        out_shape=outs,
        scratch_shapes=list(scratch),
        compiler_params=pltpu.CompilerParams(vmem_limit_bytes=VMEM_LIMIT),
        cost_estimate=pl.CostEstimate(flops=flops, bytes_accessed=1 << 20, transcendentals=0),
        name=name,
    )(*args)


def shape(*dims, dtype=BF16):
    return jax.ShapeDtypeStruct(dims, dtype)


def total_kernel(group, backward, pos_ref, *refs):
    count = len(refs) - 2
    tg_refs, o_refs, (total_ref, store) = refs[:group], refs[group:count], refs[count:]
    pos = pos_ref[0]
    share = total_ref.shape[1]
    for d in range(group):
        store[d, 0] = tg_refs[d][0]
        store[d, 1] = tg_refs[d][1] if backward else o_refs[d][...]
    order = list(range(group))
    if backward:
        order.reverse()
    for i in range(share):
        first = pos ^ order[0]
        t, o = store[first, 0, i], store[first, 1, i]
        for j in order[1:]:
            slot = pos ^ j
            tj, oj = store[slot, 0, i], store[slot, 1, i].astype(F32)
            if backward:
                o, t = low(oj + dot(tj, o, 0, 0)), low(dot(t, tj))
            else:
                o, t = low(oj + dot(tj, o)), low(dot(tj, t))
        total_ref[0, i] = t
        total_ref[1, i] = o


def spread_kernel(group, outer, backward, pos_ref, *refs):
    reach = outer - 1
    tg_refs, refs = refs[:group], refs[group:]
    o_refs, refs = (None, refs) if backward else (refs[:group], refs[group:])
    far_refs, out_refs, store, result = refs[:reach], refs[reach : reach + group], refs[-2], refs[-1]
    pos = pos_ref[0]
    share = out_refs[0].shape[0]
    for d in range(group):
        store[d, 0] = tg_refs[d][0]
        store[d, 1] = tg_refs[d][1] if backward else o_refs[d][...]
    turn = (lambda t, x: dot(t, x, 0, 0)) if backward else (lambda t, x: dot(t, x))
    state = [jnp.zeros(store.shape[3:], BF16)] * share
    for far in reversed(far_refs):
        if far is far_refs[-1]:
            state = [far[far.shape[0] - 1, i] for i in range(share)]
        else:
            state = [low(far[1, i].astype(F32) + turn(far[0, i], x)) for i, x in enumerate(state)]
    order = list(range(group))
    if backward:
        order.reverse()
    for j in order:
        slot = pos ^ j
        for i in range(share):
            result[slot, i] = state[i]
        if j != order[-1]:
            state = [
                low(store[slot, 1, i].astype(F32) + turn(store[slot, 0, i], x))
                for i, x in enumerate(state)
            ]
    for d in range(group):
        out_refs[d][...] = result[d]


def group_size(count, heads):
    size = 1
    while size * size < count and count % (2 * size) == 0 and heads % (2 * size) == 0:
        size *= 2
    return size


def per_device(queries, keys, hidden, value_weight, beta_pre, decay_pre, decay_rate, out_grad):
    heads = decay_rate.shape[0]
    n, width = queries.shape
    dk = width // heads
    dv = value_weight.shape[1] // heads
    model = hidden.shape[1]
    spans = lax.axis_size("sp")
    group = group_size(spans, heads)
    outer = spans // group
    place = lax.axis_index("sp")
    pos = lax.rem(place, group)
    lead = lax.div(place, group)
    pos_arr = jnp.full((1,), pos, jnp.int32)
    share = heads // group
    beta_t, decay_t = beta_pre.T, decay_pre.T
    big = heads * n * n * 256

    def near(x, d):
        return lax.ppermute(x, "sp", [(s, s ^ d) for s in range(spans)]) if d else x

    def along(x, d):
        return lax.ppermute(
            x, "sp", [(s, s + d * group) for s in range(spans) if 0 <= s + d * group < spans]
        )

    def tied(x, after):
        return lax.optimization_barrier((x, after))[0]

    rows = model // spans
    by_owner = hidden.reshape(n, outer, group, rows)

    def hidden_part(d):
        return lax.dynamic_index_in_dim(by_owner, pos ^ d, 2, False).reshape(n, outer * rows)

    hidden_parts = [near(hidden_part(d), d) for d in range(group)]

    col_scratch = [
        pltpu.VMEM((n, 128), F32), pltpu.VMEM((n, 128), F32), pltpu.VMEM((heads, n), F32)
    ]
    *tg, inv, dr, y = call(
        functools.partial(local_kernel, PACK, share),
        "local",
        [pos_arr, queries, keys, out_grad, beta_t, decay_t, decay_rate],
        [shape(2, share, dk, dv)] * group + [shape(heads, n, n), shape(n, width), shape(n, width)],
        col_scratch,
        big,
    )
    small = group * share * dk * dk * dk * 4
    store = pltpu.VMEM((group, 2, share, dk, dv), BF16)
    result = pltpu.VMEM((group, share, dk, dv), BF16)

    def states(backward, maps, offsets):
        name = "back" if backward else "forward"
        (total,) = call(
            functools.partial(total_kernel, group, backward), "total_" + name,
            [pos_arr, *maps, *offsets], [shape(2, share, dk, dv)], [store], small,
        )
        sign = -1 if backward else 1
        far = [
            along(total if d < outer - 1 else total[1:], sign * d) for d in range(1, outer)
        ]
        spread = call(
            functools.partial(spread_kernel, group, outer, backward), "spread_" + name,
            [pos_arr, *maps, *offsets, *far], [shape(share, dk, dv)] * group, [store, result], small,
        )
        return [near(x, d) for d, x in enumerate(spread)], total, far

    tg = [near(x, d) for d, x in enumerate(tg)]
    end_grad, back_total, back_far = states(True, tg, [])

    (d_values,) = call(
        functools.partial(values_kernel, share),
        "values",
        [pos_arr, dr, y, beta_t, *end_grad],
        [shape(n, width)],
        [pltpu.VMEM((n, 128), F32)],
        heads * n * dk * dv * 2,
    )
    chunk = width // CHUNKS
    pieces = []
    for c in range(CHUNKS):
        own = lax.slice_in_dim(d_values, c * chunk, (c + 1) * chunk, axis=1)
        partial = sum(
            lax.dot_general(a, near(own, d), (((0,), (0,)), ((), ())), preferred_element_type=F32)
            for d, a in enumerate(hidden_parts)
        ).reshape(outer, rows, chunk)
        total = lax.dynamic_index_in_dim(partial, lead, 0, False)
        for e in range(1, outer):
            piece = lax.dynamic_index_in_dim(partial, lax.rem(lead + e, outer), 0, False)
            moved = lax.ppermute(
                piece.astype(BF16), "sp", [(s, (s + e * group) % spans) for s in range(spans)]
            )
            total = total + moved.astype(F32)
        pieces.append(total)
    d_weight = jnp.concatenate(pieces, axis=1)

    values = jnp.dot(hidden, value_weight, preferred_element_type=F32).astype(BF16)
    offset = call(
        functools.partial(offset_kernel, share),
        "offset",
        [pos_arr, y, values, beta_t],
        [shape(share, dk, dv)] * group,
        [pltpu.VMEM((n, 128), F32)],
        heads * n * dk * dv * 2,
    )
    offset = tied(offset, back_total)
    offset = [near(x, d) for d, x in enumerate(offset)]
    start_state, _, _ = states(False, tg, offset)

    core = lax.axis_index("tp")
    cores = lax.axis_size("tp")
    own_rows = n // cores

    def input_grad(which):
        piece = lax.dynamic_slice_in_dim(d_values, which * own_rows, own_rows, 0)
        return lax.dot_general(
            piece, value_weight, (((1,), (1,)), ((), ())), preferred_element_type=F32
        )

    d_hidden = input_grad(core)
    for d in range(1, cores):
        moved = lax.ppermute(
            input_grad(lax.rem(core + d, cores)).astype(BF16),
            "tp",
            [(c, (c + d) % cores) for c in range(cores)],
        )
        d_hidden = d_hidden + moved.astype(F32)
    d_hidden = d_hidden.astype(BF16)

    d_queries, d_keys, d_beta, d_decay = call(
        functools.partial(grads_kernel, PACK, share),
        "grads",
        [pos_arr, queries, keys, values, out_grad, beta_t, decay_t, decay_rate, inv, dr, y, *start_state, *end_grad],
        [shape(n, width), shape(n, width), shape(heads, n, dtype=F32), shape(heads, n, dtype=F32)],
        col_scratch + [pltpu.VMEM((n, dk), F32), pltpu.VMEM((heads, n), F32), pltpu.VMEM((n, dk), F32)],
        big,
    )
    return (d_queries, d_keys, d_beta.T, d_decay.T, d_hidden, d_weight)


def solution(mesh):
    return jax.shard_map(
        per_device,
        mesh=mesh,
        in_specs=(
            P("sp", "tp"),
            P("sp", "tp"),
            P("sp", None),
            P(None, "tp"),
            P("sp", "tp"),
            P("sp", "tp"),
            P("tp"),
            P("sp", "tp"),
        ),
        out_specs=(
            P("sp", "tp"),
            P("sp", "tp"),
            P("sp", "tp"),
            P("sp", "tp"),
            P(("sp", "tp"), None),
            P("sp", "tp"),
        ),
        check_vma=False,
    )
```

time: 835 us -> 132 us (0.16); the launches traced: 824 us -> 131 us
  waiting for transfers between devices: 335 us -> 23.6 us
  matrix products: 236 us -> 13.1 us
  other arithmetic: 181 us -> 0.95 us
  local copies, waits for them, and re-layouts: 53.3 us -> 7.55 us
  starting transfers between devices: 0.92 us -> 44.3 us
  Pallas kernels: 0 us -> 40.6 us
  between operations: 15.5 us -> 1.08 us
    dot_general x99 -> x11, matrix products: 223 us -> 13.1 us  [the longest x2 6.08 us: input_grad(): lax.dot_general(piece, value_weight, (((1,), (1,)), ((), ())), preferred_...]
    all_gather x4 -> x0, waiting for transfers between devices: 203 us -> none  [prefix(): lax.all_gather(a.astype(kind), axis)]
    another operation x6 -> x0, other arithmetic: 162 us -> none  [the longest x4 158 us: span_pieces(): jax.scipy.linalg.solve_triangular(system, right_side, lower=True, unit_di...]
    reduce_scatter x2 -> x0, waiting for transfers between devices: 131 us -> none  [the longest x1 120 us: per_device(): lax.psum_scatter(weight_term(hidden, [local_grad, carried_grad]), 'sp', s...]
    ppermute x0 -> x34, starting transfers between devices: none -> 44.3 us  [the longest x21 25.6 us: near(): return lax.ppermute(x, 'sp', [(s, s ^ d) for s in range(spans)]) if d else x]
    pallas_call x0 -> x8, Pallas kernels: none -> 40.6 us  [call(): pl.pallas_call(body, in_specs=[place(a) for a in args], out_specs=[pl.Blo...]
    ppermute x0 -> x34, waiting for transfers between devices: none -> 23.6 us  [the longest x6 14.6 us: per_device(): lax.ppermute(piece.astype(BF16), 'sp', [(s, (s + e * group) % spans) for...]
    another operation x5 -> x0, matrix products: 13.1 us -> none  [the longest x3 7.27 us: span_pieces(): jax.scipy.linalg.solve_triangular(system, right_side, lower=True, unit_di...]
  transfers between devices with their start and end apart: 6 -> 34, of which waited for: 5 -> 9; matrix products, arithmetic and copies ran while one was open for 19% -> 12% of each run, Pallas kernels for 0% -> 19%
where the time goes in v2:
time: 132 us; the launch traced here: 131 us
  starting transfers between devices  44.3 us (34%)
  Pallas kernels  40.6 us (31%)
  waiting for transfers between devices  23.6 us (18%)
  matrix products  13.1 us (10%)
  local copies, waits for them, and re-layouts  7.55 us (6%)
    pallas_call x8, Pallas kernels, call(): pl.pallas_call(body, in_specs=[place(a) for a in args], out_specs=[pl.Blo...  40.6 us
    ppermute x21, starting transfers between devices, near(): return lax.ppermute(x, 'sp', [(s, s ^ d) for s in range(spans)]) if d else x  25.6 us
    ppermute x6, starting transfers between devices, along(): lax.ppermute(x, 'sp', [(s, s + d * group) for s in range(spans) if 0 <= s...  15.2 us
    ppermute x6, waiting for transfers between devices, per_device(): lax.ppermute(piece.astype(BF16), 'sp', [(s, (s + e * group) % spans) for...  14.6 us
    ppermute x21, waiting for transfers between devices, near(): return lax.ppermute(x, 'sp', [(s, s ^ d) for s in range(spans)]) if d else x  8.97 us
    dot_general x2, matrix products, input_grad(): lax.dot_general(piece, value_weight, (((1,), (1,)), ((), ())), preferred_...  6.08 us
    dot_general x1, matrix products, per_device(): jnp.dot(hidden, value_weight, preferred_element_type=F32).astype(BF16)  4.63 us
    unnamed x43, local copies, waits for them, and re-layouts  4.6 us
  transfers between devices with their start and end apart: 34, of which 9 were waited for; matrix products, arithmetic and copies ran while one was open for 12% of the time, Pallas kernels for 19%

profile of v2, /device:TPU:0, one launch (start us, length us, event | category | flops | bytes accessed | tf_op | source)
XLA Modules:
  0.0 131.1 jit_solution(652641425421406451)
XLA Ops:
  0.6 13.8 %local.1 = (bf16[2,2,128,128]{3,2,1,0:T(8,128)(2,1)}, bf16[2,2,128,128]{3,2,1,0:T(8,128)(2,1)}, bf16[2,2,128,128]{3,2,1,0:T(8,128)(2,1)}, bf16[2,2,128,128]{3,2,...) custom-call(s32[1]{0:T(128)} %bitcast.pos_ref, ...), custom_call_target="tpu_custom_call" | custom-call | flops 134217728 | bytes 1048576 | tf_op jit(solution)/shard_map/local/pallas_call | solution.py:280
  14.4 3.0 %collective-permute-start = (bf16[2,2,128,128]{3,2,1,0:T(8,128)(2,1)}, bf16[2,2,128,128]{3,2,1,0:T(8,128)(2,1)S(1)}, u32[]{:S(2)}, u32[]{:S(2)}) collective-permute-start(bf16[2,2,128,128]{3,2,1,0:T(8,128)(2,1)} %get-tuple-element.37), channel_id=1, source_target_pairs={{0,2},{2,0},{4,6},{6,4},{8,10},{10,8},{12,14},{14,12},{16,18},{18,... | collective-permute-start | bytes 393224 | tf_op jit(solution)/shard_map/ppermute | solution.py:379
  17.4 1.5 %collective-permute-start.1 = (bf16[2,2,128,128]{3,2,1,0:T(8,128)(2,1)}, bf16[2,2,128,128]{3,2,1,0:T(8,128)(2,1)S(1)}, u32[]{:S(2)}, u32[]{:S(2)}) collective-permute-start(bf16[2,2,128,128]{3,2,1,0:T(8,128)(2,1)} %get-tuple-element.38), channel_id=1, source_target_pairs={{0,4},{2,6},{4,0},{6,2},{8,12},{10,14},{12,8},{14,10},{16,20},{18,... | collective-permute-start | bytes 393224 | tf_op jit(solution)/shard_map/ppermute | solution.py:379
  18.9 4.6 %convolution_convert_fusion.1.v_ref = bf16[256,1024]{1,0:T(8,128)(2,1)} fusion(bf16[256,2048]{1,0:T(8,128)(2,1)} %param.10, bf16[2048,1024]{1,0:T(8,128)(2,1)} %param.11), kind=kOutput, calls=%fused_computation.9 | convolution fusion | flops 1074003968 | bytes 5767168 | tf_op jit(solution)/shard_map/dot_general | solution.py:457
  23.5 3.1 %offset.1 = (bf16[2,128,128]{2,1,0:T(8,128)(2,1)}, bf16[2,128,128]{2,1,0:T(8,128)(2,1)}, bf16[2,128,128]{2,1,0:T(8,128)(2,1)}, bf16[2,128,128]{2,1,0:T(8,128)(2,1)}) custom-call(s32[1]{0:T(128)} %bitcast.pos_ref, bf16[256,1024]{1,0:T(8,128)(2,1)} %get-tuple-element.35.y_ref, bf16[256,1024]{1,0:T(8,128)(2,1)} %convolution_convert_fusion.1.v_ref, ...), custom_call_target="tpu_custom_call" | custom-call | flops 67108864 | bytes 1048576 | tf_op jit(solution)/shard_map/offset/pallas_call | solution.py:280
  27.6 2.5 %total_back.1 = bf16[2,2,128,128]{3,2,1,0:T(8,128)(2,1)} custom-call(s32[1]{0:T(128)} %bitcast.pos_ref, bf16[2,2,128,128]{3,2,1,0:T(8,128)(2,1)} %get-tuple-element.36.refs_0_, bf16[2,2,128,128]{3,2,1,0:T(8,128)(2,1)} %copy-done.2, bf16[2,2,128,128]{3,2,1,0:T(8,128)(2,1)} %copy-done.3, bf16[2,2,128,128]{3,2,1,0:T(8,128)(2,1)} %copy-done.4), custom_call_target="tpu_custom_call" | custom-call | flops 67108864 | bytes 1048576 | tf_op jit(solution)/shard_map/total_back/pallas_call | solution.py:280
  30.1 1.9 %collective-permute-start.3 = (bf16[2,128,128]{2,1,0:T(8,128)(2,1)}, bf16[2,128,128]{2,1,0:T(8,128)(2,1)S(1)}, u32[]{:S(2)}, u32[]{:S(2)}) collective-permute-start(bf16[2,128,128]{2,1,0:T(8,128)(2,1)} %get-tuple-element.45), channel_id=1, source_target_pairs={{0,2},{2,0},{4,6},{6,4},{8,10},{10,8},{12,14},{14,12},{16,18},{18,... | collective-permute-start | bytes 196616 | tf_op jit(solution)/shard_map/ppermute | solution.py:379
  34.6 1.6 %collective-permute-start.4 = (bf16[2,128,128]{2,1,0:T(8,128)(2,1)}, bf16[2,128,128]{2,1,0:T(8,128)(2,1)S(1)}, u32[]{:S(2)}, u32[]{:S(2)}) collective-permute-start(bf16[2,128,128]{2,1,0:T(8,128)(2,1)} %get-tuple-element.46), channel_id=1, source_target_pairs={{0,4},{2,6},{4,0},{6,2},{8,12},{10,14},{12,8},{14,10},{16,20},{18,... | collective-permute-start | bytes 196616 | tf_op jit(solution)/shard_map/ppermute | solution.py:379
  39.7 1.8 %collective-permute-done.5.refs_7_ = bf16[2,128,128]{2,1,0:T(8,128)(2,1)S(1)} collective-permute-done((bf16[2,128,128]{2,1,0:T(8,128)(2,1)}, bf16[2,128,128]{2,1,0:T(8,128)(2,1)S(1)}, u32[]{:S(2)}, u32[]{:S(2)}) %collective-permute-start.5) | collective-permute-done | bytes 65568 | tf_op jit(solution)/shard_map/ppermute | solution.py:379
  42.1 2.6 %total_forward.1 = bf16[2,2,128,128]{3,2,1,0:T(8,128)(2,1)} custom-call(s32[1]{0:T(128)} %bitcast.pos_ref, bf16[2,2,128,128]{3,2,1,0:T(8,128)(2,1)} %get-tuple-element.36.refs_0_, bf16[2,2,128,128]{3,2,1,0:T(8,128)(2,1)} %copy-done.2, bf16[2,2,128,128]{3,2,1,0:T(8,128)(2,1)} %copy-done.3, bf16[2,2,128,128]{3,2,1,0:T(8,128)(2,1)} %copy-done.4, ...), custom_call_target="tpu_custom_call" | custom-call | flops 67108864 | bytes 1048576 | tf_op jit(solution)/shard_map/total_forward/pallas_call | solution.py:280
  45.5 7.5 %collective-permute-start.8 = (bf16[1,2,128,128]{3,2,1,0:T(8,128)(2,1)S(1)}, bf16[1,2,128,128]{3,2,1,0:T(8,128)(2,1)S(1)}, u32[]{:S(2)}, u32[]{:S(2)}) collective-permute-start(bf16[1,2,128,128]{3,2,1,0:T(8,128)(2,1)S(1)} %slice.16), channel_id=1, source_target_pairs={{0,24},{2,26},{4,28},{6,30},{1,25},{3,27},{5,29},{7,31}} | collective-permute-start | bytes 196616 | tf_op jit(solution)/shard_map/ppermute | solution.py:382
  53.6 1.3 collective-permute-start.6
  55.0 2.5 %collective-permute-start.7 = (bf16[2,2,128,128]{3,2,1,0:T(8,128)(2,1)}, bf16[2,2,128,128]{3,2,1,0:T(8,128)(2,1)S(1)}, u32[]{:S(2)}, u32[]{:S(2)}) collective-permute-start(bf16[2,2,128,128]{3,2,1,0:T(8,128)(2,1)} %total_forward.1), channel_id=1, source_target_pairs={{0,16},{2,18},{4,20},{6,22},{8,24},{10,26},{12,28},{14,30},{1,17},... | collective-permute-start | bytes 393224 | tf_op jit(solution)/shard_map/ppermute | solution.py:382
  58.8 2.7 %spread_back.1 = (bf16[2,128,128]{2,1,0:T(8,128)(2,1)}, bf16[2,128,128]{2,1,0:T(8,128)(2,1)}, bf16[2,128,128]{2,1,0:T(8,128)(2,1)}, bf16[2,128,128]{2,1,0:T(8,128)(2,1)}) custom-call(s32[1]{0:T(128)} %bitcast.pos_ref, bf16[2,2,128,128]{3,2,1,0:T(8,128)(2,1)} %get-tuple-element.36.refs_0_, bf16[2,2,128,128]{3,2,1,0:T(8,128)(2,1)} %copy-done.2, ...), custom_call_target="tpu_custom_call" | custom-call | flops 67108864 | bytes 1048576 | tf_op jit(solution)/shard_map/spread_back/pallas_call | solution.py:280
  62.3 2.6 %collective-permute-start.17 = (bf16[2,128,128]{2,1,0:T(8,128)(2,1)}, bf16[2,128,128]{2,1,0:T(8,128)(2,1)S(1)}, u32[]{:S(2)}, u32[]{:S(2)}) collective-permute-start(bf16[2,128,128]{2,1,0:T(8,128)(2,1)} %get-tuple-element.55), channel_id=1, source_target_pairs={{0,6},{2,4},{4,2},{6,0},{8,14},{10,12},{12,10},{14,8},{16,22},{18,... | collective-permute-start | bytes 196616 | tf_op jit(solution)/shard_map/ppermute | solution.py:379
  66.4 2.7 %spread_forward.1 = (bf16[2,128,128]{2,1,0:T(8,128)(2,1)}, bf16[2,128,128]{2,1,0:T(8,128)(2,1)}, bf16[2,128,128]{2,1,0:T(8,128)(2,1)}, bf16[2,128,128]{2,1,0:T(8,128)(2,1)}) custom-call(s32[1]{0:T(128)} %bitcast.pos_ref, bf16[2,2,128,128]{3,2,1,0:T(8,128)(2,1)} %get-tuple-element.36.refs_0_, bf16[2,2,128,128]{3,2,1,0:T(8,128)(2,1)} %copy-done.2, ...), custom_call_target="tpu_custom_call" | custom-call | flops 67108864 | bytes 1048576 | tf_op jit(solution)/shard_map/spread_forward/pallas_call | solution.py:280
  69.1 1.4 %collective-permute-start.9 = (bf16[2,128,128]{2,1,0:T(8,128)(2,1)}, bf16[2,128,128]{2,1,0:T(8,128)(2,1)S(1)}, u32[]{:S(2)}, u32[]{:S(2)}) collective-permute-start(bf16[2,128,128]{2,1,0:T(8,128)(2,1)} %get-tuple-element.49), channel_id=1, source_target_pairs={{0,2},{2,0},{4,6},{6,4},{8,10},{10,8},{12,14},{14,12},{16,18},{18,... | collective-permute-start | bytes 196616 | tf_op jit(solution)/shard_map/ppermute | solution.py:379
  70.5 1.5 %collective-permute-start.10 = (bf16[2,128,128]{2,1,0:T(8,128)(2,1)}, bf16[2,128,128]{2,1,0:T(8,128)(2,1)S(1)}, u32[]{:S(2)}, u32[]{:S(2)}) collective-permute-start(bf16[2,128,128]{2,1,0:T(8,128)(2,1)} %get-tuple-element.50), channel_id=1, source_target_pairs={{0,4},{2,6},{4,0},{6,2},{8,12},{10,14},{12,8},{14,10},{16,20},{18,... | collective-permute-start | bytes 196616 | tf_op jit(solution)/shard_map/ppermute | solution.py:379
  73.2 3.1 %values.1 = bf16[256,1024]{1,0:T(8,128)(2,1)} custom-call(s32[1]{0:T(128)} %bitcast.pos_ref, bf16[256,1024]{1,0:T(8,128)(2,1)} %get-tuple-element.34.dr_ref, bf16[256,1024]{1,0:T(8,128)(2,1)} %get-tuple-element.35.y_ref, f32[8,256]{1,0:T(8,128)} %bitcast.66, bf16[2,128,128]{2,1,0:T(8,128)(2,1)} %get-tuple-element.52.refs_4_.refs_0_, ...), custom_call_target="tpu_custom_call" | custom-call | flops 67108864 | bytes 1048576 | tf_op jit(solution)/shard_map/values/pallas_call | solution.py:280
  77.4 2.4 %collective-permute-start.30 = (bf16[256,512]{1,0:T(8,128)(2,1)S(1)}, bf16[256,512]{1,0:T(8,128)(2,1)S(1)}, u32[]{:S(2)}, u32[]{:S(2)}) collective-permute-start(bf16[256,512]{1,0:T(8,128)(2,1)S(1)} %get-tuple-element.71), channel_id=1, source_target_pairs={{0,6},{2,4},{4,2},{6,0},{8,14},{10,12},{12,10},{14,8},{16,22},{18,... | collective-permute-start | bytes 786440 | tf_op jit(solution)/shard_map/ppermute | solution.py:379
  79.8 3.8 %convolution_convert_fusion = bf16[128,2048]{1,0:T(8,128)(2,1)S(1)} fusion(bf16[2048,1024]{1,0:T(8,128)(2,1)} %param.11, bf16[256,1024]{1,0:T(8,128)(2,1)} %values.1, s32[]{:T(128)S(6)} %select_n.37), kind=kOutput, calls=%fused_computation.2 | convolution fusion | flops 537133056 | bytes 4980740 | tf_op jit(solution)/shard_map/dot_general | solution.py:476
  84.8 1.5 %collective-permute-start.29 = (bf16[256,512]{1,0:T(8,128)(2,1)S(1)}, bf16[256,512]{1,0:T(8,128)(2,1)S(1)}, u32[]{:S(2)}, u32[]{:S(2)}) collective-permute-start(bf16[256,512]{1,0:T(8,128)(2,1)S(1)} %get-tuple-element.71), channel_id=1, source_target_pairs={{0,4},{2,6},{4,0},{6,2},{8,12},{10,14},{12,8},{14,10},{16,20},{18,... | collective-permute-start | bytes 786440 | tf_op jit(solution)/shard_map/ppermute | solution.py:379
  86.3 10.1 %grads.1 = (bf16[256,1024]{1,0:T(8,128)(2,1)}, bf16[256,1024]{1,0:T(8,128)(2,1)}, f32[8,256]{1,0:T(8,128)}, f32[8,256]{1,0:T(8,128)}) custom-call(s32[1]{0:T(128)} %bitcast.pos_ref, bf16[256,1024]{1,0:T(8,128)(2,1)} %q_ref.3, bf16[256,1024]{1,0:T(8,128)(2,1)} %k_ref.3, bf16[256,1024]{1,0:T(8,128)(2,1)} %convolution_convert_fusion.1.v_ref, ...), custom_call_target="tpu_custom_call" | custom-call | flops 134217728 | bytes 1048576 | tf_op jit(solution)/shard_map/grads/pallas_call | solution.py:280
  96.4 1.5 %collective-permute-start.28 = (bf16[256,512]{1,0:T(8,128)(2,1)S(1)}, bf16[256,512]{1,0:T(8,128)(2,1)S(1)}, u32[]{:S(2)}, u32[]{:S(2)}) collective-permute-start(bf16[256,512]{1,0:T(8,128)(2,1)S(1)} %get-tuple-element.71), channel_id=1, source_target_pairs={{0,2},{2,0},{4,6},{6,4},{8,10},{10,8},{12,14},{14,12},{16,18},{18,... | collective-permute-start | bytes 786440 | tf_op jit(solution)/shard_map/ppermute | solution.py:379
  98.8 1.5 %collective-permute-start.22 = (bf16[256,512]{1,0:T(8,128)(2,1)S(1)}, bf16[256,512]{1,0:T(8,128)(2,1)S(1)}, u32[]{:S(2)}, u32[]{:S(2)}) collective-permute-start(bf16[256,512]{1,0:T(8,128)(2,1)S(1)} %get-tuple-element.70), channel_id=1, source_target_pairs={{0,4},{2,6},{4,0},{6,2},{8,12},{10,14},{12,8},{14,10},{16,20},{18,... | collective-permute-start | bytes 786440 | tf_op jit(solution)/shard_map/ppermute | solution.py:379
  100.3 1.4 %collective-permute-start.20 = (bf16[256,512]{1,0:T(8,128)(2,1)S(1)}, bf16[256,512]{1,0:T(8,128)(2,1)S(1)}, u32[]{:S(2)}, u32[]{:S(2)}) collective-permute-start(bf16[256,512]{1,0:T(8,128)(2,1)S(1)} %get-tuple-element.70), channel_id=1, source_target_pairs={{0,2},{2,0},{4,6},{6,4},{8,10},{10,8},{12,14},{14,12},{16,18},{18,... | collective-permute-start | bytes 786440 | tf_op jit(solution)/shard_map/ppermute | solution.py:379
  102.2 1.3 collective-permute-done.28
  104.2 2.7 %collective-permute-done.24 = bf16[256,512]{1,0:T(8,128)(2,1)S(1)} collective-permute-done((bf16[256,512]{1,0:T(8,128)(2,1)S(1)}, bf16[256,512]{1,0:T(8,128)(2,1)S(1)}, u32[]{:S(2)}, u32[]{:S(2)}) %collective-permute-start.24) | collective-permute-done | bytes 262176 | tf_op jit(solution)/shard_map/ppermute | solution.py:379
  109.8 3.1 %collective-permute-start.27 = (bf16[128,512]{1,0:T(8,128)(2,1)S(1)}, bf16[128,512]{1,0:T(8,128)(2,1)S(1)}, u32[]{:S(2)}, u32[]{:S(2)}) collective-permute-start(bf16[128,512]{1,0:T(8,128)(2,1)S(1)} %get-tuple-element.61), channel_id=1, source_target_pairs={{0,24},{2,26},{4,28},{6,30},{8,0},{10,2},{12,4},{14,6},{16,8},{18,... | collective-permute-start | bytes 393224 | tf_op jit(solution)/shard_map/ppermute | solution.py:450
  113.3 7.5 %collective-permute-done.32 = bf16[128,512]{1,0:T(8,128)(2,1)S(1)} collective-permute-done((bf16[128,512]{1,0:T(8,128)(2,1)S(1)}, bf16[128,512]{1,0:T(8,128)(2,1)S(1)}, u32[]{:S(2)}, u32[]{:S(2)}) %collective-permute-start.32) | collective-permute-done | bytes 131104 | tf_op jit(solution)/shard_map/ppermute | solution.py:450
  120.9 7.1 %collective-permute-done.26 = bf16[128,512]{1,0:T(8,128)(2,1)S(1)} collective-permute-done((bf16[128,512]{1,0:T(8,128)(2,1)S(1)}, bf16[128,512]{1,0:T(8,128)(2,1)S(1)}, u32[]{:S(2)}, u32[]{:S(2)}) %collective-permute-start.26) | collective-permute-done | bytes 131104 | tf_op jit(solution)/shard_map/ppermute | solution.py:450
  128.8 2.3 %fusion = bf16[128,2048]{1,0:T(8,128)(2,1)} fusion(bf16[2048,1024]{1,0:T(8,128)(2,1)S(1)} %copy-done, bf16[128,2048]{1,0:T(8,128)(2,1)S(1)} %collective-permute-done.18, bf16[256,1024]{1,0:T(8,128)(2,1)S(1)} %copy-done.1, s32[]{:T(128)S(6)} %select_n.36), kind=kOutput, calls=%fused_computation.1 | convolution fusion | flops 537657344 | bytes 5505028 | tf_op jit(solution)/shard_map/dot_general | solution.py:476
  (107 shorter events, 22.1 us)
Async XLA Ops:
  14.4 12.3 %collective-permute-start = (bf16[2,2,128,128]{3,2,1,0:T(8,128)(2,1)}, bf16[2,2,128,128]{3,2,1,0:T(8,128)(2,1)S(1)}, u32[]{:S(2)}, u32[]{:S(2)}) collective-permute-start(bf16[2,2,128,128]{3,2,1,0:T(8,128)(2,1)} %get-tuple-element.37), channel_id=1, source_target_pairs={{0,2},{2,0},{4,6},{6,4},{8,10},{10,8},{12,14},{14,12},{16,18},{18,... | collective-permute-start | bytes 393224 | tf_op jit(solution)/shard_map/ppermute | solution.py:379
  17.4 9.3 %collective-permute-start.1 = (bf16[2,2,128,128]{3,2,1,0:T(8,128)(2,1)}, bf16[2,2,128,128]{3,2,1,0:T(8,128)(2,1)S(1)}, u32[]{:S(2)}, u32[]{:S(2)}) collective-permute-start(bf16[2,2,128,128]{3,2,1,0:T(8,128)(2,1)} %get-tuple-element.38), channel_id=1, source_target_pairs={{0,4},{2,6},{4,0},{6,2},{8,12},{10,14},{12,8},{14,10},{16,20},{18,... | collective-permute-start | bytes 393224 | tf_op jit(solution)/shard_map/ppermute | solution.py:379
  18.9 8.0 %collective-permute-start.2 = (bf16[2,2,128,128]{3,2,1,0:T(8,128)(2,1)}, bf16[2,2,128,128]{3,2,1,0:T(8,128)(2,1)S(1)}, u32[]{:S(2)}, u32[]{:S(2)}) collective-permute-start(bf16[2,2,128,128]{3,2,1,0:T(8,128)(2,1)} %get-tuple-element.39), channel_id=1, source_target_pairs={{0,6},{2,4},{4,2},{6,0},{8,14},{10,12},{12,10},{14,8},{16,22},{18,... | collective-permute-start | bytes 393224 | tf_op jit(solution)/shard_map/ppermute | solution.py:379
  30.1 7.0 %collective-permute-start.3 = (bf16[2,128,128]{2,1,0:T(8,128)(2,1)}, bf16[2,128,128]{2,1,0:T(8,128)(2,1)S(1)}, u32[]{:S(2)}, u32[]{:S(2)}) collective-permute-start(bf16[2,128,128]{2,1,0:T(8,128)(2,1)} %get-tuple-element.45), channel_id=1, source_target_pairs={{0,2},{2,0},{4,6},{6,4},{8,10},{10,8},{12,14},{14,12},{16,18},{18,... | collective-permute-start | bytes 196616 | tf_op jit(solution)/shard_map/ppermute | solution.py:379
  32.0 25.5 %collective-permute-start.12 = (bf16[2,2,128,128]{3,2,1,0:T(8,128)(2,1)}, bf16[2,2,128,128]{3,2,1,0:T(8,128)(2,1)S(1)}, u32[]{:S(2)}, u32[]{:S(2)}) collective-permute-start(bf16[2,2,128,128]{3,2,1,0:T(8,128)(2,1)} %total_back.1), channel_id=1, source_target_pairs={{8,0},{10,2},{12,4},{14,6},{16,8},{18,10},{20,12},{22,14},{24,16},... | collective-permute-start | bytes 393224 | tf_op jit(solution)/shard_map/ppermute | solution.py:382
  33.3 24.2 %collective-permute-start.13 = (bf16[2,2,128,128]{3,2,1,0:T(8,128)(2,1)}, bf16[2,2,128,128]{3,2,1,0:T(8,128)(2,1)S(1)}, u32[]{:S(2)}, u32[]{:S(2)}) collective-permute-start(bf16[2,2,128,128]{3,2,1,0:T(8,128)(2,1)} %total_back.1), channel_id=1, source_target_pairs={{16,0},{18,2},{20,4},{22,6},{24,8},{26,10},{28,12},{30,14},{17,1},... | collective-permute-start | bytes 393224 | tf_op jit(solution)/shard_map/ppermute | solution.py:382
  37.1 17.9 %collective-permute-start.14 = (bf16[1,2,128,128]{3,2,1,0:T(8,128)(2,1)S(1)}, bf16[1,2,128,128]{3,2,1,0:T(8,128)(2,1)S(1)}, u32[]{:S(2)}, u32[]{:S(2)}) collective-permute-start(bf16[1,2,128,128]{3,2,1,0:T(8,128)(2,1)S(1)} %slice.17), channel_id=1, source_target_pairs={{24,0},{26,2},{28,4},{30,6},{25,1},{27,3},{29,5},{31,7}} | collective-permute-start | bytes 196616 | tf_op jit(solution)/shard_map/ppermute | solution.py:382
  45.5 16.8 %collective-permute-start.8 = (bf16[1,2,128,128]{3,2,1,0:T(8,128)(2,1)S(1)}, bf16[1,2,128,128]{3,2,1,0:T(8,128)(2,1)S(1)}, u32[]{:S(2)}, u32[]{:S(2)}) collective-permute-start(bf16[1,2,128,128]{3,2,1,0:T(8,128)(2,1)S(1)} %slice.16), channel_id=1, source_target_pairs={{0,24},{2,26},{4,28},{6,30},{1,25},{3,27},{5,29},{7,31}} | collective-permute-start | bytes 196616 | tf_op jit(solution)/shard_map/ppermute | solution.py:382
  53.6 11.4 %collective-permute-start.6 = (bf16[2,2,128,128]{3,2,1,0:T(8,128)(2,1)}, bf16[2,2,128,128]{3,2,1,0:T(8,128)(2,1)S(1)}, u32[]{:S(2)}, u32[]{:S(2)}) collective-permute-start(bf16[2,2,128,128]{3,2,1,0:T(8,128)(2,1)} %total_forward.1), channel_id=1, source_target_pairs={{0,8},{2,10},{4,12},{6,14},{8,16},{10,18},{12,20},{14,22},{16,24},... | collective-permute-start | bytes 393224 | tf_op jit(solution)/shard_map/ppermute | solution.py:382
  55.0 10.5 %collective-permute-start.7 = (bf16[2,2,128,128]{3,2,1,0:T(8,128)(2,1)}, bf16[2,2,128,128]{3,2,1,0:T(8,128)(2,1)S(1)}, u32[]{:S(2)}, u32[]{:S(2)}) collective-permute-start(bf16[2,2,128,128]{3,2,1,0:T(8,128)(2,1)} %total_forward.1), channel_id=1, source_target_pairs={{0,16},{2,18},{4,20},{6,22},{8,24},{10,26},{12,28},{14,30},{1,17},... | collective-permute-start | bytes 393224 | tf_op jit(solution)/shard_map/ppermute | solution.py:382
  61.4 9.1 %collective-permute-start.15 = (bf16[2,128,128]{2,1,0:T(8,128)(2,1)}, bf16[2,128,128]{2,1,0:T(8,128)(2,1)S(1)}, u32[]{:S(2)}, u32[]{:S(2)}) collective-permute-start(bf16[2,128,128]{2,1,0:T(8,128)(2,1)} %get-tuple-element.53), channel_id=1, source_target_pairs={{0,2},{2,0},{4,6},{6,4},{8,10},{10,8},{12,14},{14,12},{16,18},{18,... | collective-permute-start | bytes 196616 | tf_op jit(solution)/shard_map/ppermute | solution.py:379
  62.0 10.0 %collective-permute-start.16 = (bf16[2,128,128]{2,1,0:T(8,128)(2,1)}, bf16[2,128,128]{2,1,0:T(8,128)(2,1)S(1)}, u32[]{:S(2)}, u32[]{:S(2)}) collective-permute-start(bf16[2,128,128]{2,1,0:T(8,128)(2,1)} %get-tuple-element.54), channel_id=1, source_target_pairs={{0,4},{2,6},{4,0},{6,2},{8,12},{10,14},{12,8},{14,10},{16,20},{18,... | collective-permute-start | bytes 196616 | tf_op jit(solution)/shard_map/ppermute | solution.py:379
  62.3 10.3 %collective-permute-start.17 = (bf16[2,128,128]{2,1,0:T(8,128)(2,1)}, bf16[2,128,128]{2,1,0:T(8,128)(2,1)S(1)}, u32[]{:S(2)}, u32[]{:S(2)}) collective-permute-start(bf16[2,128,128]{2,1,0:T(8,128)(2,1)} %get-tuple-element.55), channel_id=1, source_target_pairs={{0,6},{2,4},{4,2},{6,0},{8,14},{10,12},{12,10},{14,8},{16,22},{18,... | collective-permute-start | bytes 196616 | tf_op jit(solution)/shard_map/ppermute | solution.py:379
  65.1 31.3 %collective-permute-start.23 = (bf16[256,512]{0,1:T(8,128)(2,1)S(1)}, bf16[256,512]{0,1:T(8,128)(2,1)S(1)}, u32[]{:S(2)}, u32[]{:S(2)}) collective-permute-start(bf16[256,512]{0,1:T(8,128)(2,1)S(1)} %bitcast.63), channel_id=1, source_target_pairs={{0,6},{2,4},{4,2},{6,0},{8,14},{10,12},{12,10},{14,8},{16,22},{18,... | collective-permute-start | bytes 786440 | tf_op jit(solution)/shard_map/ppermute | solution.py:379
  69.1 14.5 %collective-permute-start.9 = (bf16[2,128,128]{2,1,0:T(8,128)(2,1)}, bf16[2,128,128]{2,1,0:T(8,128)(2,1)S(1)}, u32[]{:S(2)}, u32[]{:S(2)}) collective-permute-start(bf16[2,128,128]{2,1,0:T(8,128)(2,1)} %get-tuple-element.49), channel_id=1, source_target_pairs={{0,2},{2,0},{4,6},{6,4},{8,10},{10,8},{12,14},{14,12},{16,18},{18,... | collective-permute-start | bytes 196616 | tf_op jit(solution)/shard_map/ppermute | solution.py:379
  70.5 13.7 %collective-permute-start.10 = (bf16[2,128,128]{2,1,0:T(8,128)(2,1)}, bf16[2,128,128]{2,1,0:T(8,128)(2,1)S(1)}, u32[]{:S(2)}, u32[]{:S(2)}) collective-permute-start(bf16[2,128,128]{2,1,0:T(8,128)(2,1)} %get-tuple-element.50), channel_id=1, source_target_pairs={{0,4},{2,6},{4,0},{6,2},{8,12},{10,14},{12,8},{14,10},{16,20},{18,... | collective-permute-start | bytes 196616 | tf_op jit(solution)/shard_map/ppermute | solution.py:379
  72.0 12.8 %collective-permute-start.11 = (bf16[2,128,128]{2,1,0:T(8,128)(2,1)}, bf16[2,128,128]{2,1,0:T(8,128)(2,1)S(1)}, u32[]{:S(2)}, u32[]{:S(2)}) collective-permute-start(bf16[2,128,128]{2,1,0:T(8,128)(2,1)} %get-tuple-element.51), channel_id=1, source_target_pairs={{0,6},{2,4},{4,2},{6,0},{8,14},{10,12},{12,10},{14,8},{16,22},{18,... | collective-permute-start | bytes 196616 | tf_op jit(solution)/shard_map/ppermute | solution.py:379
  77.4 20.5 %collective-permute-start.30 = (bf16[256,512]{1,0:T(8,128)(2,1)S(1)}, bf16[256,512]{1,0:T(8,128)(2,1)S(1)}, u32[]{:S(2)}, u32[]{:S(2)}) collective-permute-start(bf16[256,512]{1,0:T(8,128)(2,1)S(1)} %get-tuple-element.71), channel_id=1, source_target_pairs={{0,6},{2,4},{4,2},{6,0},{8,14},{10,12},{12,10},{14,8},{16,22},{18,... | collective-permute-start | bytes 786440 | tf_op jit(solution)/shard_map/ppermute | solution.py:379
  83.6 15.2 %collective-permute-start.21 = (bf16[256,512]{0,1:T(8,128)(2,1)S(1)}, bf16[256,512]{0,1:T(8,128)(2,1)S(1)}, u32[]{:S(2)}, u32[]{:S(2)}) collective-permute-start(bf16[256,512]{0,1:T(8,128)(2,1)S(1)} %bitcast.62), channel_id=1, source_target_pairs={{0,4},{2,6},{4,0},{6,2},{8,12},{10,14},{12,8},{14,10},{16,20},{18,... | collective-permute-start | bytes 786440 | tf_op jit(solution)/shard_map/ppermute | solution.py:379
  84.2 17.9 %collective-permute-start.19 = (bf16[256,512]{0,1:T(8,128)(2,1)S(1)}, bf16[256,512]{0,1:T(8,128)(2,1)S(1)}, u32[]{:S(2)}, u32[]{:S(2)}) collective-permute-start(bf16[256,512]{0,1:T(8,128)(2,1)S(1)} %bitcast.61), channel_id=1, source_target_pairs={{0,2},{2,0},{4,6},{6,4},{8,10},{10,8},{12,14},{14,12},{16,18},{18,... | collective-permute-start | bytes 786440 | tf_op jit(solution)/shard_map/ppermute | solution.py:379
  84.8 15.5 %collective-permute-start.29 = (bf16[256,512]{1,0:T(8,128)(2,1)S(1)}, bf16[256,512]{1,0:T(8,128)(2,1)S(1)}, u32[]{:S(2)}, u32[]{:S(2)}) collective-permute-start(bf16[256,512]{1,0:T(8,128)(2,1)S(1)} %get-tuple-element.71), channel_id=1, source_target_pairs={{0,4},{2,6},{4,0},{6,2},{8,12},{10,14},{12,8},{14,10},{16,20},{18,... | collective-permute-start | bytes 786440 | tf_op jit(solution)/shard_map/ppermute | solution.py:379
  96.4 7.1 %collective-permute-start.28 = (bf16[256,512]{1,0:T(8,128)(2,1)S(1)}, bf16[256,512]{1,0:T(8,128)(2,1)S(1)}, u32[]{:S(2)}, u32[]{:S(2)}) collective-permute-start(bf16[256,512]{1,0:T(8,128)(2,1)S(1)} %get-tuple-element.71), channel_id=1, source_target_pairs={{0,2},{2,0},{4,6},{6,4},{8,10},{10,8},{12,14},{14,12},{16,18},{18,... | collective-permute-start | bytes 786440 | tf_op jit(solution)/shard_map/ppermute | solution.py:379
  97.9 9.0 %collective-permute-start.24 = (bf16[256,512]{1,0:T(8,128)(2,1)S(1)}, bf16[256,512]{1,0:T(8,128)(2,1)S(1)}, u32[]{:S(2)}, u32[]{:S(2)}) collective-permute-start(bf16[256,512]{1,0:T(8,128)(2,1)S(1)} %get-tuple-element.70), channel_id=1, source_target_pairs={{0,6},{2,4},{4,2},{6,0},{8,14},{10,12},{12,10},{14,8},{16,22},{18,... | collective-permute-start | bytes 786440 | tf_op jit(solution)/shard_map/ppermute | solution.py:379
  98.8 9.2 %collective-permute-start.22 = (bf16[256,512]{1,0:T(8,128)(2,1)S(1)}, bf16[256,512]{1,0:T(8,128)(2,1)S(1)}, u32[]{:S(2)}, u32[]{:S(2)}) collective-permute-start(bf16[256,512]{1,0:T(8,128)(2,1)S(1)} %get-tuple-element.70), channel_id=1, source_target_pairs={{0,4},{2,6},{4,0},{6,2},{8,12},{10,14},{12,8},{14,10},{16,20},{18,... | collective-permute-start | bytes 786440 | tf_op jit(solution)/shard_map/ppermute | solution.py:379
  100.3 8.8 %collective-permute-start.20 = (bf16[256,512]{1,0:T(8,128)(2,1)S(1)}, bf16[256,512]{1,0:T(8,128)(2,1)S(1)}, u32[]{:S(2)}, u32[]{:S(2)}) collective-permute-start(bf16[256,512]{1,0:T(8,128)(2,1)S(1)} %get-tuple-element.70), channel_id=1, source_target_pairs={{0,2},{2,0},{4,6},{6,4},{8,10},{10,8},{12,14},{14,12},{16,18},{18,... | collective-permute-start | bytes 786440 | tf_op jit(solution)/shard_map/ppermute | solution.py:379
  102.1 26.8 %collective-permute-start.18 = (bf16[128,2048]{1,0:T(8,128)(2,1)S(1)}, bf16[128,2048]{1,0:T(8,128)(2,1)S(1)}, u32[]{:S(2)}, u32[]{:S(2)}) collective-permute-start(bf16[128,2048]{1,0:T(8,128)(2,1)S(1)} %convolution_convert_fusion), channel_id=1, source_target_pairs={{0,1},{1,0},{2,3},{3,2},{4,5},{5,4},{6,7},{7,6},{8,9},{9,8},{10,11... | collective-permute-start | bytes 1572872 | tf_op jit(solution)/shard_map/ppermute | solution.py:482
  104.1 8.7 %collective-permute-start.33 = (bf16[128,512]{1,0:T(8,128)(2,1)S(1)}, bf16[128,512]{1,0:T(8,128)(2,1)S(1)}, u32[]{:S(2)}, u32[]{:S(2)}) collective-permute-start(bf16[128,512]{1,0:T(8,128)(2,1)S(1)} %get-tuple-element.64), channel_id=1, source_target_pairs={{0,24},{2,26},{4,28},{6,30},{8,0},{10,2},{12,4},{14,6},{16,8},{18,... | collective-permute-start | bytes 393224 | tf_op jit(solution)/shard_map/ppermute | solution.py:450
  106.9 13.9 %collective-permute-start.32 = (bf16[128,512]{1,0:T(8,128)(2,1)S(1)}, bf16[128,512]{1,0:T(8,128)(2,1)S(1)}, u32[]{:S(2)}, u32[]{:S(2)}) collective-permute-start(bf16[128,512]{1,0:T(8,128)(2,1)S(1)} %get-tuple-element.65), channel_id=1, source_target_pairs={{0,16},{2,18},{4,20},{6,22},{8,24},{10,26},{12,28},{14,30},{16,0},... | collective-permute-start | bytes 393224 | tf_op jit(solution)/shard_map/ppermute | solution.py:450
  108.0 12.8 %collective-permute-start.31 = (bf16[128,512]{1,0:T(8,128)(2,1)S(1)}, bf16[128,512]{1,0:T(8,128)(2,1)S(1)}, u32[]{:S(2)}, u32[]{:S(2)}) collective-permute-start(bf16[128,512]{1,0:T(8,128)(2,1)S(1)} %get-tuple-element.63), channel_id=1, source_target_pairs={{0,8},{2,10},{4,12},{6,14},{8,16},{10,18},{12,20},{14,22},{16,24},... | collective-permute-start | bytes 393224 | tf_op jit(solution)/shard_map/ppermute | solution.py:450
  109.8 11.0 %collective-permute-start.27 = (bf16[128,512]{1,0:T(8,128)(2,1)S(1)}, bf16[128,512]{1,0:T(8,128)(2,1)S(1)}, u32[]{:S(2)}, u32[]{:S(2)}) collective-permute-start(bf16[128,512]{1,0:T(8,128)(2,1)S(1)} %get-tuple-element.61), channel_id=1, source_target_pairs={{0,24},{2,26},{4,28},{6,30},{8,0},{10,2},{12,4},{14,6},{16,8},{18,... | collective-permute-start | bytes 393224 | tf_op jit(solution)/shard_map/ppermute | solution.py:450
  112.9 15.0 %collective-permute-start.26 = (bf16[128,512]{1,0:T(8,128)(2,1)S(1)}, bf16[128,512]{1,0:T(8,128)(2,1)S(1)}, u32[]{:S(2)}, u32[]{:S(2)}) collective-permute-start(bf16[128,512]{1,0:T(8,128)(2,1)S(1)} %get-tuple-element.62), channel_id=1, source_target_pairs={{0,16},{2,18},{4,20},{6,22},{8,24},{10,26},{12,28},{14,30},{16,0},... | collective-permute-start | bytes 393224 | tf_op jit(solution)/shard_map/ppermute | solution.py:450
  120.8 7.1 %collective-permute-start.25 = (bf16[128,512]{1,0:T(8,128)(2,1)S(1)}, bf16[128,512]{1,0:T(8,128)(2,1)S(1)}, u32[]{:S(2)}, u32[]{:S(2)}) collective-permute-start(bf16[128,512]{1,0:T(8,128)(2,1)S(1)} %get-tuple-element.60), channel_id=1, source_target_pairs={{0,8},{2,10},{4,12},{6,14},{8,16},{10,18},{12,20},{14,22},{16,24},... | collective-permute-start | bytes 393224 | tf_op jit(solution)/shard_map/ppermute | solution.py:450
  (23 other events, 108.3 us)

commit v3 on v2

v3 whole, which is shorter than its diff:
```python
import functools

import jax
import jax.numpy as jnp
from jax import lax
from jax.experimental import pallas as pl
from jax.experimental.pallas import tpu as pltpu
from jax.sharding import PartitionSpec as P


NORM_FLOOR = 16.0
F32 = jnp.float32
BF16 = jnp.bfloat16
HIGHEST = lax.Precision.HIGHEST
VMEM_LIMIT = 56 * 1024 * 1024
PACK = 8
CHUNKS = 2


def dot(a, b, ca=1, cb=0, precision=None):
    return lax.dot_general(
        a, b, (((ca,), (cb,)), ((), ())), precision=precision, preferred_element_type=F32
    )


def low(x):
    return x.astype(BF16)


def iotas(n):
    rows = lax.broadcasted_iota(jnp.int32, (n, n), 0)
    cols = lax.broadcasted_iota(jnp.int32, (n, n), 1)
    return rows, cols


def columns(rows):
    count, n = rows.shape
    return jnp.transpose(jnp.concatenate([rows, jnp.zeros((128 - count, n), F32)], axis=0))


def rate_column(rate_ref):
    count = rate_ref.shape[0]
    row = lax.broadcasted_iota(jnp.int32, (count, 1), 0)
    out = jnp.zeros((count, 1), F32)
    for h in range(count):
        out = jnp.where(row == h, rate_ref[h], out)
    return out


def sigmoid(x):
    return 1.0 / (1.0 + jnp.exp(-x))


def head_columns(beta_ref, decay_ref, rate_ref, g_ref, b_ref, gt_ref):
    decay = decay_ref[...]
    n = decay.shape[1]
    rows, cols = iotas(n)
    log_decay = -rate_column(rate_ref) * (
        jnp.maximum(decay, 0.0) + jnp.log1p(jnp.exp(-jnp.abs(decay)))
    )
    sums = dot(log_decay, (rows <= cols).astype(F32), precision=HIGHEST)
    gt_ref[...] = sums
    g_ref[...] = columns(sums)
    b_ref[...] = columns(sigmoid(beta_ref[...]))


def lane_column(ref, head):
    return jnp.broadcast_to(ref[:, head : head + 1], ref.shape)


class Head:
    pass


def lanes_of(head, size):
    return slice(head * size, (head + 1) * size)


def head_common(q_ref, k_ref, head, size, g_ref, b_ref, gt_ref):
    h = Head()
    n = q_ref.shape[0]
    h.head, h.n, h.size = head, n, size
    h.lanes = lanes_of(head, size)
    h.k16, h.q16 = k_ref[:, h.lanes], q_ref[:, h.lanes]
    k32, q32 = h.k16.astype(F32), h.q16.astype(F32)
    h.g = lane_column(g_ref, head)
    h.beta = lane_column(b_ref, head)
    norm = lambda x: jnp.broadcast_to(
        lax.rsqrt(jnp.sum(x * x, axis=1, keepdims=True) + NORM_FLOOR), (n, size)
    )
    h.rk, h.rq = norm(k32), norm(q32)
    g_row = gt_ref[head : head + 1, :]
    rk_row = jnp.transpose(h.rk)[0:1, :]
    rows, cols = iotas(n)
    h.tile = lambda x: jnp.concatenate([x] * (n // size), axis=1)
    spread = jnp.where(rows >= cols, h.tile(h.g) - g_row, -1e30)
    h.gamma_rk = jnp.exp(spread) * rk_row
    gram = dot(jnp.concatenate([h.k16, h.q16], axis=0), h.k16, 1, 1)
    h.scale = size**-0.5
    h.a0 = jnp.where(rows > cols, gram[:n] * h.gamma_rk * h.tile(h.rk), 0.0)
    h.p = gram[n:] * h.gamma_rk * h.tile(h.rq * h.scale)
    g_end = h.g[n - 1 : n, :]
    h.k_hat, h.q_hat = k32 * h.rk, q32 * (h.rq * h.scale)
    h.gain, h.tail, h.gain_end = jnp.exp(h.g), jnp.exp(g_end - h.g), jnp.exp(g_end)
    return h


def unit_lower_inverses(mats):
    n = mats[0].shape[0]
    rows, cols = iotas(n)
    differ = rows ^ cols
    eye = (rows == cols).astype(F32)
    high = [low(a) for a in mats]
    xs = [low(eye) - a * low((differ == 1).astype(F32)) for a in high]
    size = 2
    while 2 * size < n:
        mask = low(((differ >= size) & (differ < 2 * size)).astype(F32))
        ys = [low(dot(a * mask, x)) for a, x in zip(high, xs)]
        xs = [x - low(dot(x, y)) for x, y in zip(xs, ys)]
        size *= 2
    ys = [low(dot(a[size:, :size], x[:size, :size])) for a, x in zip(high, xs)]
    zs = [low(-dot(x[size:, size:], y)) for x, y in zip(xs, ys)]
    xs = [
        jnp.concatenate([x[:size], jnp.concatenate([z, x[size:, size:]], axis=1)], axis=0)
        for x, z in zip(xs, zs)
    ]
    rest = [low(a - h.astype(F32)) for a, h in zip(mats, high)]
    products = [
        dot(jnp.concatenate([h, l], axis=1), jnp.concatenate([x, x], axis=0))
        for h, l, x in zip(high, rest, xs)
    ]
    return [
        low(x.astype(F32) + dot(x, low(eye - x.astype(F32) - y))) for x, y in zip(xs, products)
    ]


def local_kernel(pack, share, outer, pos_ref, q_ref, k_ref, do_ref, hid_ref, w_ref, bp_ref, dp_ref, rate_ref, maps,
                 *refs):
    inv_ref, dr_ref, y_ref, bdr_ref, by_ref, v_ref, g_ref, b_ref, gt_ref, hid, hid_t, w, sems = refs[: 6] + refs[6 + maps.shape[0] :]
    hid_parts = refs[6 : 6 + maps.shape[0]]
    copies = [
        pltpu.make_async_copy(hid_ref, hid, sems.at[0]),
        pltpu.make_async_copy(w_ref, w, sems.at[1]),
    ]
    for copy in copies:
        copy.start()
    head_columns(bp_ref, dp_ref, rate_ref, g_ref, b_ref, gt_ref)
    size = maps.shape[-1]
    for start in range(0, maps.shape[0] * share, pack):
        places = range(start, start + pack)
        heads = [head_common(q_ref, k_ref, p, size, g_ref, b_ref, gt_ref) for p in places]
        outs = [do_ref[:, h.lanes] for h in heads]
        d_written = [low(dot(low(h.p), do16, 0, 0)) for h, do16 in zip(heads, outs)]
        invs = unit_lower_inverses([h.a0 * h.tile(h.beta) for h in heads])
        tails = [low(h.k_hat * h.tail) for h in heads]
        both = [
            dot(inv, jnp.concatenate([d, t], axis=1), 0, 0)
            for inv, d, t in zip(invs, d_written, tails)
        ]
        if start == 0:
            for copy in copies:
                copy.wait()
            v_ref[...] = low(dot(hid[...], w[...]))
            rows = hid.shape[1] // outer // maps.shape[0]
            hid_t[...] = jnp.transpose(hid[...])
            for d, part in enumerate(hid_parts):
                for e in range(outer):
                    at = pl.multiple_of((e * maps.shape[0] + (pos_ref[0] ^ d)) * rows, rows)
                    part[e * rows : (e + 1) * rows, :] = hid_t[pl.ds(at, rows), :]
        eye = lax.broadcasted_iota(jnp.int32, (size, size), 0) == lax.broadcasted_iota(
            jnp.int32, (size, size), 1
        )
        for p, h, inv, do16, b32 in zip(places, heads, invs, outs, both):
            dr16, y16 = low(b32[:, :size]), low(b32[:, size:])
            inv_ref[p] = inv
            dr_ref[:, h.lanes] = dr16
            y_ref[:, h.lanes] = y16
            bdr_ref[:, h.lanes] = low(h.beta * b32[:, :size])
            by_ref[:, h.lanes] = low(h.beta * b32[:, size:])
            k_in = low(h.k_hat * h.beta * h.gain)
            value = low(h.beta * v_ref[:, h.lanes].astype(F32))
            out = maps.at[p // share]
            into = dot(y16, jnp.concatenate([k_in, value], axis=1), 0, 0)
            out[0, p % share] = low(jnp.where(eye, h.gain_end, 0.0) - into[:, :size])
            own = dot(
                jnp.concatenate([do16, dr16], axis=0),
                jnp.concatenate([low(h.q_hat * h.gain), -k_in], axis=0), 0, 0,
            )
            out[1, p % share] = low(own)
            out[2, p % share] = low(into[:, size:])


def values_kernel(share, chunks, bdr_ref, by_ref, states, dv_ref, *parts):
    size = states.shape[-1]
    count = states.shape[0] * share
    per = count // chunks
    for h in range(count):
        lanes = slice(h * size, (h + 1) * size)
        dv = low(bdr_ref[:, lanes].astype(F32) + dot(by_ref[:, lanes], states[h // share, 0, h % share], 1, 1))
        dv_ref[:, lanes] = dv
        parts[h // per][:, (h % per) * size : (h % per + 1) * size] = dv


def weight_kernel(group, outer, lead_ref, *refs):
    hid_refs, grad_refs, out_refs, store = refs[:group], refs[group : 2 * group], refs[2 * group : -1], refs[-1]
    rows = store.shape[0] // outer
    store[...] = dot(
        jnp.concatenate([r[...] for r in hid_refs], axis=1),
        jnp.concatenate([r[...] for r in grad_refs], axis=0),
    )
    lead = lead_ref[0]
    for e in range(outer):
        block = store[pl.ds(pl.multiple_of(lax.rem(lead + e, outer) * rows, rows), rows), :]
        out_refs[e][...] = block.astype(out_refs[e].dtype)


def input_kernel(cores, core_ref, dv_ref, w_ref, *refs):
    out_refs, store = refs[:-1], refs[-1]
    rows = dv_ref.shape[0] // cores
    core = core_ref[0]
    store[...] = dot(dv_ref[...], w_ref[...], 1, 1)
    for d, out_ref in enumerate(out_refs):
        start = pl.multiple_of(lax.rem(core + d, cores) * rows, rows)
        out_ref[...] = store[pl.ds(start, rows), :].astype(out_ref.dtype)


def add_kernel(*refs):
    refs[-1][...] = low(sum(r[...].astype(F32) for r in refs[:-1]))


def sum_kernel(outer, *refs):
    out_ref = refs[-1]
    chunks = (len(refs) - 1) // outer
    width = refs[0].shape[1]
    for c in range(chunks):
        parts = refs[c * outer : (c + 1) * outer]
        out_ref[:, c * width : (c + 1) * width] = sum(r[...].astype(F32) for r in parts)


def grads_kernel(pack, share, q_ref, k_ref, v_ref, do_ref, bp_ref, dp_ref, rate_ref, inv_ref, dr_ref, y_ref, states,
                 dq_ref, dk_ref, db_ref, dd_ref, g_ref, b_ref, gt_ref, row_acc, col_acc, db_acc):
    size = states.shape[-1]
    head_columns(bp_ref, dp_ref, rate_ref, g_ref, b_ref, gt_ref)
    count = states.shape[0] * share
    n = q_ref.shape[0]
    rows, cols = iotas(n)
    lane = lax.broadcasted_iota(jnp.int32, (n, size), 1)
    row_acc[...] = jnp.zeros_like(row_acc)
    db_acc[...] = jnp.zeros_like(db_acc)
    for start in range(0, count, pack):
        places = range(start, start + pack)
        heads = [head_common(q_ref, k_ref, p, size, g_ref, b_ref, gt_ref) for p in places]
        for p, h in zip(places, heads):
            h.e16, h.s16 = states[p // share, 0, p % share], states[p // share, 1, p % share]
            h.do16 = do_ref[:, h.lanes]
            inner = v_ref[:, h.lanes].astype(F32) - h.gain * (h.rk * dot(h.k16, h.s16))
            h.right = low(h.beta * inner)
            h.dr = dr_ref[:, h.lanes].astype(F32) + dot(y_ref[:, h.lanes], h.e16, 1, 1)
            h.dr16 = low(h.dr)
        for p, h in zip(places, heads):
            h.written = dot(inv_ref[p], h.right)
            h.w16 = low(h.written)
            at_s = dot(jnp.concatenate([h.do16, h.dr16], axis=0), h.s16, 1, 1)
            h.d_qd, h.dr_s = at_s[:n], at_s[n:]
        for h in heads:
            pair = dot(jnp.concatenate([-h.dr16, h.do16], axis=0), h.w16, 1, 1)
            d_a, d_p = pair[:n], pair[n:]
            h.weights = d_a * h.a0 * h.tile(h.beta) + d_p * h.p
            x1 = low(jnp.where(rows > cols, d_a * h.gamma_rk, 0.0))
            x2 = low(d_p * h.gamma_rk)
            h.xs = jnp.concatenate([x1, x2], axis=0)
            h.d_kt = dot(h.w16, h.e16)
        for h in heads:
            row_side = dot(h.xs, h.k16)
            col_side = dot(
                h.xs, jnp.concatenate([low(h.beta * h.k_hat), low(h.q_hat)], axis=0), 0, 0
            )
            d_q = row_side[n:] + h.gain * h.d_qd
            in_term = h.beta * h.gain * h.dr_s
            d_k = h.rk * (h.beta * row_side[:n] - in_term + h.tail * h.d_kt) + col_side
            unit = h.q16.astype(F32) * h.rq
            d_q = h.rq * h.scale * (d_q - unit * jnp.sum(unit * d_q, axis=1, keepdims=True))
            d_k = d_k - h.k_hat * jnp.sum(h.k_hat * d_k, axis=1, keepdims=True)
            dq_ref[:, h.lanes] = low(d_q)
            dk_ref[:, h.lanes] = low(d_k)
            tail_term = h.d_kt * h.k_hat * h.tail
            direct = h.gain * h.d_qd * h.q_hat - in_term * h.k_hat - tail_term
            folded = sum(h.weights[:, i * size : (i + 1) * size] for i in range(n // size))
            row_sum = jnp.sum(folded + direct, axis=1, keepdims=True)
            end = jnp.sum(
                jnp.sum(tail_term, axis=0, keepdims=True)
                + jnp.sum(h.gain_end * (h.s16.astype(F32) * jnp.transpose(h.e16.astype(F32))), axis=0, keepdims=True),
                axis=1, keepdims=True,
            )
            last = lax.broadcasted_iota(jnp.int32, (1, n), 1) == n - 1
            col_acc[h.head : h.head + 1, :] = jnp.where(last, end, 0.0) - jnp.sum(
                h.weights, axis=0, keepdims=True
            )
            row_acc[...] = jnp.where(lane == h.head, row_sum, row_acc[...])
            d_beta = (1.0 - h.beta) * jnp.sum(h.dr * h.written, axis=1, keepdims=True)
            db_acc[...] = jnp.where(lane == h.head, d_beta, db_acc[...])
    d_sums = jnp.transpose(row_acc[...])[0:count] + col_acc[...]
    d_log = dot(d_sums, (rows >= cols).astype(F32), precision=HIGHEST)
    dd_ref[...] = -rate_column(rate_ref) * sigmoid(dp_ref[...]) * d_log
    db_ref[...] = jnp.transpose(db_acc[...])[0:count]


def call(body, args, outs, scratch=(), flops=0, anywhere=()):
    def place(i, a):
        space = pltpu.SMEM if a.ndim == 1 else pl.ANY if i in anywhere else pltpu.VMEM
        return pl.BlockSpec(memory_space=space)

    return pl.pallas_call(
        body,
        in_specs=[place(i, a) for i, a in enumerate(args)],
        out_specs=[pl.BlockSpec(memory_space=pltpu.VMEM) for _ in outs],
        out_shape=outs,
        scratch_shapes=list(scratch),
        compiler_params=pltpu.CompilerParams(vmem_limit_bytes=VMEM_LIMIT),
        cost_estimate=pl.CostEstimate(flops=flops, bytes_accessed=1 << 20, transcendentals=0),
    )(*args)


def shape(*dims, dtype=BF16):
    return jax.ShapeDtypeStruct(dims, dtype)


def total_kernel(maps, total_ref):
    group, _, share = maps.shape[:3]
    for i in range(share):
        g, o, t = maps[group - 1, 1, i], maps[0, 2, i], maps[0, 0, i]
        for j in range(1, group):
            b = group - 1 - j
            g = low(maps[b, 1, i].astype(F32) + dot(g, maps[b, 0, i]))
            o = low(maps[j, 2, i].astype(F32) + dot(maps[j, 0, i], o))
            t = low(dot(maps[j, 0, i], t))
        total_ref[0, i], total_ref[1, i], total_ref[2, i] = t, g, o


def join_kernel(level, last, lead_ref, own, other, out_ref, both):
    lead = lead_ref[0]
    bit = (lead >> level) & 1
    both[bit] = own[...]
    both[1 - bit] = other[...]
    for i in range(own.shape[1]):
        g = low(both[0, 1, i].astype(F32) + dot(both[1, 1, i], both[0, 0, i]))
        o = low(both[1, 2, i].astype(F32) + dot(both[1, 0, i], both[0, 2, i]))
        if last:
            out_ref[i] = jnp.where((lead >> (level + 1)) & 1 == 0, o, g)
        else:
            out_ref[0, i], out_ref[1, i], out_ref[2, i] = low(dot(both[1, 0, i], both[0, 0, i])), g, o


def spread_kernel(levels, lead_ref, maps, *refs):
    ranges, far, result = refs[: 2 * levels], refs[2 * levels], refs[2 * levels + 1]
    lead = lead_ref[0]
    group, _, share = maps.shape[:3]
    later = (lead >> levels) & 1
    zero = jnp.zeros(far.shape[1:], BF16)
    es = [jnp.where(later == 0, far[i], zero) for i in range(share)]
    ss = [jnp.where(later == 0, zero, far[i]) for i in range(share)]
    for level in range(levels - 1, -1, -1):
        other = ranges[2 * level + 1]
        bit = (lead >> level) & 1
        for i in range(share):
            e = low(other[1, i].astype(F32) + dot(es[i], other[0, i]))
            s = low(other[2, i].astype(F32) + dot(other[0, i], ss[i]))
            es[i], ss[i] = jnp.where(bit == 0, e, es[i]), jnp.where(bit == 0, ss[i], s)
    for j in range(group):
        b = group - 1 - j
        for i in range(share):
            result[b, 0, i], result[j, 1, i] = es[i], ss[i]
            if j < group - 1:
                es[i] = low(maps[b, 1, i].astype(F32) + dot(es[i], maps[b, 0, i]))
                ss[i] = low(maps[j, 2, i].astype(F32) + dot(maps[j, 0, i], ss[i]))


def group_size(count, heads):
    size = 1
    while size * size < count and count % (2 * size) == 0 and heads % (2 * size) == 0:
        size *= 2
    return size


def per_device(queries, keys, hidden, value_weight, beta_pre, decay_pre, decay_rate, out_grad):
    heads = decay_rate.shape[0]
    n, width = queries.shape
    dk = width // heads
    dv = value_weight.shape[1] // heads
    model = hidden.shape[1]
    spans = lax.axis_size("sp")
    group = group_size(spans, heads)
    outer = spans // group
    place = lax.axis_index("sp")
    pos = lax.rem(place, group)
    lead = lax.div(place, group)
    lead_arr = jnp.full((1,), lead, jnp.int32)
    share = heads // group
    beta_t, decay_t = beta_pre.T, decay_pre.T
    big = heads * n * n * 256
    teams = [list(range(s, s + group)) for s in range(0, spans, group)]

    def swap(x):
        return lax.all_to_all(x, "sp", 0, 0, axis_index_groups=teams)

    def near(x, d):
        return lax.ppermute(x, "sp", [(s, s ^ d) for s in range(spans)]) if d else x

    def across(x, reach):
        return lax.ppermute(x, "sp", [(s, s ^ (reach * group)) for s in range(spans)])

    rows = model // spans
    col_scratch = [
        pltpu.VMEM((n, 128), F32), pltpu.VMEM((n, 128), F32), pltpu.VMEM((heads, n), F32)
    ]
    maps, inv, dr, y, bdr, by, values, *hidden_t = call(
        functools.partial(local_kernel, PACK, share, outer),
        [jnp.full((1,), pos, jnp.int32), queries, keys, out_grad, hidden, value_weight, beta_t, decay_t, decay_rate],
        [shape(group, 3, share, dk, dv), shape(heads, n, n)]
        + [shape(n, width)] * 5
        + [shape(outer * rows, n)] * group,
        col_scratch
        + [pltpu.VMEM(hidden.shape, BF16), pltpu.VMEM((model, n), BF16), pltpu.VMEM(value_weight.shape, BF16), pltpu.SemaphoreType.DMA((2,))],
        big,
        (4, 5),
    )
    small = group * share * dk * dk * dk * 4
    triple, single = shape(3, share, dk, dv), shape(share, dk, dv)

    maps = swap(maps)
    (total,) = call(total_kernel, [maps], [triple], (), small)
    levels = outer.bit_length() - 2
    ranges = []
    for level in range(levels):
        other = across(total, 1 << level)
        ranges += [total, other]
        last = level == levels - 1
        (total,) = call(
            functools.partial(join_kernel, level, last), [lead_arr, total, other],
            [single if last else triple], [pltpu.VMEM((2,) + triple.shape, BF16)], small,
        )
    far = across(total, 1 << levels)
    moved = []
    for d, part in enumerate(hidden_t):
        moved.append(near(part, d))
    hidden_t = moved
    (states,) = call(
        functools.partial(spread_kernel, levels), [lead_arr, maps, *ranges, far],
        [shape(group, 2, share, dk, dv)], (), small,
    )
    states = swap(states)

    chunk = width // CHUNKS
    d_values, *grad_chunks = call(
        functools.partial(values_kernel, share, CHUNKS),
        [bdr, by, states],
        [shape(n, width)] + [shape(n, chunk)] * CHUNKS,
        (),
        heads * n * dk * dv * 2,
    )
    pieces = []
    for own in grad_chunks:
        parts = []
        for d in range(group):
            parts.append(near(own, d))
        blocks = call(
            functools.partial(weight_kernel, group, outer),
            [lead_arr, *hidden_t, *parts],
            [shape(rows, chunk, dtype=BF16 if e else F32) for e in range(outer)],
            [pltpu.VMEM((outer * rows, chunk), F32)],
            2 * group * n * outer * rows * chunk,
        )
        for e, block in enumerate(blocks):
            step = [(s, (s + e * group) % spans) for s in range(spans)]
            pieces.append(lax.ppermute(block, "sp", step) if e else block)
    (d_weight,) = call(functools.partial(sum_kernel, outer), pieces, [shape(rows, width, dtype=F32)], (), rows * width)

    core = lax.axis_index("tp")
    cores = lax.axis_size("tp")
    own_rows = n // cores
    shares = call(
        functools.partial(input_kernel, cores),
        [jnp.full((1,), core, jnp.int32), d_values, value_weight],
        [shape(own_rows, model, dtype=BF16 if d else F32) for d in range(cores)],
        [pltpu.VMEM((n, model), F32)], n * width * model * 2,
    )
    shares = [
        lax.ppermute(x, "tp", [(c, (c + d) % cores) for c in range(cores)]) if d else x
        for d, x in enumerate(shares)
    ]
    (d_hidden,) = call(add_kernel, shares, [shape(own_rows, model)], (), own_rows * model)

    d_queries, d_keys, d_beta, d_decay = call(
        functools.partial(grads_kernel, PACK, share),
        [queries, keys, values, out_grad, beta_t, decay_t, decay_rate, inv, dr, y, states],
        [shape(n, width), shape(n, width), shape(heads, n, dtype=F32), shape(heads, n, dtype=F32)],
        col_scratch + [pltpu.VMEM((n, dk), F32), pltpu.VMEM((heads, n), F32), pltpu.VMEM((n, dk), F32)],
        big,
    )
    return (d_queries, d_keys, d_beta.T, d_decay.T, d_hidden, d_weight)


def solution(mesh):
    return jax.shard_map(
        per_device,
        mesh=mesh,
        in_specs=(
            P("sp", "tp"),
            P("sp", "tp"),
            P("sp", None),
            P(None, "tp"),
            P("sp", "tp"),
            P("sp", "tp"),
            P("tp"),
            P("sp", "tp"),
        ),
        out_specs=(
            P("sp", "tp"),
            P("sp", "tp"),
            P("sp", "tp"),
            P("sp", "tp"),
            P(("sp", "tp"), None),
            P("sp", "tp"),
        ),
        check_vma=False,
    )
```

time: 132 us -> 125 us (0.947)
  blocking collectives: 0 us -> 17.3 us
  matrix products: 13.1 us -> 0 us
  starting transfers between devices: 44.3 us -> 33.3 us
  Pallas kernels: 40.6 us -> 49.2 us
  waiting for transfers between devices: 23.6 us -> 18.8 us
  local copies, waits for them, and re-layouts: 7.55 us -> 5.06 us
    all_to_all x0 -> x1, blocking collectives: none -> 17.3 us  [swap(): return lax.all_to_all(x, 'sp', 0, 0, axis_index_groups=teams)]
    dot_general x11 -> x0, matrix products: 13.1 us -> none  [the longest x2 6.08 us: input_grad(): lax.dot_general(piece, value_weight, (((1,), (1,)), ((), ())), preferred_...]
    ppermute x21 -> x9, starting transfers between devices: 25.6 us -> 12.5 us  [near(): return lax.ppermute(x, 'sp', [(s, s ^ d) for s in range(spans)]) if d else x]
    pallas_call x8 -> x11, Pallas kernels: 40.6 us -> 49.2 us  [call(): pl.pallas_call(body, in_specs=[place(i, a) for i, a in enumerate(args)],...]
    ppermute x13 -> x9, waiting for transfers between devices: 14.6 us -> 6.74 us  [the longest x2 6.72 us: across(): return lax.ppermute(x, 'sp', [(s, s ^ reach * group) for s in range(spans)])]
    all_to_all x0 -> x1, waiting for transfers between devices: none -> 5.6 us  [swap(): return lax.all_to_all(x, 'sp', 0, 0, axis_index_groups=teams)]
    all_to_all x0 -> x1, starting transfers between devices: none -> 3.65 us  [swap(): return lax.all_to_all(x, 'sp', 0, 0, axis_index_groups=teams)]
    slice x3 -> x0, local copies, waits for them, and re-layouts: 2.75 us -> none  [the longest x2 1.69 us: states(): total[1:]]
  transfers between devices with their start and end apart: 34 -> 19, of which waited for: 9 -> 5; matrix products, arithmetic and copies ran while one was open for 12% -> 0% of each run, Pallas kernels for 19% -> 21%
where the time goes in v3:
time: 125 us; the launch traced here: 124 us
  Pallas kernels  49.2 us (39%)
  starting transfers between devices  33.3 us (27%)
  waiting for transfers between devices  18.8 us (15%)
  blocking collectives  17.3 us (14%)
  local copies, waits for them, and re-layouts  5.06 us (4%)
    pallas_call x11, Pallas kernels, call(): pl.pallas_call(body, in_specs=[place(i, a) for i, a in enumerate(args)],...  49.2 us
    all_to_all x1, blocking collectives, swap(): return lax.all_to_all(x, 'sp', 0, 0, axis_index_groups=teams)  17.3 us
    ppermute x9, starting transfers between devices, near(): return lax.ppermute(x, 'sp', [(s, s ^ d) for s in range(spans)]) if d else x  12.5 us
    ppermute x6, starting transfers between devices, per_device(): pieces.append(lax.ppermute(block, 'sp', step) if e else block)  12.5 us
    ppermute x2, waiting for transfers between devices, across(): return lax.ppermute(x, 'sp', [(s, s ^ reach * group) for s in range(spans)])  6.72 us
    ppermute x9, waiting for transfers between devices, near(): return lax.ppermute(x, 'sp', [(s, s ^ d) for s in range(spans)]) if d else x  6.43 us
    all_to_all x1, waiting for transfers between devices, swap(): return lax.all_to_all(x, 'sp', 0, 0, axis_index_groups=teams)  5.6 us
    unnamed x46, local copies, waits for them, and re-layouts  5.06 us
  transfers between devices with their start and end apart: 19, of which 5 were waited for; matrix products, arithmetic and copies ran while one was open for 0% of the time, Pallas kernels for 21%

profile of v3, /device:TPU:0, one launch (start us, length us, event | category | flops | bytes accessed | tf_op | source)
XLA Modules:
  0.0 124.4 jit_solution(12316333659110090877)
XLA Ops:
  0.6 13.7 %shard_map.127 = (bf16[4,3,2,128,128]{4,3,2,1,0:T(8,128)(2,1)}, bf16[8,256,256]{2,1,0:T(8,128)(2,1)}, bf16[256,1024]{1,0:T(8,128)(2,1)}, bf16[256,1024]{1,0:T(8,...) custom-call(s32[1]{0:T(128)} %bitcast.pos_ref, ...), custom_call_target="tpu_custom_call" | custom-call | flops 134217728 | bytes 1048576 | tf_op jit(solution)/shard_map/pallas_call | solution.py:313
  14.3 17.3 %all_to_all.10.maps = bf16[4,3,2,128,128]{4,3,2,1,0:T(8,128)(2,1)} all-to-all(bf16[4,3,2,128,128]{4,3,2,1,0:T(8,128)(2,1)} %get-tuple-element.38), channel_id=1, replica_groups={{0,2,4,6},{8,10,12,14},{16,18,20,22},{24,26,28,30},{1,3,5,7},{9,11,13,1..., dimensions={0} | all-to-all | bytes 1572864 | tf_op jit(solution)/shard_map/all_to_all | solution.py:404
  31.6 2.5 %shard_map.128.own.refs_0_ = bf16[3,2,128,128]{3,2,1,0:T(8,128)(2,1)} custom-call(bf16[4,3,2,128,128]{4,3,2,1,0:T(8,128)(2,1)} %all_to_all.10.maps), custom_call_target="tpu_custom_call" | custom-call | flops 67108864 | bytes 1048576 | tf_op jit(solution)/shard_map/pallas_call | solution.py:313
  34.2 1.8 %collective-permute-start = (bf16[3,2,128,128]{3,2,1,0:T(8,128)(2,1)}, bf16[3,2,128,128]{3,2,1,0:T(8,128)(2,1)S(1)}, u32[]{:S(2)}, u32[]{:S(2)}) collective-permute-start(bf16[3,2,128,128]{3,2,1,0:T(8,128)(2,1)} %shard_map.128.own.refs_0_), channel_id=1, source_target_pairs={{0,8},{2,10},{4,12},{6,14},{8,0},{10,2},{12,4},{14,6},{16,24},{18,... | collective-permute-start | bytes 589832 | tf_op jit(solution)/shard_map/ppermute | solution.py:410
  35.9 4.1 %collective-permute-done.other.refs_1_ = bf16[3,2,128,128]{3,2,1,0:T(8,128)(2,1)S(1)} collective-permute-done((bf16[3,2,128,128]{3,2,1,0:T(8,128)(2,1)}, bf16[3,2,128,128]{3,2,1,0:T(8,128)(2,1)S(1)}, u32[]{:S(2)}, u32[]{:S(2)}) %collective-permute-start) | collective-permute-done | bytes 196640 | tf_op jit(solution)/shard_map/ppermute | solution.py:410
  40.8 1.9 %shard_map.129 = bf16[2,128,128]{2,1,0:T(8,128)(2,1)} custom-call(s32[1]{0:T(128)} %bitcast.3.lead_ref, bf16[3,2,128,128]{3,2,1,0:T(8,128)(2,1)} %shard_map.128.own.refs_0_, bf16[3,2,128,128]{3,2,1,0:T(8,128)(2,1)} %copy-done.4), custom_call_target="tpu_custom_call" | custom-call | flops 67108864 | bytes 1048576 | tf_op jit(solution)/shard_map/pallas_call | solution.py:313
  42.7 2.8 %collective-permute-start.1 = (bf16[2,128,128]{2,1,0:T(8,128)(2,1)}, bf16[2,128,128]{2,1,0:T(8,128)(2,1)S(1)}, u32[]{:S(2)}, u32[]{:S(2)}) collective-permute-start(bf16[2,128,128]{2,1,0:T(8,128)(2,1)} %shard_map.129), channel_id=1, source_target_pairs={{0,16},{2,18},{4,20},{6,22},{8,24},{10,26},{12,28},{14,30},{16,0},... | collective-permute-start | bytes 196616 | tf_op jit(solution)/shard_map/ppermute | solution.py:410
  45.5 2.6 %collective-permute-done.1.refs_2_ = bf16[2,128,128]{2,1,0:T(8,128)(2,1)S(1)} collective-permute-done((bf16[2,128,128]{2,1,0:T(8,128)(2,1)}, bf16[2,128,128]{2,1,0:T(8,128)(2,1)S(1)}, u32[]{:S(2)}, u32[]{:S(2)}) %collective-permute-start.1) | collective-permute-done | bytes 65568 | tf_op jit(solution)/shard_map/ppermute | solution.py:410
  48.7 2.7 %shard_map.130 = bf16[4,2,2,128,128]{4,3,2,1,0:T(8,128)(2,1)} custom-call(s32[1]{0:T(128)} %bitcast.3.lead_ref, bf16[4,3,2,128,128]{4,3,2,1,0:T(8,128)(2,1)} %all_to_all.10.maps, bf16[3,2,128,128]{3,2,1,0:T(8,128)(2,1)} %shard_map.128.own.refs_0_, bf16[3,2,128,128]{3,2,1,0:T(8,128)(2,1)} %copy-done.4, bf16[2,128,128]{2,1,0:T(8,128)(2,1)} %copy-done.19), custom_call_target="tpu_custom_call" | custom-call | flops 67108864 | bytes 1048576 | tf_op jit(solution)/shard_map/pallas_call | solution.py:313
  51.4 3.6 %all-to-all-start.1 = ((bf16[4,2,2,128,128]{4,3,2,1,0:T(8,128)(2,1)}), bf16[4,2,2,128,128]{4,3,2,1,0:T(8,128)(2,1)S(1)}, u32[]{:S(2)}, u32[]{:S(2)}) async-start(bf16[4,2,2,128,128]{4,3,2,1,0:T(8,128)(2,1)} %shard_map.130), calls=%async_computation.1 | async-start | bytes 1048576 | tf_op jit(solution)/shard_map/all_to_all | solution.py:404
  55.0 1.8 %collective-permute-start.3 = (bf16[512,256]{1,0:T(8,128)(2,1)S(1)}, bf16[512,256]{1,0:T(8,128)(2,1)S(1)}, u32[]{:S(2)}, u32[]{:S(2)}) collective-permute-start(bf16[512,256]{1,0:T(8,128)(2,1)S(1)} %copy-done.22), channel_id=1, source_target_pairs={{0,2},{2,0},{4,6},{6,4},{8,10},{10,8},{12,14},{14,12},{16,18},{18,... | collective-permute-start | bytes 786440 | tf_op jit(solution)/shard_map/ppermute | solution.py:407
  56.8 1.5 %collective-permute-start.4 = (bf16[512,256]{1,0:T(8,128)(2,1)S(1)}, bf16[512,256]{1,0:T(8,128)(2,1)S(1)}, u32[]{:S(2)}, u32[]{:S(2)}) collective-permute-start(bf16[512,256]{1,0:T(8,128)(2,1)S(1)} %copy-done.21), channel_id=1, source_target_pairs={{0,4},{2,6},{4,0},{6,2},{8,12},{10,14},{12,8},{14,10},{16,20},{18,... | collective-permute-start | bytes 786440 | tf_op jit(solution)/shard_map/ppermute | solution.py:407
  58.6 5.6 %all-to-all-done.1.states = bf16[4,2,2,128,128]{4,3,2,1,0:T(8,128)(2,1)S(1)} async-done(((bf16[4,2,2,128,128]{4,3,2,1,0:T(8,128)(2,1)}), bf16[4,2,2,128,128]{4,3,2,1,0:T(8,128)(2,1)S(1)}, u32[]{:S(2)}, u32[]{:S(2)}) %all-to-all-start.1) | async-done | bytes 524320 | tf_op jit(solution)/shard_map/all_to_all | solution.py:404
  64.2 0.8 copy-done
  65.0 2.6 %shard_map.132 = (bf16[256,1024]{1,0:T(8,128)(2,1)}, bf16[256,512]{1,0:T(8,128)(2,1)}, bf16[256,512]{1,0:T(8,128)(2,1)}) custom-call(bf16[256,1024]{1,0:T(8,128)(2,1)} %get-tuple-element.43.bdr_ref, bf16[256,1024]{1,0:T(8,128)(2,1)} %get-tuple-element.44.by_ref, bf16[4,2,2,128,128]{4,3,2,1,0:T(8,128)(2,1)} %copy-done), custom_call_target="tpu_custom_call" | custom-call | flops 67108864 | bytes 1048576 | tf_op jit(solution)/shard_map/pallas_call | solution.py:313
  67.6 1.2 collective-permute-start.14
  68.8 1.8 %collective-permute-start.13 = (bf16[256,512]{1,0:T(8,128)(2,1)}, bf16[256,512]{1,0:T(8,128)(2,1)S(1)}, u32[]{:S(2)}, u32[]{:S(2)}) collective-permute-start(bf16[256,512]{1,0:T(8,128)(2,1)} %get-tuple-element.57.refs_4_), channel_id=1, source_target_pairs={{0,4},{2,6},{4,0},{6,2},{8,12},{10,14},{12,8},{14,10},{16,20},{18,... | collective-permute-start | bytes 786440 | tf_op jit(solution)/shard_map/ppermute | solution.py:407
  71.1 5.8 %collective-permute-done.4.refs_2_ = bf16[512,256]{1,0:T(8,128)(2,1)S(1)} collective-permute-done((bf16[512,256]{1,0:T(8,128)(2,1)S(1)}, bf16[512,256]{1,0:T(8,128)(2,1)S(1)}, u32[]{:S(2)}, u32[]{:S(2)}) %collective-permute-start.4) | collective-permute-done | bytes 262176 | tf_op jit(solution)/shard_map/ppermute | solution.py:407
  76.9 3.2 %collective-permute-start.8 = (bf16[256,512]{1,0:T(8,128)(2,1)}, bf16[256,512]{1,0:T(8,128)(2,1)S(1)}, u32[]{:S(2)}, u32[]{:S(2)}) collective-permute-start(bf16[256,512]{1,0:T(8,128)(2,1)} %get-tuple-element.52.refs_4_), channel_id=1, source_target_pairs={{0,6},{2,4},{4,2},{6,0},{8,14},{10,12},{12,10},{14,8},{16,22},{18,... | collective-permute-start | bytes 786440 | tf_op jit(solution)/shard_map/ppermute | solution.py:407
  80.1 5.1 %shard_map.133 = (f32[128,2048]{1,0:T(8,128)}, bf16[128,2048]{1,0:T(8,128)(2,1)}) custom-call(s32[1]{0:T(128)} %bitcast.6.core_ref, bf16[256,1024]{1,0:T(8,128)(2,1)} %get-tuple-element.45.dv_ref, bf16[2048,1024]{1,0:T(8,128)(2,1)} %w_ref.3), custom_call_target="tpu_custom_call" | custom-call | flops 1073741824 | bytes 1048576 | tf_op jit(solution)/shard_map/pallas_call | solution.py:313
  85.2 1.1 collective-permute-start.7
  86.3 1.2 collective-permute-start.6
  88.3 3.1 %shard_map.136 = (f32[128,512]{1,0:T(8,128)}, bf16[128,512]{1,0:T(8,128)(2,1)}, bf16[128,512]{1,0:T(8,128)(2,1)}, bf16[128,512]{1,0:T(8,128)(2,1)}) custom-call(s32[1]{0:T(128)} %bitcast.3.lead_ref, bf16[512,256]{1,0:T(8,128)(2,1)} %get-tuple-element.48.refs_0_, bf16[512,256]{1,0:T(8,128)(2,1)} %copy-done.1, bf16[512,256]{1,0:T(8,128)(2,1)} %copy-done.2, ...), custom_call_target="tpu_custom_call" | custom-call | flops 536870912 | bytes 1048576 | tf_op jit(solution)/shard_map/pallas_call | solution.py:313
  91.9 3.0 %collective-permute-start.16 = (bf16[128,512]{1,0:T(8,128)(2,1)}, bf16[128,512]{1,0:T(8,128)(2,1)S(1)}, u32[]{:S(2)}, u32[]{:S(2)}) collective-permute-start(bf16[128,512]{1,0:T(8,128)(2,1)} %get-tuple-element.60), channel_id=1, source_target_pairs={{0,16},{2,18},{4,20},{6,22},{8,24},{10,26},{12,28},{14,30},{16,0},... | collective-permute-start | bytes 393224 | tf_op jit(solution)/shard_map/ppermute | solution.py:475
  95.5 2.9 %collective-permute-start.17 = (bf16[128,512]{1,0:T(8,128)(2,1)}, bf16[128,512]{1,0:T(8,128)(2,1)S(1)}, u32[]{:S(2)}, u32[]{:S(2)}) collective-permute-start(bf16[128,512]{1,0:T(8,128)(2,1)} %get-tuple-element.61), channel_id=1, source_target_pairs={{0,24},{2,26},{4,28},{6,30},{8,0},{10,2},{12,4},{14,6},{16,8},{18,... | collective-permute-start | bytes 393224 | tf_op jit(solution)/shard_map/ppermute | solution.py:475
  99.2 3.1 %shard_map.135 = (f32[128,512]{1,0:T(8,128)}, bf16[128,512]{1,0:T(8,128)(2,1)}, bf16[128,512]{1,0:T(8,128)(2,1)}, bf16[128,512]{1,0:T(8,128)(2,1)}) custom-call(s32[1]{0:T(128)} %bitcast.3.lead_ref, bf16[512,256]{1,0:T(8,128)(2,1)} %get-tuple-element.48.refs_0_, bf16[512,256]{1,0:T(8,128)(2,1)} %copy-done.1, bf16[512,256]{1,0:T(8,128)(2,1)} %copy-done.2, ...), custom_call_target="tpu_custom_call" | custom-call | flops 536870912 | bytes 1048576 | tf_op jit(solution)/shard_map/pallas_call | solution.py:313
  102.3 1.3 %collective-permute-start.10 = (bf16[128,512]{1,0:T(8,128)(2,1)}, bf16[128,512]{1,0:T(8,128)(2,1)S(1)}, u32[]{:S(2)}, u32[]{:S(2)}) collective-permute-start(bf16[128,512]{1,0:T(8,128)(2,1)} %get-tuple-element.55), channel_id=1, source_target_pairs={{0,16},{2,18},{4,20},{6,22},{8,24},{10,26},{12,28},{14,30},{16,0},... | collective-permute-start | bytes 393224 | tf_op jit(solution)/shard_map/ppermute | solution.py:475
  103.6 4.8 %collective-permute-start.11 = (bf16[128,512]{1,0:T(8,128)(2,1)}, bf16[128,512]{1,0:T(8,128)(2,1)S(1)}, u32[]{:S(2)}, u32[]{:S(2)}) collective-permute-start(bf16[128,512]{1,0:T(8,128)(2,1)} %get-tuple-element.56), channel_id=1, source_target_pairs={{0,24},{2,26},{4,28},{6,30},{8,0},{10,2},{12,4},{14,6},{16,8},{18,... | collective-permute-start | bytes 393224 | tf_op jit(solution)/shard_map/ppermute | solution.py:475
  108.4 9.9 %shard_map.131 = (bf16[256,1024]{1,0:T(8,128)(2,1)}, bf16[256,1024]{1,0:T(8,128)(2,1)}, f32[8,256]{1,0:T(8,128)}, f32[8,256]{1,0:T(8,128)}) custom-call(bf16[256,1024]{1,0:T(8,128)(2,1)} %q_ref.3, bf16[256,1024]{1,0:T(8,128)(2,1)} %k_ref.3, bf16[256,1024]{1,0:T(8,128)(2,1)} %get-tuple-element.34.v_ref, bf16[256,1024]{1,0:T(8,128)(2,1)} %do_ref.3, ...), custom_call_target="tpu_custom_call" | custom-call | flops 134217728 | bytes 1048576 | tf_op jit(solution)/shard_map/pallas_call | solution.py:313
  119.1 2.2 %shard_map.137 = f32[128,1024]{1,0:T(8,128)} custom-call(f32[128,512]{1,0:T(8,128)} %get-tuple-element.53.refs_0_, bf16[128,512]{1,0:T(8,128)(2,1)} %copy-done.16, bf16[128,512]{1,0:T(8,128)(2,1)} %copy-done.17, bf16[128,512]{1,0:T(8,128)(2,1)} %copy-done.18, f32[128,512]{1,0:T(8,128)} %get-tuple-element.58.refs_4_, bf16[128,512]{1,0:T(8,128)(2,1)} %copy-done.13, ...), custom_call_target="tpu_custom_call" | custom-call | flops 131072 | bytes 1048576 | tf_op jit(solution)/shard_map/pallas_call | solution.py:313
  121.4 0.8 copy-done.5
  122.2 2.2 %shard_map.134 = bf16[128,2048]{1,0:T(8,128)(2,1)} custom-call(f32[128,2048]{1,0:T(8,128)} %get-tuple-element.46.refs_0_, bf16[128,2048]{1,0:T(8,128)(2,1)} %copy-done.5), custom_call_target="tpu_custom_call" | custom-call | flops 262144 | bytes 1048576 | tf_op jit(solution)/shard_map/pallas_call | solution.py:313
  (64 shorter events, 5.4 us)
Async XLA Ops:
  14.3 40.7 %copy-start.22 = (bf16[512,256]{1,0:T(8,128)(2,1)S(1)}, bf16[512,256]{1,0:T(8,128)(2,1)}, u32[]{:S(2)}) copy-start(bf16[512,256]{1,0:T(8,128)(2,1)} %get-tuple-element.49) | copy-start | bytes 786436
  14.3 42.5 %copy-start.21 = (bf16[512,256]{1,0:T(8,128)(2,1)S(1)}, bf16[512,256]{1,0:T(8,128)(2,1)}, u32[]{:S(2)}) copy-start(bf16[512,256]{1,0:T(8,128)(2,1)} %get-tuple-element.50) | copy-start | bytes 786436
  14.3 44.0 %copy-start.20 = (bf16[512,256]{1,0:T(8,128)(2,1)S(1)}, bf16[512,256]{1,0:T(8,128)(2,1)}, u32[]{:S(2)}) copy-start(bf16[512,256]{1,0:T(8,128)(2,1)} %get-tuple-element.51) | copy-start | bytes 786436
  34.2 5.9 %collective-permute-start = (bf16[3,2,128,128]{3,2,1,0:T(8,128)(2,1)}, bf16[3,2,128,128]{3,2,1,0:T(8,128)(2,1)S(1)}, u32[]{:S(2)}, u32[]{:S(2)}) collective-permute-start(bf16[3,2,128,128]{3,2,1,0:T(8,128)(2,1)} %shard_map.128.own.refs_0_), channel_id=1, source_target_pairs={{0,8},{2,10},{4,12},{6,14},{8,0},{10,2},{12,4},{14,6},{16,24},{18,... | collective-permute-start | bytes 589832 | tf_op jit(solution)/shard_map/ppermute | solution.py:410
  42.7 5.4 %collective-permute-start.1 = (bf16[2,128,128]{2,1,0:T(8,128)(2,1)}, bf16[2,128,128]{2,1,0:T(8,128)(2,1)S(1)}, u32[]{:S(2)}, u32[]{:S(2)}) collective-permute-start(bf16[2,128,128]{2,1,0:T(8,128)(2,1)} %shard_map.129), channel_id=1, source_target_pairs={{0,16},{2,18},{4,20},{6,22},{8,24},{10,26},{12,28},{14,30},{16,0},... | collective-permute-start | bytes 196616 | tf_op jit(solution)/shard_map/ppermute | solution.py:410
  51.4 12.8 %all-to-all-start.1 = ((bf16[4,2,2,128,128]{4,3,2,1,0:T(8,128)(2,1)}), bf16[4,2,2,128,128]{4,3,2,1,0:T(8,128)(2,1)S(1)}, u32[]{:S(2)}, u32[]{:S(2)}) async-start(bf16[4,2,2,128,128]{4,3,2,1,0:T(8,128)(2,1)} %shard_map.130), calls=%async_computation.1 | async-start | bytes 1048576 | tf_op jit(solution)/shard_map/all_to_all | solution.py:404
  55.0 15.6 %collective-permute-start.3 = (bf16[512,256]{1,0:T(8,128)(2,1)S(1)}, bf16[512,256]{1,0:T(8,128)(2,1)S(1)}, u32[]{:S(2)}, u32[]{:S(2)}) collective-permute-start(bf16[512,256]{1,0:T(8,128)(2,1)S(1)} %copy-done.22), channel_id=1, source_target_pairs={{0,2},{2,0},{4,6},{6,4},{8,10},{10,8},{12,14},{14,12},{16,18},{18,... | collective-permute-start | bytes 786440 | tf_op jit(solution)/shard_map/ppermute | solution.py:407
  56.8 20.1 %collective-permute-start.4 = (bf16[512,256]{1,0:T(8,128)(2,1)S(1)}, bf16[512,256]{1,0:T(8,128)(2,1)S(1)}, u32[]{:S(2)}, u32[]{:S(2)}) collective-permute-start(bf16[512,256]{1,0:T(8,128)(2,1)S(1)} %copy-done.21), channel_id=1, source_target_pairs={{0,4},{2,6},{4,0},{6,2},{8,12},{10,14},{12,8},{14,10},{16,20},{18,... | collective-permute-start | bytes 786440 | tf_op jit(solution)/shard_map/ppermute | solution.py:407
  58.3 26.9 %collective-permute-start.5 = (bf16[512,256]{1,0:T(8,128)(2,1)S(1)}, bf16[512,256]{1,0:T(8,128)(2,1)S(1)}, u32[]{:S(2)}, u32[]{:S(2)}) collective-permute-start(bf16[512,256]{1,0:T(8,128)(2,1)S(1)} %copy-done.20), channel_id=1, source_target_pairs={{0,6},{2,4},{4,2},{6,0},{8,14},{10,12},{12,10},{14,8},{16,22},{18,... | collective-permute-start | bytes 786440 | tf_op jit(solution)/shard_map/ppermute | solution.py:407
  67.6 17.6 %copy-start.6 = (bf16[256,512]{1,0:T(8,128)(2,1)S(1)}, bf16[256,512]{1,0:T(8,128)(2,1)}, u32[]{:S(2)}) copy-start(bf16[256,512]{1,0:T(8,128)(2,1)} %get-tuple-element.52.refs_4_) | copy-start | bytes 786436
  67.6 17.6 %collective-permute-start.14 = (bf16[256,512]{1,0:T(8,128)(2,1)}, bf16[256,512]{1,0:T(8,128)(2,1)S(1)}, u32[]{:S(2)}, u32[]{:S(2)}) collective-permute-start(bf16[256,512]{1,0:T(8,128)(2,1)} %get-tuple-element.57.refs_4_), channel_id=1, source_target_pairs={{0,6},{2,4},{4,2},{6,0},{8,14},{10,12},{12,10},{14,8},{16,22},{18,... | collective-permute-start | bytes 786440 | tf_op jit(solution)/shard_map/ppermute | solution.py:407
  68.8 17.6 %collective-permute-start.13 = (bf16[256,512]{1,0:T(8,128)(2,1)}, bf16[256,512]{1,0:T(8,128)(2,1)S(1)}, u32[]{:S(2)}, u32[]{:S(2)}) collective-permute-start(bf16[256,512]{1,0:T(8,128)(2,1)} %get-tuple-element.57.refs_4_), channel_id=1, source_target_pairs={{0,4},{2,6},{4,0},{6,2},{8,12},{10,14},{12,8},{14,10},{16,20},{18,... | collective-permute-start | bytes 786440 | tf_op jit(solution)/shard_map/ppermute | solution.py:407
  70.6 16.9 %copy-start.1 = (bf16[512,256]{1,0:T(8,128)(2,1)}, bf16[512,256]{1,0:T(8,128)(2,1)S(1)}, u32[]{:S(2)}) copy-start(bf16[512,256]{1,0:T(8,128)(2,1)S(1)} %collective-permute-done.3.refs_1_) | copy-start | bytes 786436
  70.6 16.9 %collective-permute-start.12 = (bf16[256,512]{1,0:T(8,128)(2,1)}, bf16[256,512]{1,0:T(8,128)(2,1)S(1)}, u32[]{:S(2)}, u32[]{:S(2)}) collective-permute-start(bf16[256,512]{1,0:T(8,128)(2,1)} %get-tuple-element.57.refs_4_), channel_id=1, source_target_pairs={{0,2},{2,0},{4,6},{6,4},{8,10},{10,8},{12,14},{14,12},{16,18},{18,... | collective-permute-start | bytes 786440 | tf_op jit(solution)/shard_map/ppermute | solution.py:407
  76.9 10.7 %copy-start.2 = (bf16[512,256]{1,0:T(8,128)(2,1)}, bf16[512,256]{1,0:T(8,128)(2,1)S(1)}, u32[]{:S(2)}) copy-start(bf16[512,256]{1,0:T(8,128)(2,1)S(1)} %collective-permute-done.4.refs_2_) | copy-start | bytes 786436
  76.9 15.0 %collective-permute-start.8 = (bf16[256,512]{1,0:T(8,128)(2,1)}, bf16[256,512]{1,0:T(8,128)(2,1)S(1)}, u32[]{:S(2)}, u32[]{:S(2)}) collective-permute-start(bf16[256,512]{1,0:T(8,128)(2,1)} %get-tuple-element.52.refs_4_), channel_id=1, source_target_pairs={{0,6},{2,4},{4,2},{6,0},{8,14},{10,12},{12,10},{14,8},{16,22},{18,... | collective-permute-start | bytes 786440 | tf_op jit(solution)/shard_map/ppermute | solution.py:407
  85.2 2.4 %copy-start.3 = (bf16[512,256]{1,0:T(8,128)(2,1)}, bf16[512,256]{1,0:T(8,128)(2,1)S(1)}, u32[]{:S(2)}) copy-start(bf16[512,256]{1,0:T(8,128)(2,1)S(1)} %collective-permute-done.5.refs_3_) | copy-start | bytes 786436
  85.2 36.2 %collective-permute-start.2 = (bf16[128,2048]{1,0:T(8,128)(2,1)}, bf16[128,2048]{1,0:T(8,128)(2,1)S(1)}, u32[]{:S(2)}, u32[]{:S(2)}) collective-permute-start(bf16[128,2048]{1,0:T(8,128)(2,1)} %get-tuple-element.47), channel_id=1, source_target_pairs={{0,1},{1,0},{2,3},{3,2},{4,5},{5,4},{6,7},{7,6},{8,9},{9,8},{10,11... | collective-permute-start | bytes 1572872 | tf_op jit(solution)/shard_map/ppermute | solution.py:488
  85.2 2.4 %copy-start.8 = (bf16[256,512]{1,0:T(8,128)(2,1)}, bf16[256,512]{1,0:T(8,128)(2,1)S(1)}, u32[]{:S(2)}) copy-start(bf16[256,512]{1,0:T(8,128)(2,1)S(1)} %collective-permute-done.14.refs_7_) | copy-start | bytes 786436
  85.2 10.3 %collective-permute-start.7 = (bf16[256,512]{1,0:T(8,128)(2,1)S(1)}, bf16[256,512]{1,0:T(8,128)(2,1)S(1)}, u32[]{:S(2)}, u32[]{:S(2)}) collective-permute-start(bf16[256,512]{1,0:T(8,128)(2,1)S(1)} %copy-done.6), channel_id=1, source_target_pairs={{0,4},{2,6},{4,0},{6,2},{8,12},{10,14},{12,8},{14,10},{16,20},{18,... | collective-permute-start | bytes 786440 | tf_op jit(solution)/shard_map/ppermute | solution.py:407
  86.3 1.2 %copy-start.9 = (bf16[256,512]{1,0:T(8,128)(2,1)}, bf16[256,512]{1,0:T(8,128)(2,1)S(1)}, u32[]{:S(2)}) copy-start(bf16[256,512]{1,0:T(8,128)(2,1)S(1)} %collective-permute-done.13.refs_6_) | copy-start | bytes 786436
  86.3 12.1 %collective-permute-start.6 = (bf16[256,512]{1,0:T(8,128)(2,1)S(1)}, bf16[256,512]{1,0:T(8,128)(2,1)S(1)}, u32[]{:S(2)}, u32[]{:S(2)}) collective-permute-start(bf16[256,512]{1,0:T(8,128)(2,1)S(1)} %copy-done.6), channel_id=1, source_target_pairs={{0,2},{2,0},{4,6},{6,4},{8,10},{10,8},{12,14},{14,12},{16,18},{18,... | collective-permute-start | bytes 786440 | tf_op jit(solution)/shard_map/ppermute | solution.py:407
  91.4 10.9 %collective-permute-start.15 = (bf16[128,512]{1,0:T(8,128)(2,1)}, bf16[128,512]{1,0:T(8,128)(2,1)S(1)}, u32[]{:S(2)}, u32[]{:S(2)}) collective-permute-start(bf16[128,512]{1,0:T(8,128)(2,1)} %get-tuple-element.59), channel_id=1, source_target_pairs={{0,8},{2,10},{4,12},{6,14},{8,16},{10,18},{12,20},{14,22},{16,24},... | collective-permute-start | bytes 393224 | tf_op jit(solution)/shard_map/ppermute | solution.py:475
  91.9 6.5 %copy-start.7 = (bf16[256,512]{1,0:T(8,128)(2,1)}, bf16[256,512]{1,0:T(8,128)(2,1)S(1)}, u32[]{:S(2)}) copy-start(bf16[256,512]{1,0:T(8,128)(2,1)S(1)} %collective-permute-done.8.refs_7_) | copy-start | bytes 786436
  91.9 11.7 %collective-permute-start.16 = (bf16[128,512]{1,0:T(8,128)(2,1)}, bf16[128,512]{1,0:T(8,128)(2,1)S(1)}, u32[]{:S(2)}, u32[]{:S(2)}) collective-permute-start(bf16[128,512]{1,0:T(8,128)(2,1)} %get-tuple-element.60), channel_id=1, source_target_pairs={{0,16},{2,18},{4,20},{6,22},{8,24},{10,26},{12,28},{14,30},{16,0},... | collective-permute-start | bytes 393224 | tf_op jit(solution)/shard_map/ppermute | solution.py:475
  95.5 2.9 %copy-start.10 = (bf16[256,512]{1,0:T(8,128)(2,1)}, bf16[256,512]{1,0:T(8,128)(2,1)S(1)}, u32[]{:S(2)}) copy-start(bf16[256,512]{1,0:T(8,128)(2,1)S(1)} %collective-permute-done.7.refs_6_) | copy-start | bytes 786436
  95.5 22.9 %collective-permute-start.17 = (bf16[128,512]{1,0:T(8,128)(2,1)}, bf16[128,512]{1,0:T(8,128)(2,1)S(1)}, u32[]{:S(2)}, u32[]{:S(2)}) collective-permute-start(bf16[128,512]{1,0:T(8,128)(2,1)} %get-tuple-element.61), channel_id=1, source_target_pairs={{0,24},{2,26},{4,28},{6,30},{8,0},{10,2},{12,4},{14,6},{16,8},{18,... | collective-permute-start | bytes 393224 | tf_op jit(solution)/shard_map/ppermute | solution.py:475
  102.3 16.1 %collective-permute-start.9 = (bf16[128,512]{1,0:T(8,128)(2,1)}, bf16[128,512]{1,0:T(8,128)(2,1)S(1)}, u32[]{:S(2)}, u32[]{:S(2)}) collective-permute-start(bf16[128,512]{1,0:T(8,128)(2,1)} %get-tuple-element.54), channel_id=1, source_target_pairs={{0,8},{2,10},{4,12},{6,14},{8,16},{10,18},{12,20},{14,22},{16,24},... | collective-permute-start | bytes 393224 | tf_op jit(solution)/shard_map/ppermute | solution.py:475
  102.3 16.1 %copy-start.13 = (bf16[128,512]{1,0:T(8,128)(2,1)}, bf16[128,512]{1,0:T(8,128)(2,1)S(1)}, u32[]{:S(2)}) copy-start(bf16[128,512]{1,0:T(8,128)(2,1)S(1)} %collective-permute-done.15.refs_5_) | copy-start | bytes 393220
  102.3 16.1 %collective-permute-start.10 = (bf16[128,512]{1,0:T(8,128)(2,1)}, bf16[128,512]{1,0:T(8,128)(2,1)S(1)}, u32[]{:S(2)}, u32[]{:S(2)}) collective-permute-start(bf16[128,512]{1,0:T(8,128)(2,1)} %get-tuple-element.55), channel_id=1, source_target_pairs={{0,16},{2,18},{4,20},{6,22},{8,24},{10,26},{12,28},{14,30},{16,0},... | collective-permute-start | bytes 393224 | tf_op jit(solution)/shard_map/ppermute | solution.py:475
  103.6 14.8 %copy-start.14 = (bf16[128,512]{1,0:T(8,128)(2,1)}, bf16[128,512]{1,0:T(8,128)(2,1)S(1)}, u32[]{:S(2)}) copy-start(bf16[128,512]{1,0:T(8,128)(2,1)S(1)} %collective-permute-done.16.refs_6_) | copy-start | bytes 393220
  103.6 14.8 %collective-permute-start.11 = (bf16[128,512]{1,0:T(8,128)(2,1)}, bf16[128,512]{1,0:T(8,128)(2,1)S(1)}, u32[]{:S(2)}, u32[]{:S(2)}) collective-permute-start(bf16[128,512]{1,0:T(8,128)(2,1)} %get-tuple-element.56), channel_id=1, source_target_pairs={{0,24},{2,26},{4,28},{6,30},{8,0},{10,2},{12,4},{14,6},{16,8},{18,... | collective-permute-start | bytes 393224 | tf_op jit(solution)/shard_map/ppermute | solution.py:475
  (10 other events, 7.1 us)

commit v4 on v3

--- a/solution.py
+++ b/solution.py
@@ -12,7 +12,8 @@
 F32 = jnp.float32
 BF16 = jnp.bfloat16
 HIGHEST = lax.Precision.HIGHEST
-VMEM_LIMIT = 56 * 1024 * 1024
+MIB = 1024 * 1024
+VMEM = {"local": 56, "grads": 28, "weight": 8, "input": 14}
 PACK = 8
 CHUNKS = 2
 
@@ -134,17 +135,17 @@
     ]
 
 
-def local_kernel(pack, share, outer, pos_ref, q_ref, k_ref, do_ref, hid_ref, w_ref, bp_ref, dp_ref, rate_ref, maps,
+def local_kernel(pack, share, outer, pos_ref, q_hbm, k_hbm, do_hbm, hid_ref, w_ref, bp_ref, dp_ref, rate_ref, maps,
                  *refs):
-    inv_ref, dr_ref, y_ref, bdr_ref, by_ref, v_ref, g_ref, b_ref, gt_ref, hid, hid_t, w, sems = refs[: 6] + refs[6 + maps.shape[0] :]
+    inv_ref, dr_ref, y_ref, bdr_ref, by_ref, v_ref, g_ref, b_ref, gt_ref, q_ref, k_ref, do_ref, hid, hid_t, w, sems = refs[: 6] + refs[6 + maps.shape[0] :]
     hid_parts = refs[6 : 6 + maps.shape[0]]
-    copies = [
-        pltpu.make_async_copy(hid_ref, hid, sems.at[0]),
-        pltpu.make_async_copy(w_ref, w, sems.at[1]),
-    ]
+    pairs = [(k_hbm, k_ref), (q_hbm, q_ref), (do_hbm, do_ref), (hid_ref, hid), (w_ref, w)]
+    copies = [pltpu.make_async_copy(a, b, sems.at[i]) for i, (a, b) in enumerate(pairs)]
     for copy in copies:
         copy.start()
     head_columns(bp_ref, dp_ref, rate_ref, g_ref, b_ref, gt_ref)
+    for copy in copies[:3]:
+        copy.wait()
     size = maps.shape[-1]
     for start in range(0, maps.shape[0] * share, pack):
         places = range(start, start + pack)
@@ -158,7 +159,7 @@
             for inv, d, t in zip(invs, d_written, tails)
         ]
         if start == 0:
-            for copy in copies:
+            for copy in copies[3:]:
                 copy.wait()
             v_ref[...] = low(dot(hid[...], w[...]))
             rows = hid.shape[1] // outer // maps.shape[0]
@@ -210,7 +211,7 @@
     )
     lead = lead_ref[0]
     for e in range(outer):
-        block = store[pl.ds(pl.multiple_of(lax.rem(lead + e, outer) * rows, rows), rows), :]
+        block = store[pl.ds(pl.multiple_of((lead ^ e) * rows, rows), rows), :]
         out_refs[e][...] = block.astype(out_refs[e].dtype)
 
 
@@ -305,9 +306,9 @@
     db_ref[...] = jnp.transpose(db_acc[...])[0:count]
 
 
-def call(body, args, outs, scratch=(), flops=0, anywhere=()):
+def call(body, name, args, outs, scratch=(), flops=0, anywhere=()):
     def place(i, a):
-        space = pltpu.SMEM if a.ndim == 1 else pl.ANY if i in anywhere else pltpu.VMEM
+        space = pltpu.SMEM if a.ndim == 1 else pltpu.HBM if i in anywhere else pltpu.VMEM
         return pl.BlockSpec(memory_space=space)
 
     return pl.pallas_call(
@@ -316,7 +317,7 @@
         out_specs=[pl.BlockSpec(memory_space=pltpu.VMEM) for _ in outs],
         out_shape=outs,
         scratch_shapes=list(scratch),
-        compiler_params=pltpu.CompilerParams(vmem_limit_bytes=VMEM_LIMIT),
+        compiler_params=pltpu.CompilerParams(vmem_limit_bytes=VMEM.get(name, 6) * MIB),
         cost_estimate=pl.CostEstimate(flops=flops, bytes_accessed=1 << 20, transcendentals=0),
     )(*args)
 
@@ -415,20 +416,22 @@
     ]
     maps, inv, dr, y, bdr, by, values, *hidden_t = call(
         functools.partial(local_kernel, PACK, share, outer),
+        "local",
         [jnp.full((1,), pos, jnp.int32), queries, keys, out_grad, hidden, value_weight, beta_t, decay_t, decay_rate],
         [shape(group, 3, share, dk, dv), shape(heads, n, n)]
         + [shape(n, width)] * 5
         + [shape(outer * rows, n)] * group,
         col_scratch
-        + [pltpu.VMEM(hidden.shape, BF16), pltpu.VMEM((model, n), BF16), pltpu.VMEM(value_weight.shape, BF16), pltpu.SemaphoreType.DMA((2,))],
+        + [pltpu.VMEM((n, width), BF16)] * 3
+        + [pltpu.VMEM(hidden.shape, BF16), pltpu.VMEM((model, n), BF16), pltpu.VMEM(value_weight.shape, BF16), pltpu.SemaphoreType.DMA((5,))],
         big,
-        (4, 5),
+        (1, 2, 3, 4, 5),
     )
     small = group * share * dk * dk * dk * 4
     triple, single = shape(3, share, dk, dv), shape(share, dk, dv)
 
     maps = swap(maps)
-    (total,) = call(total_kernel, [maps], [triple], (), small)
+    (total,) = call(total_kernel, "total", [maps], [triple], (), small)
     levels = outer.bit_length() - 2
     ranges = []
     for level in range(levels):
@@ -436,7 +439,7 @@
         ranges += [total, other]
         last = level == levels - 1
         (total,) = call(
-            functools.partial(join_kernel, level, last), [lead_arr, total, other],
+            functools.partial(join_kernel, level, last), "join", [lead_arr, total, other],
             [single if last else triple], [pltpu.VMEM((2,) + triple.shape, BF16)], small,
         )
     far = across(total, 1 << levels)
@@ -445,7 +448,7 @@
         moved.append(near(part, d))
     hidden_t = moved
     (states,) = call(
-        functools.partial(spread_kernel, levels), [lead_arr, maps, *ranges, far],
+        functools.partial(spread_kernel, levels), "spread", [lead_arr, maps, *ranges, far],
         [shape(group, 2, share, dk, dv)], (), small,
     )
     states = swap(states)
@@ -453,6 +456,7 @@
     chunk = width // CHUNKS
     d_values, *grad_chunks = call(
         functools.partial(values_kernel, share, CHUNKS),
+        "values",
         [bdr, by, states],
         [shape(n, width)] + [shape(n, chunk)] * CHUNKS,
         (),
@@ -465,21 +469,23 @@
             parts.append(near(own, d))
         blocks = call(
             functools.partial(weight_kernel, group, outer),
+            "weight",
             [lead_arr, *hidden_t, *parts],
             [shape(rows, chunk, dtype=BF16 if e else F32) for e in range(outer)],
             [pltpu.VMEM((outer * rows, chunk), F32)],
             2 * group * n * outer * rows * chunk,
         )
         for e, block in enumerate(blocks):
-            step = [(s, (s + e * group) % spans) for s in range(spans)]
-            pieces.append(lax.ppermute(block, "sp", step) if e else block)
-    (d_weight,) = call(functools.partial(sum_kernel, outer), pieces, [shape(rows, width, dtype=F32)], (), rows * width)
+            pieces.append(across(block, e) if e else block)
+    (d_weight,) = call(
+        functools.partial(sum_kernel, outer), "sum", pieces, [shape(rows, width, dtype=F32)], (), rows * width
+    )
 
     core = lax.axis_index("tp")
     cores = lax.axis_size("tp")
     own_rows = n // cores
     shares = call(
-        functools.partial(input_kernel, cores),
+        functools.partial(input_kernel, cores), "input",
         [jnp.full((1,), core, jnp.int32), d_values, value_weight],
         [shape(own_rows, model, dtype=BF16 if d else F32) for d in range(cores)],
         [pltpu.VMEM((n, model), F32)], n * width * model * 2,
@@ -488,10 +494,11 @@
         lax.ppermute(x, "tp", [(c, (c + d) % cores) for c in range(cores)]) if d else x
         for d, x in enumerate(shares)
     ]
-    (d_hidden,) = call(add_kernel, shares, [shape(own_rows, model)], (), own_rows * model)
+    (d_hidden,) = call(add_kernel, "add", shares, [shape(own_rows, model)], (), own_rows * model)
 
     d_queries, d_keys, d_beta, d_decay = call(
         functools.partial(grads_kernel, PACK, share),
+        "grads",
         [queries, keys, values, out_grad, beta_t, decay_t, decay_rate, inv, dr, y, states],
         [shape(n, width), shape(n, width), shape(heads, n, dtype=F32), shape(heads, n, dtype=F32)],
         col_scratch + [pltpu.VMEM((n, dk), F32), pltpu.VMEM((heads, n), F32), pltpu.VMEM((n, dk), F32)],

time: 125 us -> 110 us (0.88)
  Pallas kernels: 49.2 us -> 31.6 us
  waiting for transfers between devices: 18.8 us -> 23.2 us
  local copies, waits for them, and re-layouts: 5.06 us -> 2.96 us
    pallas_call x11, Pallas kernels: 49.2 us -> 31.6 us  [call(): pl.pallas_call(body, in_specs=[place(i, a) for i, a in enumerate(args)],...]
    ppermute x6 -> x0, starting transfers between devices: 12.5 us -> none  [per_device(): pieces.append(lax.ppermute(block, 'sp', step) if e else block)]
    ppermute x2 -> x8, starting transfers between devices: 4.54 us -> 16 us  [across(): return lax.ppermute(x, 'sp', [(s, s ^ reach * group) for s in range(spans)])]
    ppermute x2 -> x8, waiting for transfers between devices: 6.72 us -> 9.71 us  [across(): return lax.ppermute(x, 'sp', [(s, s ^ reach * group) for s in range(spans)])]
    unnamed x46 -> x32, local copies, waits for them, and re-layouts: 5.06 us -> 2.96 us
    ppermute x9, starting transfers between devices: 12.5 us -> 14.6 us  [near(): return lax.ppermute(x, 'sp', [(s, s ^ d) for s in range(spans)]) if d else x]
    ppermute x9, waiting for transfers between devices: 6.43 us -> 7.8 us  [near(): return lax.ppermute(x, 'sp', [(s, s ^ d) for s in range(spans)]) if d else x]
  transfers between devices with their start and end apart: 19 -> 19, of which waited for: 5 -> 8; matrix products, arithmetic and copies ran while one was open for 0% -> 0% of each run, Pallas kernels for 21% -> 13%
where the time goes in v4:
time: 110 us
  starting transfers between devices  34.2 us (31%)
  Pallas kernels  31.6 us (29%)
  waiting for transfers between devices  23.2 us (21%)
  blocking collectives  16.7 us (15%)
  local copies, waits for them, and re-layouts  2.96 us (3%)
    pallas_call x11, Pallas kernels, call(): pl.pallas_call(body, in_specs=[place(i, a) for i, a in enumerate(args)],...  31.6 us
    all_to_all x1, blocking collectives, swap(): return lax.all_to_all(x, 'sp', 0, 0, axis_index_groups=teams)  16.7 us
    ppermute x8, starting transfers between devices, across(): return lax.ppermute(x, 'sp', [(s, s ^ reach * group) for s in range(spans)])  16 us
    ppermute x9, starting transfers between devices, near(): return lax.ppermute(x, 'sp', [(s, s ^ d) for s in range(spans)]) if d else x  14.6 us
    ppermute x8, waiting for transfers between devices, across(): return lax.ppermute(x, 'sp', [(s, s ^ reach * group) for s in range(spans)])  9.71 us
    ppermute x9, waiting for transfers between devices, near(): return lax.ppermute(x, 'sp', [(s, s ^ d) for s in range(spans)]) if d else x  7.8 us
    all_to_all x1, waiting for transfers between devices, swap(): return lax.all_to_all(x, 'sp', 0, 0, axis_index_groups=teams)  5.65 us
    all_to_all x1, starting transfers between devices, swap(): return lax.all_to_all(x, 'sp', 0, 0, axis_index_groups=teams)  3.65 us
  transfers between devices with their start and end apart: 19, of which 8 were waited for; matrix products, arithmetic and copies ran while one was open for 0% of the time, Pallas kernels for 13%

profile of v4, /device:TPU:0, one launch (start us, length us, event | category | flops | bytes accessed | tf_op | source)
XLA Modules:
  0.0 109.6 jit_solution(17850864676539211730)
XLA Ops:
  0.6 14.1 %shard_map.127 = (bf16[4,3,2,128,128]{4,3,2,1,0:T(8,128)(2,1)}, bf16[8,256,256]{2,1,0:T(8,128)(2,1)}, bf16[256,1024]{1,0:T(8,128)(2,1)}, bf16[256,1024]{1,0:T(8,...) custom-call(s32[1]{0:T(128)} %bitcast.pos_ref, ...), custom_call_target="tpu_custom_call" | custom-call | flops 134217728 | bytes 1048576 | tf_op jit(solution)/shard_map/pallas_call | solution.py:314
  14.8 16.7 %all_to_all.10.maps = bf16[4,3,2,128,128]{4,3,2,1,0:T(8,128)(2,1)S(1)} all-to-all(bf16[4,3,2,128,128]{4,3,2,1,0:T(8,128)(2,1)} %get-tuple-element.38), channel_id=1, replica_groups={{0,2,4,6},{8,10,12,14},{16,18,20,22},{24,26,28,30},{1,3,5,7},{9,11,13,1..., dimensions={0} | all-to-all | bytes 1572864 | tf_op jit(solution)/shard_map/all_to_all | solution.py:405
  32.2 1.7 %collective-permute-start = (bf16[3,2,128,128]{3,2,1,0:T(8,128)(2,1)S(1)}, bf16[3,2,128,128]{3,2,1,0:T(8,128)(2,1)S(1)}, u32[]{:S(2)}, u32[]{:S(2)}) collective-permute-start(bf16[3,2,128,128]{3,2,1,0:T(8,128)(2,1)S(1)} %shard_map.128.own.refs_0_), channel_id=1, source_target_pairs={{0,8},{2,10},{4,12},{6,14},{8,0},{10,2},{12,4},{14,6},{16,24},{18,... | collective-permute-start | bytes 589832 | tf_op jit(solution)/shard_map/ppermute | solution.py:411
  33.9 4.1 %collective-permute-done.other.refs_1_ = bf16[3,2,128,128]{3,2,1,0:T(8,128)(2,1)S(1)} collective-permute-done((bf16[3,2,128,128]{3,2,1,0:T(8,128)(2,1)S(1)}, bf16[3,2,128,128]{3,2,1,0:T(8,128)(2,1)S(1)}, u32[]{:S(2)}, u32[]{:S(2)}) %collective-permute-start) | collective-permute-done | bytes 196640 | tf_op jit(solution)/shard_map/ppermute | solution.py:411
  38.2 2.7 %collective-permute-start.1 = (bf16[2,128,128]{2,1,0:T(8,128)(2,1)S(1)}, bf16[2,128,128]{2,1,0:T(8,128)(2,1)S(1)}, u32[]{:S(2)}, u32[]{:S(2)}) collective-permute-start(bf16[2,128,128]{2,1,0:T(8,128)(2,1)S(1)} %shard_map.129), channel_id=1, source_target_pairs={{0,16},{2,18},{4,20},{6,22},{8,24},{10,26},{12,28},{14,30},{16,0},... | collective-permute-start | bytes 196616 | tf_op jit(solution)/shard_map/ppermute | solution.py:411
  40.9 2.5 %collective-permute-done.1.refs_2_ = bf16[2,128,128]{2,1,0:T(8,128)(2,1)S(1)} collective-permute-done((bf16[2,128,128]{2,1,0:T(8,128)(2,1)S(1)}, bf16[2,128,128]{2,1,0:T(8,128)(2,1)S(1)}, u32[]{:S(2)}, u32[]{:S(2)}) %collective-permute-start.1) | collective-permute-done | bytes 65568 | tf_op jit(solution)/shard_map/ppermute | solution.py:411
  43.4 1.4 %shard_map.130 = bf16[4,2,2,128,128]{4,3,2,1,0:T(8,128)(2,1)} custom-call(s32[1]{0:T(128)} %bitcast.3.lead_ref, bf16[4,3,2,128,128]{4,3,2,1,0:T(8,128)(2,1)S(1)} %all_to_all.10.maps, bf16[3,2,128,128]{3,2,1,0:T(8,128)(2,1)S(1)} %shard_map.128.own.refs_0_, bf16[3,2,128,128]{3,2,1,0:T(8,128)(2,1)S(1)} %collective-permute-done.other.refs_1_, ...), custom_call_target="tpu_custom_call" | custom-call | flops 67108864 | bytes 1048576 | tf_op jit(solution)/shard_map/pallas_call | solution.py:314
  44.8 3.6 %all-to-all-start.1 = ((bf16[4,2,2,128,128]{4,3,2,1,0:T(8,128)(2,1)}), bf16[4,2,2,128,128]{4,3,2,1,0:T(8,128)(2,1)S(1)}, u32[]{:S(2)}, u32[]{:S(2)}) async-start(bf16[4,2,2,128,128]{4,3,2,1,0:T(8,128)(2,1)} %shard_map.130), calls=%async_computation.1 | async-start | bytes 1048576 | tf_op jit(solution)/shard_map/all_to_all | solution.py:405
  48.5 1.8 %collective-permute-start.3 = (bf16[512,256]{1,0:T(8,128)(2,1)}, bf16[512,256]{1,0:T(8,128)(2,1)S(1)}, u32[]{:S(2)}, u32[]{:S(2)}) collective-permute-start(bf16[512,256]{1,0:T(8,128)(2,1)} %get-tuple-element.49), channel_id=1, source_target_pairs={{0,2},{2,0},{4,6},{6,4},{8,10},{10,8},{12,14},{14,12},{16,18},{18,... | collective-permute-start | bytes 786440 | tf_op jit(solution)/shard_map/ppermute | solution.py:408
  50.3 1.5 %collective-permute-start.4 = (bf16[512,256]{1,0:T(8,128)(2,1)}, bf16[512,256]{1,0:T(8,128)(2,1)S(1)}, u32[]{:S(2)}, u32[]{:S(2)}) collective-permute-start(bf16[512,256]{1,0:T(8,128)(2,1)} %get-tuple-element.50), channel_id=1, source_target_pairs={{0,4},{2,6},{4,0},{6,2},{8,12},{10,14},{12,8},{14,10},{16,20},{18,... | collective-permute-start | bytes 786440 | tf_op jit(solution)/shard_map/ppermute | solution.py:408
  52.0 5.7 %all-to-all-done.1.states = bf16[4,2,2,128,128]{4,3,2,1,0:T(8,128)(2,1)S(1)} async-done(((bf16[4,2,2,128,128]{4,3,2,1,0:T(8,128)(2,1)}), bf16[4,2,2,128,128]{4,3,2,1,0:T(8,128)(2,1)S(1)}, u32[]{:S(2)}, u32[]{:S(2)}) %all-to-all-start.1) | async-done | bytes 524320 | tf_op jit(solution)/shard_map/all_to_all | solution.py:405
  57.7 1.0 shard_map.132
  59.4 1.2 %collective-permute-start.14 = (bf16[256,512]{1,0:T(8,128)(2,1)}, bf16[256,512]{1,0:T(8,128)(2,1)S(1)}, u32[]{:S(2)}, u32[]{:S(2)}) collective-permute-start(bf16[256,512]{1,0:T(8,128)(2,1)} %get-tuple-element.57.refs_4_), channel_id=1, source_target_pairs={{0,6},{2,4},{4,2},{6,0},{8,14},{10,12},{12,10},{14,8},{16,22},{18,... | collective-permute-start | bytes 786440 | tf_op jit(solution)/shard_map/ppermute | solution.py:408
  60.5 1.8 %collective-permute-start.13 = (bf16[256,512]{1,0:T(8,128)(2,1)}, bf16[256,512]{1,0:T(8,128)(2,1)S(1)}, u32[]{:S(2)}, u32[]{:S(2)}) collective-permute-start(bf16[256,512]{1,0:T(8,128)(2,1)} %get-tuple-element.57.refs_4_), channel_id=1, source_target_pairs={{0,4},{2,6},{4,0},{6,2},{8,12},{10,14},{12,8},{14,10},{16,20},{18,... | collective-permute-start | bytes 786440 | tf_op jit(solution)/shard_map/ppermute | solution.py:408
  62.4 0.9 collective-permute-done.3.refs_1_
  63.5 5.8 %collective-permute-done.4.refs_2_ = bf16[512,256]{1,0:T(8,128)(2,1)S(1)} collective-permute-done((bf16[512,256]{1,0:T(8,128)(2,1)}, bf16[512,256]{1,0:T(8,128)(2,1)S(1)}, u32[]{:S(2)}, u32[]{:S(2)}) %collective-permute-start.4) | collective-permute-done | bytes 262176 | tf_op jit(solution)/shard_map/ppermute | solution.py:408
  69.3 2.6 %collective-permute-start.8 = (bf16[256,512]{1,0:T(8,128)(2,1)}, bf16[256,512]{1,0:T(8,128)(2,1)S(1)}, u32[]{:S(2)}, u32[]{:S(2)}) collective-permute-start(bf16[256,512]{1,0:T(8,128)(2,1)} %copy-done.11), channel_id=1, source_target_pairs={{0,6},{2,4},{4,2},{6,0},{8,14},{10,12},{12,10},{14,8},{16,22},{18,... | collective-permute-start | bytes 786440 | tf_op jit(solution)/shard_map/ppermute | solution.py:408
  71.9 2.2 %copy-done = bf16[2048,1024]{1,0:T(8,128)(2,1)S(1)} copy-done((bf16[2048,1024]{1,0:T(8,128)(2,1)S(1)}, bf16[2048,1024]{1,0:T(8,128)(2,1)}, u32[]{:S(2)}) %copy-start) | copy-done | bytes 4194328
  74.2 1.6 %shard_map.133 = (f32[128,2048]{1,0:T(8,128)S(1)}, bf16[128,2048]{1,0:T(8,128)(2,1)S(1)}) custom-call(s32[1]{0:T(128)} %bitcast.6.core_ref, bf16[256,1024]{1,0:T(8,128)(2,1)S(1)} %get-tuple-element.45.dv_ref, bf16[2048,1024]{1,0:T(8,128)(2,1)S(1)} %copy-done), custom_call_target="tpu_custom_call" | custom-call | flops 1073741824 | bytes 1048576 | tf_op jit(solution)/shard_map/pallas_call | solution.py:314
  76.0 1.0 collective-permute-start.7
  76.9 1.0 collective-permute-done.13.refs_6_
  78.0 4.2 %collective-permute-start.6 = (bf16[256,512]{1,0:T(8,128)(2,1)S(1)}, bf16[256,512]{1,0:T(8,128)(2,1)S(1)}, u32[]{:S(2)}, u32[]{:S(2)}) collective-permute-start(bf16[256,512]{1,0:T(8,128)(2,1)S(1)} %copy-done.12), channel_id=1, source_target_pairs={{0,2},{2,0},{4,6},{6,4},{8,10},{10,8},{12,14},{14,12},{16,18},{18,... | collective-permute-start | bytes 786440 | tf_op jit(solution)/shard_map/ppermute | solution.py:408
  82.2 1.7 %shard_map.136 = (f32[128,512]{1,0:T(8,128)S(1)}, bf16[128,512]{1,0:T(8,128)(2,1)S(1)}, bf16[128,512]{1,0:T(8,128)(2,1)S(1)}, bf16[128,512]{1,0:T(8,128)(2,1)S(1)}) custom-call(s32[1]{0:T(128)} %bitcast.3.lead_ref, bf16[512,256]{1,0:T(8,128)(2,1)S(1)} %copy-done.5, bf16[512,256]{1,0:T(8,128)(2,1)S(1)} %collective-permute-done.3.refs_1_, ...), custom_call_target="tpu_custom_call" | custom-call | flops 536870912 | bytes 1048576 | tf_op jit(solution)/shard_map/pallas_call | solution.py:314
  83.9 1.6 %collective-permute-start.15 = (bf16[128,512]{1,0:T(8,128)(2,1)S(1)}, bf16[128,512]{1,0:T(8,128)(2,1)S(1)}, u32[]{:S(2)}, u32[]{:S(2)}) collective-permute-start(bf16[128,512]{1,0:T(8,128)(2,1)S(1)} %get-tuple-element.59), channel_id=1, source_target_pairs={{0,8},{2,10},{4,12},{6,14},{8,0},{10,2},{12,4},{14,6},{16,24},{18,... | collective-permute-start | bytes 393224 | tf_op jit(solution)/shard_map/ppermute | solution.py:411
  85.5 3.3 %collective-permute-start.16 = (bf16[128,512]{1,0:T(8,128)(2,1)S(1)}, bf16[128,512]{1,0:T(8,128)(2,1)S(1)}, u32[]{:S(2)}, u32[]{:S(2)}) collective-permute-start(bf16[128,512]{1,0:T(8,128)(2,1)S(1)} %get-tuple-element.60), channel_id=1, source_target_pairs={{0,16},{2,18},{4,20},{6,22},{8,24},{10,26},{12,28},{14,30},{16,0},... | collective-permute-start | bytes 393224 | tf_op jit(solution)/shard_map/ppermute | solution.py:411
  88.8 2.8 %collective-permute-start.17 = (bf16[128,512]{1,0:T(8,128)(2,1)S(1)}, bf16[128,512]{1,0:T(8,128)(2,1)S(1)}, u32[]{:S(2)}, u32[]{:S(2)}) collective-permute-start(bf16[128,512]{1,0:T(8,128)(2,1)S(1)} %get-tuple-element.61), channel_id=1, source_target_pairs={{0,24},{2,26},{4,28},{6,30},{8,16},{10,18},{12,20},{14,22},{16,8},... | collective-permute-start | bytes 393224 | tf_op jit(solution)/shard_map/ppermute | solution.py:411
  92.5 1.6 %collective-permute-start.10 = (bf16[128,512]{1,0:T(8,128)(2,1)S(1)}, bf16[128,512]{1,0:T(8,128)(2,1)S(1)}, u32[]{:S(2)}, u32[]{:S(2)}) collective-permute-start(bf16[128,512]{1,0:T(8,128)(2,1)S(1)} %get-tuple-element.55), channel_id=1, source_target_pairs={{0,16},{2,18},{4,20},{6,22},{8,24},{10,26},{12,28},{14,30},{16,0},... | collective-permute-start | bytes 393224 | tf_op jit(solution)/shard_map/ppermute | solution.py:411
  94.0 2.0 %collective-permute-done.16.refs_6_ = bf16[128,512]{1,0:T(8,128)(2,1)S(1)} collective-permute-done((bf16[128,512]{1,0:T(8,128)(2,1)S(1)}, bf16[128,512]{1,0:T(8,128)(2,1)S(1)}, u32[]{:S(2)}, u32[]{:S(2)}) %collective-permute-start.16) | collective-permute-done | bytes 131104 | tf_op jit(solution)/shard_map/ppermute | solution.py:411
  96.1 2.3 %collective-permute-start.11 = (bf16[128,512]{1,0:T(8,128)(2,1)S(1)}, bf16[128,512]{1,0:T(8,128)(2,1)S(1)}, u32[]{:S(2)}, u32[]{:S(2)}) collective-permute-start(bf16[128,512]{1,0:T(8,128)(2,1)S(1)} %get-tuple-element.56), channel_id=1, source_target_pairs={{0,24},{2,26},{4,28},{6,30},{8,16},{10,18},{12,20},{14,22},{16,8},... | collective-permute-start | bytes 393224 | tf_op jit(solution)/shard_map/ppermute | solution.py:411
  98.4 8.3 %shard_map.131 = (bf16[256,1024]{1,0:T(8,128)(2,1)}, bf16[256,1024]{1,0:T(8,128)(2,1)}, f32[8,256]{1,0:T(8,128)}, f32[8,256]{1,0:T(8,128)}) custom-call(bf16[256,1024]{1,0:T(8,128)(2,1)S(1)} %copy-done.1, bf16[256,1024]{1,0:T(8,128)(2,1)S(1)} %copy-done.2, bf16[256,1024]{1,0:T(8,128)(2,1)S(1)} %copy-done.8, bf16[256,1024]{1,0:T(8,128)(2,1)S(1)} %copy-done.3, ...), custom_call_target="tpu_custom_call" | custom-call | flops 134217728 | bytes 1048576 | tf_op jit(solution)/shard_map/pallas_call | solution.py:314
  106.7 1.1 collective-permute-done.10.refs_2_
  107.8 0.9 shard_map.137
  (50 shorter events, 4.0 us)
Async XLA Ops:
  14.8 42.9 %copy-start.9 = (bf16[256,1024]{1,0:T(8,128)(2,1)S(1)}, bf16[256,1024]{1,0:T(8,128)(2,1)}, u32[]{:S(2)}) copy-start(bf16[256,1024]{1,0:T(8,128)(2,1)} %get-tuple-element.43.bdr_ref) | copy-start | bytes 1572868
  14.8 42.9 %copy-start.10 = (bf16[256,1024]{1,0:T(8,128)(2,1)S(1)}, bf16[256,1024]{1,0:T(8,128)(2,1)}, u32[]{:S(2)}) copy-start(bf16[256,1024]{1,0:T(8,128)(2,1)} %get-tuple-element.44.by_ref) | copy-start | bytes 1572868
  32.2 5.7 %collective-permute-start = (bf16[3,2,128,128]{3,2,1,0:T(8,128)(2,1)S(1)}, bf16[3,2,128,128]{3,2,1,0:T(8,128)(2,1)S(1)}, u32[]{:S(2)}, u32[]{:S(2)}) collective-permute-start(bf16[3,2,128,128]{3,2,1,0:T(8,128)(2,1)S(1)} %shard_map.128.own.refs_0_), channel_id=1, source_target_pairs={{0,8},{2,10},{4,12},{6,14},{8,0},{10,2},{12,4},{14,6},{16,24},{18,... | collective-permute-start | bytes 589832 | tf_op jit(solution)/shard_map/ppermute | solution.py:411
  38.2 44.0 %copy-start.5 = (bf16[512,256]{1,0:T(8,128)(2,1)S(1)}, bf16[512,256]{1,0:T(8,128)(2,1)}, u32[]{:S(2)}) copy-start(bf16[512,256]{1,0:T(8,128)(2,1)} %get-tuple-element.48.refs_0_) | copy-start | bytes 786436
  38.2 5.2 %collective-permute-start.1 = (bf16[2,128,128]{2,1,0:T(8,128)(2,1)S(1)}, bf16[2,128,128]{2,1,0:T(8,128)(2,1)S(1)}, u32[]{:S(2)}, u32[]{:S(2)}) collective-permute-start(bf16[2,128,128]{2,1,0:T(8,128)(2,1)S(1)} %shard_map.129), channel_id=1, source_target_pairs={{0,16},{2,18},{4,20},{6,22},{8,24},{10,26},{12,28},{14,30},{16,0},... | collective-permute-start | bytes 196616 | tf_op jit(solution)/shard_map/ppermute | solution.py:411
  44.8 12.9 %all-to-all-start.1 = ((bf16[4,2,2,128,128]{4,3,2,1,0:T(8,128)(2,1)}), bf16[4,2,2,128,128]{4,3,2,1,0:T(8,128)(2,1)S(1)}, u32[]{:S(2)}, u32[]{:S(2)}) async-start(bf16[4,2,2,128,128]{4,3,2,1,0:T(8,128)(2,1)} %shard_map.130), calls=%async_computation.1 | async-start | bytes 1048576 | tf_op jit(solution)/shard_map/all_to_all | solution.py:405
  48.5 14.8 %collective-permute-start.3 = (bf16[512,256]{1,0:T(8,128)(2,1)}, bf16[512,256]{1,0:T(8,128)(2,1)S(1)}, u32[]{:S(2)}, u32[]{:S(2)}) collective-permute-start(bf16[512,256]{1,0:T(8,128)(2,1)} %get-tuple-element.49), channel_id=1, source_target_pairs={{0,2},{2,0},{4,6},{6,4},{8,10},{10,8},{12,14},{14,12},{16,18},{18,... | collective-permute-start | bytes 786440 | tf_op jit(solution)/shard_map/ppermute | solution.py:408
  50.3 19.0 %collective-permute-start.4 = (bf16[512,256]{1,0:T(8,128)(2,1)}, bf16[512,256]{1,0:T(8,128)(2,1)S(1)}, u32[]{:S(2)}, u32[]{:S(2)}) collective-permute-start(bf16[512,256]{1,0:T(8,128)(2,1)} %get-tuple-element.50), channel_id=1, source_target_pairs={{0,4},{2,6},{4,0},{6,2},{8,12},{10,14},{12,8},{14,10},{16,20},{18,... | collective-permute-start | bytes 786440 | tf_op jit(solution)/shard_map/ppermute | solution.py:408
  51.7 24.1 %collective-permute-start.5 = (bf16[512,256]{1,0:T(8,128)(2,1)}, bf16[512,256]{1,0:T(8,128)(2,1)S(1)}, u32[]{:S(2)}, u32[]{:S(2)}) collective-permute-start(bf16[512,256]{1,0:T(8,128)(2,1)} %get-tuple-element.51), channel_id=1, source_target_pairs={{0,6},{2,4},{4,2},{6,0},{8,14},{10,12},{12,10},{14,8},{16,22},{18,... | collective-permute-start | bytes 786440 | tf_op jit(solution)/shard_map/ppermute | solution.py:408
  59.4 16.5 %collective-permute-start.14 = (bf16[256,512]{1,0:T(8,128)(2,1)}, bf16[256,512]{1,0:T(8,128)(2,1)S(1)}, u32[]{:S(2)}, u32[]{:S(2)}) collective-permute-start(bf16[256,512]{1,0:T(8,128)(2,1)} %get-tuple-element.57.refs_4_), channel_id=1, source_target_pairs={{0,6},{2,4},{4,2},{6,0},{8,14},{10,12},{12,10},{14,8},{16,22},{18,... | collective-permute-start | bytes 786440 | tf_op jit(solution)/shard_map/ppermute | solution.py:408
  60.5 17.4 %collective-permute-start.13 = (bf16[256,512]{1,0:T(8,128)(2,1)}, bf16[256,512]{1,0:T(8,128)(2,1)S(1)}, u32[]{:S(2)}, u32[]{:S(2)}) collective-permute-start(bf16[256,512]{1,0:T(8,128)(2,1)} %get-tuple-element.57.refs_4_), channel_id=1, source_target_pairs={{0,4},{2,6},{4,0},{6,2},{8,12},{10,14},{12,8},{14,10},{16,20},{18,... | collective-permute-start | bytes 786440 | tf_op jit(solution)/shard_map/ppermute | solution.py:408
  63.3 18.9 %collective-permute-start.12 = (bf16[256,512]{1,0:T(8,128)(2,1)}, bf16[256,512]{1,0:T(8,128)(2,1)S(1)}, u32[]{:S(2)}, u32[]{:S(2)}) collective-permute-start(bf16[256,512]{1,0:T(8,128)(2,1)} %get-tuple-element.57.refs_4_), channel_id=1, source_target_pairs={{0,2},{2,0},{4,6},{6,4},{8,10},{10,8},{12,14},{14,12},{16,18},{18,... | collective-permute-start | bytes 786440 | tf_op jit(solution)/shard_map/ppermute | solution.py:408
  69.3 16.2 %collective-permute-start.8 = (bf16[256,512]{1,0:T(8,128)(2,1)}, bf16[256,512]{1,0:T(8,128)(2,1)S(1)}, u32[]{:S(2)}, u32[]{:S(2)}) collective-permute-start(bf16[256,512]{1,0:T(8,128)(2,1)} %copy-done.11), channel_id=1, source_target_pairs={{0,6},{2,4},{4,2},{6,0},{8,14},{10,12},{12,10},{14,8},{16,22},{18,... | collective-permute-start | bytes 786440 | tf_op jit(solution)/shard_map/ppermute | solution.py:408
  74.1 24.3 %copy-start.1 = (bf16[256,1024]{1,0:T(8,128)(2,1)S(1)}, bf16[256,1024]{1,0:T(8,128)(2,1)}, u32[]{:S(2)}) copy-start(bf16[256,1024]{1,0:T(8,128)(2,1)} %q_ref.1) | copy-start | bytes 1572868
  74.1 24.3 %copy-start.2 = (bf16[256,1024]{1,0:T(8,128)(2,1)S(1)}, bf16[256,1024]{1,0:T(8,128)(2,1)}, u32[]{:S(2)}) copy-start(bf16[256,1024]{1,0:T(8,128)(2,1)} %k_ref.1) | copy-start | bytes 1572868
  74.1 24.3 %copy-start.3 = (bf16[256,1024]{1,0:T(8,128)(2,1)S(1)}, bf16[256,1024]{1,0:T(8,128)(2,1)}, u32[]{:S(2)}) copy-start(bf16[256,1024]{1,0:T(8,128)(2,1)} %do_ref.1) | copy-start | bytes 1572868
  74.1 24.3 %copy-start.4 = (bf16[8,256,256]{2,1,0:T(8,128)(2,1)S(1)}, bf16[8,256,256]{2,1,0:T(8,128)(2,1)}, u32[]{:S(2)}) copy-start(bf16[8,256,256]{2,1,0:T(8,128)(2,1)} %get-tuple-element.35.inv_ref) | copy-start | bytes 3145732
  74.1 24.3 %copy-start.6 = (bf16[256,1024]{1,0:T(8,128)(2,1)S(1)}, bf16[256,1024]{1,0:T(8,128)(2,1)}, u32[]{:S(2)}) copy-start(bf16[256,1024]{1,0:T(8,128)(2,1)} %get-tuple-element.36.dr_ref) | copy-start | bytes 1572868
  74.1 24.3 %copy-start.7 = (bf16[256,1024]{1,0:T(8,128)(2,1)S(1)}, bf16[256,1024]{1,0:T(8,128)(2,1)}, u32[]{:S(2)}) copy-start(bf16[256,1024]{1,0:T(8,128)(2,1)} %get-tuple-element.37.y_ref) | copy-start | bytes 1572868
  74.2 24.3 %copy-start.8 = (bf16[256,1024]{1,0:T(8,128)(2,1)S(1)}, bf16[256,1024]{1,0:T(8,128)(2,1)}, u32[]{:S(2)}) copy-start(bf16[256,1024]{1,0:T(8,128)(2,1)} %get-tuple-element.34.v_ref) | copy-start | bytes 1572868
  74.2 24.3 %copy-start.13 = (f32[256,8]{0,1:T(8,128)S(1)}, f32[256,8]{0,1:T(8,128)}, u32[]{:S(2)}) copy-start(f32[256,8]{0,1:T(8,128)} %param.12) | copy-start | bytes 24580
  74.2 24.2 %copy-start.14 = (f32[256,8]{0,1:T(8,128)S(1)}, f32[256,8]{0,1:T(8,128)}, u32[]{:S(2)}) copy-start(f32[256,8]{0,1:T(8,128)} %param.13) | copy-start | bytes 24580
  74.2 24.2 %copy-start.15 = (f32[8]{0:T(128)S(1)}, f32[8]{0:T(128)}, u32[]{:S(2)}) copy-start(f32[8]{0:T(128)} %rate_ref.3) | copy-start | bytes 100
  75.9 32.8 %collective-permute-start.2 = (bf16[128,2048]{1,0:T(8,128)(2,1)S(1)}, bf16[128,2048]{1,0:T(8,128)(2,1)S(1)}, u32[]{:S(2)}, u32[]{:S(2)}) collective-permute-start(bf16[128,2048]{1,0:T(8,128)(2,1)S(1)} %get-tuple-element.47), channel_id=1, source_target_pairs={{0,1},{1,0},{2,3},{3,2},{4,5},{5,4},{6,7},{7,6},{8,9},{9,8},{10,11... | collective-permute-start | bytes 1572872 | tf_op jit(solution)/shard_map/ppermute | solution.py:494
  76.0 12.9 %collective-permute-start.7 = (bf16[256,512]{1,0:T(8,128)(2,1)S(1)}, bf16[256,512]{1,0:T(8,128)(2,1)S(1)}, u32[]{:S(2)}, u32[]{:S(2)}) collective-permute-start(bf16[256,512]{1,0:T(8,128)(2,1)S(1)} %copy-done.12), channel_id=1, source_target_pairs={{0,4},{2,6},{4,0},{6,2},{8,12},{10,14},{12,8},{14,10},{16,20},{18,... | collective-permute-start | bytes 786440 | tf_op jit(solution)/shard_map/ppermute | solution.py:408
  78.0 13.6 %collective-permute-start.6 = (bf16[256,512]{1,0:T(8,128)(2,1)S(1)}, bf16[256,512]{1,0:T(8,128)(2,1)S(1)}, u32[]{:S(2)}, u32[]{:S(2)}) collective-permute-start(bf16[256,512]{1,0:T(8,128)(2,1)S(1)} %copy-done.12), channel_id=1, source_target_pairs={{0,2},{2,0},{4,6},{6,4},{8,10},{10,8},{12,14},{14,12},{16,18},{18,... | collective-permute-start | bytes 786440 | tf_op jit(solution)/shard_map/ppermute | solution.py:408
  83.9 8.5 %collective-permute-start.15 = (bf16[128,512]{1,0:T(8,128)(2,1)S(1)}, bf16[128,512]{1,0:T(8,128)(2,1)S(1)}, u32[]{:S(2)}, u32[]{:S(2)}) collective-permute-start(bf16[128,512]{1,0:T(8,128)(2,1)S(1)} %get-tuple-element.59), channel_id=1, source_target_pairs={{0,8},{2,10},{4,12},{6,14},{8,0},{10,2},{12,4},{14,6},{16,24},{18,... | collective-permute-start | bytes 393224 | tf_op jit(solution)/shard_map/ppermute | solution.py:411
  85.5 10.5 %collective-permute-start.16 = (bf16[128,512]{1,0:T(8,128)(2,1)S(1)}, bf16[128,512]{1,0:T(8,128)(2,1)S(1)}, u32[]{:S(2)}, u32[]{:S(2)}) collective-permute-start(bf16[128,512]{1,0:T(8,128)(2,1)S(1)} %get-tuple-element.60), channel_id=1, source_target_pairs={{0,16},{2,18},{4,20},{6,22},{8,24},{10,26},{12,28},{14,30},{16,0},... | collective-permute-start | bytes 393224 | tf_op jit(solution)/shard_map/ppermute | solution.py:411
  88.8 17.9 %collective-permute-start.17 = (bf16[128,512]{1,0:T(8,128)(2,1)S(1)}, bf16[128,512]{1,0:T(8,128)(2,1)S(1)}, u32[]{:S(2)}, u32[]{:S(2)}) collective-permute-start(bf16[128,512]{1,0:T(8,128)(2,1)S(1)} %get-tuple-element.61), channel_id=1, source_target_pairs={{0,24},{2,26},{4,28},{6,30},{8,16},{10,18},{12,20},{14,22},{16,8},... | collective-permute-start | bytes 393224 | tf_op jit(solution)/shard_map/ppermute | solution.py:411
  92.4 14.3 %collective-permute-start.9 = (bf16[128,512]{1,0:T(8,128)(2,1)S(1)}, bf16[128,512]{1,0:T(8,128)(2,1)S(1)}, u32[]{:S(2)}, u32[]{:S(2)}) collective-permute-start(bf16[128,512]{1,0:T(8,128)(2,1)S(1)} %get-tuple-element.54), channel_id=1, source_target_pairs={{0,8},{2,10},{4,12},{6,14},{8,0},{10,2},{12,4},{14,6},{16,24},{18,... | collective-permute-start | bytes 393224 | tf_op jit(solution)/shard_map/ppermute | solution.py:411
  92.5 15.3 %collective-permute-start.10 = (bf16[128,512]{1,0:T(8,128)(2,1)S(1)}, bf16[128,512]{1,0:T(8,128)(2,1)S(1)}, u32[]{:S(2)}, u32[]{:S(2)}) collective-permute-start(bf16[128,512]{1,0:T(8,128)(2,1)S(1)} %get-tuple-element.55), channel_id=1, source_target_pairs={{0,16},{2,18},{4,20},{6,22},{8,24},{10,26},{12,28},{14,30},{16,0},... | collective-permute-start | bytes 393224 | tf_op jit(solution)/shard_map/ppermute | solution.py:411
  96.1 11.7 %collective-permute-start.11 = (bf16[128,512]{1,0:T(8,128)(2,1)S(1)}, bf16[128,512]{1,0:T(8,128)(2,1)S(1)}, u32[]{:S(2)}, u32[]{:S(2)}) collective-permute-start(bf16[128,512]{1,0:T(8,128)(2,1)S(1)} %get-tuple-element.56), channel_id=1, source_target_pairs={{0,24},{2,26},{4,28},{6,30},{8,16},{10,18},{12,20},{14,22},{16,8},... | collective-permute-start | bytes 393224 | tf_op jit(solution)/shard_map/ppermute | solution.py:411
  (3 other events, 4.7 us)

commit v5 on v4

--- a/solution.py
+++ b/solution.py
@@ -15,7 +15,6 @@
 MIB = 1024 * 1024
 VMEM = {"local": 56, "grads": 28, "weight": 8, "input": 14}
 PACK = 8
-CHUNKS = 2
 
 
 def dot(a, b, ca=1, cb=0, precision=None):
@@ -106,12 +105,11 @@
     return h
 
 
-def unit_lower_inverses(mats):
-    n = mats[0].shape[0]
+def unit_lower_inverses(high):
+    n = high[0].shape[0]
     rows, cols = iotas(n)
     differ = rows ^ cols
     eye = (rows == cols).astype(F32)
-    high = [low(a) for a in mats]
     xs = [low(eye) - a * low((differ == 1).astype(F32)) for a in high]
     size = 2
     while 2 * size < n:
@@ -125,14 +123,8 @@
         jnp.concatenate([x[:size], jnp.concatenate([z, x[size:, size:]], axis=1)], axis=0)
         for x, z in zip(xs, zs)
     ]
-    rest = [low(a - h.astype(F32)) for a, h in zip(mats, high)]
-    products = [
-        dot(jnp.concatenate([h, l], axis=1), jnp.concatenate([x, x], axis=0))
-        for h, l, x in zip(high, rest, xs)
-    ]
-    return [
-        low(x.astype(F32) + dot(x, low(eye - x.astype(F32) - y))) for x, y in zip(xs, products)
-    ]
+    rests = [low(eye - x.astype(F32) - dot(a, x)) for a, x in zip(high, xs)]
+    return [low(x.astype(F32) + dot(x, r)) for x, r in zip(xs, rests)]
 
 
 def local_kernel(pack, share, outer, pos_ref, q_hbm, k_hbm, do_hbm, hid_ref, w_ref, bp_ref, dp_ref, rate_ref, maps,
@@ -152,7 +144,7 @@
         heads = [head_common(q_ref, k_ref, p, size, g_ref, b_ref, gt_ref) for p in places]
         outs = [do_ref[:, h.lanes] for h in heads]
         d_written = [low(dot(low(h.p), do16, 0, 0)) for h, do16 in zip(heads, outs)]
-        invs = unit_lower_inverses([h.a0 * h.tile(h.beta) for h in heads])
+        invs = unit_lower_inverses([low(h.a0 * h.tile(h.beta)) for h in heads])
         tails = [low(h.k_hat * h.tail) for h in heads]
         both = [
             dot(inv, jnp.concatenate([d, t], axis=1), 0, 0)
@@ -191,15 +183,19 @@
             out[2, p % share] = low(into[:, size:])
 
 
-def values_kernel(share, chunks, bdr_ref, by_ref, states, dv_ref, *parts):
+def values_kernel(share, group, pos_ref, bdr_ref, by_ref, *refs):
+    state_refs, states, dv_ref, parts = refs[:group], refs[group], refs[group + 1], refs[group + 2 :]
+    for d, ref in enumerate(state_refs):
+        states[pos_ref[0] ^ d] = ref[...]
     size = states.shape[-1]
     count = states.shape[0] * share
-    per = count // chunks
+    places = [(part, i) for part in parts for i in range(part.shape[1] // size)]
     for h in range(count):
         lanes = slice(h * size, (h + 1) * size)
         dv = low(bdr_ref[:, lanes].astype(F32) + dot(by_ref[:, lanes], states[h // share, 0, h % share], 1, 1))
         dv_ref[:, lanes] = dv
-        parts[h // per][:, (h % per) * size : (h % per + 1) * size] = dv
+        part, i = places[h]
+        part[:, i * size : (i + 1) * size] = dv
 
 
 def weight_kernel(group, outer, lead_ref, *refs):
@@ -231,11 +227,12 @@
 
 def sum_kernel(outer, *refs):
     out_ref = refs[-1]
-    chunks = (len(refs) - 1) // outer
-    width = refs[0].shape[1]
-    for c in range(chunks):
-        parts = refs[c * outer : (c + 1) * outer]
-        out_ref[:, c * width : (c + 1) * width] = sum(r[...].astype(F32) for r in parts)
+    at = 0
+    for c in range(0, len(refs) - 1, outer):
+        parts = refs[c : c + outer]
+        width = parts[0].shape[1]
+        out_ref[:, at : at + width] = sum(r[...].astype(F32) for r in parts)
+        at += width
 
 
 def grads_kernel(pack, share, q_ref, k_ref, v_ref, do_ref, bp_ref, dp_ref, rate_ref, inv_ref, dr_ref, y_ref, states,
@@ -311,7 +308,7 @@
         space = pltpu.SMEM if a.ndim == 1 else pltpu.HBM if i in anywhere else pltpu.VMEM
         return pl.BlockSpec(memory_space=space)
 
-    return pl.pallas_call(
+    results = pl.pallas_call(
         body,
         in_specs=[place(i, a) for i, a in enumerate(args)],
         out_specs=[pl.BlockSpec(memory_space=pltpu.VMEM) for _ in outs],
@@ -320,6 +317,7 @@
         compiler_params=pltpu.CompilerParams(vmem_limit_bytes=VMEM.get(name, 6) * MIB),
         cost_estimate=pl.CostEstimate(flops=flops, bytes_accessed=1 << 20, transcendentals=0),
     )(*args)
+    return list(results)
 
 
 def shape(*dims, dtype=BF16):
@@ -352,8 +350,8 @@
             out_ref[0, i], out_ref[1, i], out_ref[2, i] = low(dot(both[1, 0, i], both[0, 0, i])), g, o
 
 
-def spread_kernel(levels, lead_ref, maps, *refs):
-    ranges, far, result = refs[: 2 * levels], refs[2 * levels], refs[2 * levels + 1]
+def spread_kernel(levels, lead_ref, pos_ref, maps, *refs):
+    ranges, far, out_refs, result = refs[: 2 * levels], refs[2 * levels], refs[2 * levels + 1 : -1], refs[-1]
     lead = lead_ref[0]
     group, _, share = maps.shape[:3]
     later = (lead >> levels) & 1
@@ -374,6 +372,8 @@
             if j < group - 1:
                 es[i] = low(maps[b, 1, i].astype(F32) + dot(es[i], maps[b, 0, i]))
                 ss[i] = low(maps[j, 2, i].astype(F32) + dot(maps[j, 0, i], ss[i]))
+    for d, out_ref in enumerate(out_refs):
+        out_ref[...] = result[pos_ref[0] ^ d]
 
 
 def group_size(count, heads):
@@ -396,6 +396,7 @@
     pos = lax.rem(place, group)
     lead = lax.div(place, group)
     lead_arr = jnp.full((1,), lead, jnp.int32)
+    pos_arr = jnp.full((1,), pos, jnp.int32)
     share = heads // group
     beta_t, decay_t = beta_pre.T, decay_pre.T
     big = heads * n * n * 256
@@ -417,7 +418,7 @@
     maps, inv, dr, y, bdr, by, values, *hidden_t = call(
         functools.partial(local_kernel, PACK, share, outer),
         "local",
-        [jnp.full((1,), pos, jnp.int32), queries, keys, out_grad, hidden, value_weight, beta_t, decay_t, decay_rate],
+        [pos_arr, queries, keys, out_grad, hidden, value_weight, beta_t, decay_t, decay_rate],
         [shape(group, 3, share, dk, dv), shape(heads, n, n)]
         + [shape(n, width)] * 5
         + [shape(outer * rows, n)] * group,
@@ -447,23 +448,26 @@
     for d, part in enumerate(hidden_t):
         moved.append(near(part, d))
     hidden_t = moved
-    (states,) = call(
-        functools.partial(spread_kernel, levels), "spread", [lead_arr, maps, *ranges, far],
-        [shape(group, 2, share, dk, dv)], (), small,
-    )
-    states = swap(states)
-
-    chunk = width // CHUNKS
-    d_values, *grad_chunks = call(
-        functools.partial(values_kernel, share, CHUNKS),
+    states = call(
+        functools.partial(spread_kernel, levels), "spread", [lead_arr, pos_arr, maps, *ranges, far],
+        [shape(2, share, dk, dv)] * group, [pltpu.VMEM((group, 2, share, dk, dv), BF16)], small,
+    )
+    for d in range(1, group):
+        states[d] = near(states[d], d)
+
+    first = max(1, heads * 4 // 8) * dv
+    widths = [first, width - first]
+    states, d_values, *grad_chunks = call(
+        functools.partial(values_kernel, share, group),
         "values",
-        [bdr, by, states],
-        [shape(n, width)] + [shape(n, chunk)] * CHUNKS,
+        [pos_arr, bdr, by, *states],
+        [shape(group, 2, share, dk, dv), shape(n, width)] + [shape(n, chunk) for chunk in widths],
         (),
         heads * n * dk * dv * 2,
     )
     pieces = []
-    for own in grad_chunks:
+    for c, own in enumerate(grad_chunks):
+        chunk = widths[c]
         parts = []
         for d in range(group):
             parts.append(near(own, d))

time: 110 us -> 110 us (level)
  Pallas kernels: 31.6 us -> 30.5 us
    ppermute x9 -> x12, waiting for transfers between devices: 7.8 us -> 15.1 us  [near(): return lax.ppermute(x, 'sp', [(s, s ^ d) for s in range(spans)]) if d else x]
    all_to_all x1 -> x0, waiting for transfers between devices: 5.65 us -> none  [swap(): return lax.all_to_all(x, 'sp', 0, 0, axis_index_groups=teams)]
    all_to_all x1 -> x0, starting transfers between devices: 3.65 us -> none  [swap(): return lax.all_to_all(x, 'sp', 0, 0, axis_index_groups=teams)]
    ppermute x8, starting transfers between devices: 16 us -> 18.9 us  [across(): return lax.ppermute(x, 'sp', [(s, s ^ reach * group) for s in range(spans)])]
    ppermute x9 -> x12, starting transfers between devices: 14.6 us -> 16.1 us  [near(): return lax.ppermute(x, 'sp', [(s, s ^ d) for s in range(spans)]) if d else x]
    ppermute x8, waiting for transfers between devices: 9.71 us -> 8.52 us  [across(): return lax.ppermute(x, 'sp', [(s, s ^ reach * group) for s in range(spans)])]
    pallas_call x11, Pallas kernels: 31.6 us -> 30.5 us  [call(): pl.pallas_call(body, in_specs=[place(i, a) for i, a in enumerate(args)],...]
  transfers between devices with their start and end apart: 19 -> 21, of which waited for: 8 -> 5; matrix products, arithmetic and copies ran while one was open for 0% -> 0% of each run, Pallas kernels for 13% -> 13%
where the time goes in v5:
time: 110 us
  starting transfers between devices  35 us (32%)
  Pallas kernels  30.5 us (28%)
  waiting for transfers between devices  23.6 us (21%)
  blocking collectives  16.7 us (15%)
  local copies, waits for them, and re-layouts  2.96 us (3%)
    pallas_call x11, Pallas kernels, call(): pl.pallas_call(body, in_specs=[place(i, a) for i, a in enumerate(args)],...  30.5 us
    ppermute x8, starting transfers between devices, across(): return lax.ppermute(x, 'sp', [(s, s ^ reach * group) for s in range(spans)])  18.9 us
    all_to_all x1, blocking collectives, swap(): return lax.all_to_all(x, 'sp', 0, 0, axis_index_groups=teams)  16.7 us
    ppermute x12, starting transfers between devices, near(): return lax.ppermute(x, 'sp', [(s, s ^ d) for s in range(spans)]) if d else x  16.1 us
    ppermute x12, waiting for transfers between devices, near(): return lax.ppermute(x, 'sp', [(s, s ^ d) for s in range(spans)]) if d else x  15.1 us
    ppermute x8, waiting for transfers between devices, across(): return lax.ppermute(x, 'sp', [(s, s ^ reach * group) for s in range(spans)])  8.52 us
    unnamed x32, local copies, waits for them, and re-layouts  2.96 us
  transfers between devices with their start and end apart: 21, of which 5 were waited for; matrix products, arithmetic and copies ran while one was open for 0% of the time, Pallas kernels for 13%

profile of v5, /device:TPU:0, one launch (start us, length us, event | category | flops | bytes accessed | tf_op | source)
XLA Modules:
  0.0 109.7 jit_solution(16811254831221655183)
XLA Ops:
  0.6 13.7 %shard_map.127 = (bf16[4,3,2,128,128]{4,3,2,1,0:T(8,128)(2,1)}, bf16[8,256,256]{2,1,0:T(8,128)(2,1)}, bf16[256,1024]{1,0:T(8,128)(2,1)}, bf16[256,1024]{1,0:T(8,...) custom-call(s32[1]{0:T(128)} %bitcast.pos_ref, ...), custom_call_target="tpu_custom_call" | custom-call | flops 134217728 | bytes 1048576 | tf_op jit(solution)/shard_map/pallas_call | solution.py:311
  14.4 16.7 %all_to_all.5.maps = bf16[4,3,2,128,128]{4,3,2,1,0:T(8,128)(2,1)S(1)} all-to-all(bf16[4,3,2,128,128]{4,3,2,1,0:T(8,128)(2,1)} %get-tuple-element.45), channel_id=1, replica_groups={{0,2,4,6},{8,10,12,14},{16,18,20,22},{24,26,28,30},{1,3,5,7},{9,11,13,1..., dimensions={0} | all-to-all | bytes 1572864 | tf_op jit(solution)/shard_map/all_to_all | solution.py:406
  31.8 1.7 %collective-permute-start = (bf16[3,2,128,128]{3,2,1,0:T(8,128)(2,1)S(1)}, bf16[3,2,128,128]{3,2,1,0:T(8,128)(2,1)S(1)}, u32[]{:S(2)}, u32[]{:S(2)}) collective-permute-start(bf16[3,2,128,128]{3,2,1,0:T(8,128)(2,1)S(1)} %shard_map.128.own.refs_0_), channel_id=1, source_target_pairs={{0,8},{2,10},{4,12},{6,14},{8,0},{10,2},{12,4},{14,6},{16,24},{18,... | collective-permute-start | bytes 589832 | tf_op jit(solution)/shard_map/ppermute | solution.py:412
  33.4 4.1 %collective-permute-done.other.refs_1_ = bf16[3,2,128,128]{3,2,1,0:T(8,128)(2,1)S(1)} collective-permute-done((bf16[3,2,128,128]{3,2,1,0:T(8,128)(2,1)S(1)}, bf16[3,2,128,128]{3,2,1,0:T(8,128)(2,1)S(1)}, u32[]{:S(2)}, u32[]{:S(2)}) %collective-permute-start) | collective-permute-done | bytes 196640 | tf_op jit(solution)/shard_map/ppermute | solution.py:412
  37.7 2.7 %collective-permute-start.1 = (bf16[2,128,128]{2,1,0:T(8,128)(2,1)S(1)}, bf16[2,128,128]{2,1,0:T(8,128)(2,1)S(1)}, u32[]{:S(2)}, u32[]{:S(2)}) collective-permute-start(bf16[2,128,128]{2,1,0:T(8,128)(2,1)S(1)} %shard_map.129), channel_id=1, source_target_pairs={{0,16},{2,18},{4,20},{6,22},{8,24},{10,26},{12,28},{14,30},{16,0},... | collective-permute-start | bytes 196616 | tf_op jit(solution)/shard_map/ppermute | solution.py:412
  40.4 2.5 %collective-permute-done.1.refs_2_ = bf16[2,128,128]{2,1,0:T(8,128)(2,1)S(1)} collective-permute-done((bf16[2,128,128]{2,1,0:T(8,128)(2,1)S(1)}, bf16[2,128,128]{2,1,0:T(8,128)(2,1)S(1)}, u32[]{:S(2)}, u32[]{:S(2)}) %collective-permute-start.1) | collective-permute-done | bytes 65568 | tf_op jit(solution)/shard_map/ppermute | solution.py:412
  43.6 1.0 collective-permute-start.2
  44.6 1.1 %collective-permute-start.6 = (bf16[512,256]{1,0:T(8,128)(2,1)}, bf16[512,256]{1,0:T(8,128)(2,1)S(1)}, u32[]{:S(2)}, u32[]{:S(2)}) collective-permute-start(bf16[512,256]{1,0:T(8,128)(2,1)} %get-tuple-element.59), channel_id=1, source_target_pairs={{0,2},{2,0},{4,6},{6,4},{8,10},{10,8},{12,14},{14,12},{16,18},{18,... | collective-permute-start | bytes 786440 | tf_op jit(solution)/shard_map/ppermute | solution.py:409
  45.7 0.9 collective-permute-start.7
  46.6 1.1 %collective-permute-start.3 = (bf16[2,2,128,128]{3,2,1,0:T(8,128)(2,1)S(1)}, bf16[2,2,128,128]{3,2,1,0:T(8,128)(2,1)S(1)}, u32[]{:S(2)}, u32[]{:S(2)}) collective-permute-start(bf16[2,2,128,128]{3,2,1,0:T(8,128)(2,1)S(1)} %get-tuple-element.48), channel_id=1, source_target_pairs={{0,4},{2,6},{4,0},{6,2},{8,12},{10,14},{12,8},{14,10},{16,20},{18,... | collective-permute-start | bytes 393224 | tf_op jit(solution)/shard_map/ppermute | solution.py:409
  47.7 0.9 collective-permute-start.4
  48.6 1.4 %collective-permute-done.2.refs_1_ = bf16[2,2,128,128]{3,2,1,0:T(8,128)(2,1)S(1)} collective-permute-done((bf16[2,2,128,128]{3,2,1,0:T(8,128)(2,1)S(1)}, bf16[2,2,128,128]{3,2,1,0:T(8,128)(2,1)S(1)}, u32[]{:S(2)}, u32[]{:S(2)}) %collective-permute-start.2) | collective-permute-done | bytes 131104 | tf_op jit(solution)/shard_map/ppermute | solution.py:409
  50.0 0.9 collective-permute-start.8
  50.9 13.7 %collective-permute-done.3.refs_2_ = bf16[2,2,128,128]{3,2,1,0:T(8,128)(2,1)S(1)} collective-permute-done((bf16[2,2,128,128]{3,2,1,0:T(8,128)(2,1)S(1)}, bf16[2,2,128,128]{3,2,1,0:T(8,128)(2,1)S(1)}, u32[]{:S(2)}, u32[]{:S(2)}) %collective-permute-start.3) | collective-permute-done | bytes 131104 | tf_op jit(solution)/shard_map/ppermute | solution.py:409
  64.6 1.1 shard_map.131
  66.4 3.6 %collective-permute-start.17 = (bf16[256,512]{1,0:T(8,128)(2,1)}, bf16[256,512]{1,0:T(8,128)(2,1)S(1)}, u32[]{:S(2)}, u32[]{:S(2)}) collective-permute-start(bf16[256,512]{1,0:T(8,128)(2,1)} %get-tuple-element.67.refs_4_), channel_id=1, source_target_pairs={{0,6},{2,4},{4,2},{6,0},{8,14},{10,12},{12,10},{14,8},{16,22},{18,... | collective-permute-start | bytes 786440 | tf_op jit(solution)/shard_map/ppermute | solution.py:409
  70.0 2.6 %collective-permute-start.16 = (bf16[256,512]{1,0:T(8,128)(2,1)}, bf16[256,512]{1,0:T(8,128)(2,1)S(1)}, u32[]{:S(2)}, u32[]{:S(2)}) collective-permute-start(bf16[256,512]{1,0:T(8,128)(2,1)} %get-tuple-element.67.refs_4_), channel_id=1, source_target_pairs={{0,4},{2,6},{4,0},{6,2},{8,12},{10,14},{12,8},{14,10},{16,20},{18,... | collective-permute-start | bytes 786440 | tf_op jit(solution)/shard_map/ppermute | solution.py:409
  72.6 1.5 %collective-permute-start.11 = (bf16[256,512]{1,0:T(8,128)(2,1)}, bf16[256,512]{1,0:T(8,128)(2,1)S(1)}, u32[]{:S(2)}, u32[]{:S(2)}) collective-permute-start(bf16[256,512]{1,0:T(8,128)(2,1)} %copy-done.11), channel_id=1, source_target_pairs={{0,6},{2,4},{4,2},{6,0},{8,14},{10,12},{12,10},{14,8},{16,22},{18,... | collective-permute-start | bytes 786440 | tf_op jit(solution)/shard_map/ppermute | solution.py:409
  74.1 2.2 %copy-done = bf16[2048,1024]{1,0:T(8,128)(2,1)S(1)} copy-done((bf16[2048,1024]{1,0:T(8,128)(2,1)S(1)}, bf16[2048,1024]{1,0:T(8,128)(2,1)}, u32[]{:S(2)}) %copy-start) | copy-done | bytes 4194328
  76.4 1.6 %shard_map.133 = (f32[128,2048]{1,0:T(8,128)S(1)}, bf16[128,2048]{1,0:T(8,128)(2,1)S(1)}) custom-call(s32[1]{0:T(128)} %bitcast.6.core_ref, bf16[256,1024]{1,0:T(8,128)(2,1)S(1)} %get-tuple-element.55.dv_ref, bf16[2048,1024]{1,0:T(8,128)(2,1)S(1)} %copy-done), custom_call_target="tpu_custom_call" | custom-call | flops 1073741824 | bytes 1048576 | tf_op jit(solution)/shard_map/pallas_call | solution.py:311
  78.1 2.1 %collective-permute-start.10 = (bf16[256,512]{1,0:T(8,128)(2,1)S(1)}, bf16[256,512]{1,0:T(8,128)(2,1)S(1)}, u32[]{:S(2)}, u32[]{:S(2)}) collective-permute-start(bf16[256,512]{1,0:T(8,128)(2,1)S(1)} %copy-done.12), channel_id=1, source_target_pairs={{0,4},{2,6},{4,0},{6,2},{8,12},{10,14},{12,8},{14,10},{16,20},{18,... | collective-permute-start | bytes 786440 | tf_op jit(solution)/shard_map/ppermute | solution.py:409
  80.6 1.7 %shard_map.136 = (f32[128,512]{1,0:T(8,128)S(1)}, bf16[128,512]{1,0:T(8,128)(2,1)S(1)}, bf16[128,512]{1,0:T(8,128)(2,1)S(1)}, bf16[128,512]{1,0:T(8,128)(2,1)S(1)}) custom-call(s32[1]{0:T(128)} %bitcast.3.lead_ref, bf16[512,256]{1,0:T(8,128)(2,1)S(1)} %copy-done.5, bf16[512,256]{1,0:T(8,128)(2,1)S(1)} %collective-permute-done.6.refs_1_, ...), custom_call_target="tpu_custom_call" | custom-call | flops 536870912 | bytes 1048576 | tf_op jit(solution)/shard_map/pallas_call | solution.py:311
  82.3 1.8 %collective-permute-start.18 = (bf16[128,512]{1,0:T(8,128)(2,1)S(1)}, bf16[128,512]{1,0:T(8,128)(2,1)S(1)}, u32[]{:S(2)}, u32[]{:S(2)}) collective-permute-start(bf16[128,512]{1,0:T(8,128)(2,1)S(1)} %get-tuple-element.69), channel_id=1, source_target_pairs={{0,8},{2,10},{4,12},{6,14},{8,0},{10,2},{12,4},{14,6},{16,24},{18,... | collective-permute-start | bytes 393224 | tf_op jit(solution)/shard_map/ppermute | solution.py:412
  84.0 3.1 %collective-permute-start.19 = (bf16[128,512]{1,0:T(8,128)(2,1)S(1)}, bf16[128,512]{1,0:T(8,128)(2,1)S(1)}, u32[]{:S(2)}, u32[]{:S(2)}) collective-permute-start(bf16[128,512]{1,0:T(8,128)(2,1)S(1)} %get-tuple-element.70), channel_id=1, source_target_pairs={{0,16},{2,18},{4,20},{6,22},{8,24},{10,26},{12,28},{14,30},{16,0},... | collective-permute-start | bytes 393224 | tf_op jit(solution)/shard_map/ppermute | solution.py:412
  87.1 4.2 %collective-permute-start.20 = (bf16[128,512]{1,0:T(8,128)(2,1)S(1)}, bf16[128,512]{1,0:T(8,128)(2,1)S(1)}, u32[]{:S(2)}, u32[]{:S(2)}) collective-permute-start(bf16[128,512]{1,0:T(8,128)(2,1)S(1)} %get-tuple-element.71), channel_id=1, source_target_pairs={{0,24},{2,26},{4,28},{6,30},{8,16},{10,18},{12,20},{14,22},{16,8},... | collective-permute-start | bytes 393224 | tf_op jit(solution)/shard_map/ppermute | solution.py:412
  91.3 0.8 shard_map.135
  92.2 2.0 %collective-permute-start.13 = (bf16[128,512]{1,0:T(8,128)(2,1)S(1)}, bf16[128,512]{1,0:T(8,128)(2,1)S(1)}, u32[]{:S(2)}, u32[]{:S(2)}) collective-permute-start(bf16[128,512]{1,0:T(8,128)(2,1)S(1)} %get-tuple-element.65), channel_id=1, source_target_pairs={{0,16},{2,18},{4,20},{6,22},{8,24},{10,26},{12,28},{14,30},{16,0},... | collective-permute-start | bytes 393224 | tf_op jit(solution)/shard_map/ppermute | solution.py:412
  94.2 1.9 %collective-permute-done.19.refs_6_ = bf16[128,512]{1,0:T(8,128)(2,1)S(1)} collective-permute-done((bf16[128,512]{1,0:T(8,128)(2,1)S(1)}, bf16[128,512]{1,0:T(8,128)(2,1)S(1)}, u32[]{:S(2)}, u32[]{:S(2)}) %collective-permute-start.19) | collective-permute-done | bytes 131104 | tf_op jit(solution)/shard_map/ppermute | solution.py:412
  96.1 3.4 %collective-permute-start.14 = (bf16[128,512]{1,0:T(8,128)(2,1)S(1)}, bf16[128,512]{1,0:T(8,128)(2,1)S(1)}, u32[]{:S(2)}, u32[]{:S(2)}) collective-permute-start(bf16[128,512]{1,0:T(8,128)(2,1)S(1)} %get-tuple-element.66), channel_id=1, source_target_pairs={{0,24},{2,26},{4,28},{6,30},{8,16},{10,18},{12,20},{14,22},{16,8},... | collective-permute-start | bytes 393224 | tf_op jit(solution)/shard_map/ppermute | solution.py:412
  99.6 8.3 %shard_map.132 = (bf16[256,1024]{1,0:T(8,128)(2,1)}, bf16[256,1024]{1,0:T(8,128)(2,1)}, f32[8,256]{1,0:T(8,128)}, f32[8,256]{1,0:T(8,128)}) custom-call(bf16[256,1024]{1,0:T(8,128)(2,1)S(1)} %copy-done.1, bf16[256,1024]{1,0:T(8,128)(2,1)S(1)} %copy-done.2, bf16[256,1024]{1,0:T(8,128)(2,1)S(1)} %copy-done.8, bf16[256,1024]{1,0:T(8,128)(2,1)S(1)} %copy-done.3, ...), custom_call_target="tpu_custom_call" | custom-call | flops 134217728 | bytes 1048576 | tf_op jit(solution)/shard_map/pallas_call | solution.py:311
  107.9 0.9 shard_map.137
  108.8 0.9 shard_map.134
  (54 shorter events, 2.9 us)
Async XLA Ops:
  14.3 50.3 %copy-start.9 = (bf16[256,1024]{1,0:T(8,128)(2,1)S(1)}, bf16[256,1024]{1,0:T(8,128)(2,1)}, u32[]{:S(2)}) copy-start(bf16[256,1024]{1,0:T(8,128)(2,1)} %get-tuple-element.43.bdr_ref) | copy-start | bytes 1572868
  14.3 50.3 %copy-start.10 = (bf16[256,1024]{1,0:T(8,128)(2,1)S(1)}, bf16[256,1024]{1,0:T(8,128)(2,1)}, u32[]{:S(2)}) copy-start(bf16[256,1024]{1,0:T(8,128)(2,1)} %get-tuple-element.44.by_ref) | copy-start | bytes 1572868
  31.8 48.8 %copy-start.5 = (bf16[512,256]{1,0:T(8,128)(2,1)S(1)}, bf16[512,256]{1,0:T(8,128)(2,1)}, u32[]{:S(2)}) copy-start(bf16[512,256]{1,0:T(8,128)(2,1)} %get-tuple-element.58.refs_0_) | copy-start | bytes 786436
  31.8 5.7 %collective-permute-start = (bf16[3,2,128,128]{3,2,1,0:T(8,128)(2,1)S(1)}, bf16[3,2,128,128]{3,2,1,0:T(8,128)(2,1)S(1)}, u32[]{:S(2)}, u32[]{:S(2)}) collective-permute-start(bf16[3,2,128,128]{3,2,1,0:T(8,128)(2,1)S(1)} %shard_map.128.own.refs_0_), channel_id=1, source_target_pairs={{0,8},{2,10},{4,12},{6,14},{8,0},{10,2},{12,4},{14,6},{16,24},{18,... | collective-permute-start | bytes 589832 | tf_op jit(solution)/shard_map/ppermute | solution.py:412
  37.7 5.2 %collective-permute-start.1 = (bf16[2,128,128]{2,1,0:T(8,128)(2,1)S(1)}, bf16[2,128,128]{2,1,0:T(8,128)(2,1)S(1)}, u32[]{:S(2)}, u32[]{:S(2)}) collective-permute-start(bf16[2,128,128]{2,1,0:T(8,128)(2,1)S(1)} %shard_map.129), channel_id=1, source_target_pairs={{0,16},{2,18},{4,20},{6,22},{8,24},{10,26},{12,28},{14,30},{16,0},... | collective-permute-start | bytes 196616 | tf_op jit(solution)/shard_map/ppermute | solution.py:412
  43.6 6.4 %collective-permute-start.2 = (bf16[2,2,128,128]{3,2,1,0:T(8,128)(2,1)S(1)}, bf16[2,2,128,128]{3,2,1,0:T(8,128)(2,1)S(1)}, u32[]{:S(2)}, u32[]{:S(2)}) collective-permute-start(bf16[2,2,128,128]{3,2,1,0:T(8,128)(2,1)S(1)} %get-tuple-element.47), channel_id=1, source_target_pairs={{0,2},{2,0},{4,6},{6,4},{8,10},{10,8},{12,14},{14,12},{16,18},{18,... | collective-permute-start | bytes 393224 | tf_op jit(solution)/shard_map/ppermute | solution.py:409
  44.6 28.1 %collective-permute-start.6 = (bf16[512,256]{1,0:T(8,128)(2,1)}, bf16[512,256]{1,0:T(8,128)(2,1)S(1)}, u32[]{:S(2)}, u32[]{:S(2)}) collective-permute-start(bf16[512,256]{1,0:T(8,128)(2,1)} %get-tuple-element.59), channel_id=1, source_target_pairs={{0,2},{2,0},{4,6},{6,4},{8,10},{10,8},{12,14},{14,12},{16,18},{18,... | collective-permute-start | bytes 786440 | tf_op jit(solution)/shard_map/ppermute | solution.py:409
  45.7 27.0 %collective-permute-start.7 = (bf16[512,256]{1,0:T(8,128)(2,1)}, bf16[512,256]{1,0:T(8,128)(2,1)S(1)}, u32[]{:S(2)}, u32[]{:S(2)}) collective-permute-start(bf16[512,256]{1,0:T(8,128)(2,1)} %get-tuple-element.60), channel_id=1, source_target_pairs={{0,4},{2,6},{4,0},{6,2},{8,12},{10,14},{12,8},{14,10},{16,20},{18,... | collective-permute-start | bytes 786440 | tf_op jit(solution)/shard_map/ppermute | solution.py:409
  46.6 18.0 %collective-permute-start.3 = (bf16[2,2,128,128]{3,2,1,0:T(8,128)(2,1)S(1)}, bf16[2,2,128,128]{3,2,1,0:T(8,128)(2,1)S(1)}, u32[]{:S(2)}, u32[]{:S(2)}) collective-permute-start(bf16[2,2,128,128]{3,2,1,0:T(8,128)(2,1)S(1)} %get-tuple-element.48), channel_id=1, source_target_pairs={{0,4},{2,6},{4,0},{6,2},{8,12},{10,14},{12,8},{14,10},{16,20},{18,... | collective-permute-start | bytes 393224 | tf_op jit(solution)/shard_map/ppermute | solution.py:409
  47.7 16.9 %collective-permute-start.4 = (bf16[2,2,128,128]{3,2,1,0:T(8,128)(2,1)S(1)}, bf16[2,2,128,128]{3,2,1,0:T(8,128)(2,1)S(1)}, u32[]{:S(2)}, u32[]{:S(2)}) collective-permute-start(bf16[2,2,128,128]{3,2,1,0:T(8,128)(2,1)S(1)} %get-tuple-element.49), channel_id=1, source_target_pairs={{0,6},{2,4},{4,2},{6,0},{8,14},{10,12},{12,10},{14,8},{16,22},{18,... | collective-permute-start | bytes 393224 | tf_op jit(solution)/shard_map/ppermute | solution.py:409
  50.0 28.0 %collective-permute-start.8 = (bf16[512,256]{1,0:T(8,128)(2,1)}, bf16[512,256]{1,0:T(8,128)(2,1)S(1)}, u32[]{:S(2)}, u32[]{:S(2)}) collective-permute-start(bf16[512,256]{1,0:T(8,128)(2,1)} %get-tuple-element.61), channel_id=1, source_target_pairs={{0,6},{2,4},{4,2},{6,0},{8,14},{10,12},{12,10},{14,8},{16,22},{18,... | collective-permute-start | bytes 786440 | tf_op jit(solution)/shard_map/ppermute | solution.py:409
  66.4 11.7 %collective-permute-start.17 = (bf16[256,512]{1,0:T(8,128)(2,1)}, bf16[256,512]{1,0:T(8,128)(2,1)S(1)}, u32[]{:S(2)}, u32[]{:S(2)}) collective-permute-start(bf16[256,512]{1,0:T(8,128)(2,1)} %get-tuple-element.67.refs_4_), channel_id=1, source_target_pairs={{0,6},{2,4},{4,2},{6,0},{8,14},{10,12},{12,10},{14,8},{16,22},{18,... | collective-permute-start | bytes 786440 | tf_op jit(solution)/shard_map/ppermute | solution.py:409
  70.0 10.2 %collective-permute-start.16 = (bf16[256,512]{1,0:T(8,128)(2,1)}, bf16[256,512]{1,0:T(8,128)(2,1)S(1)}, u32[]{:S(2)}, u32[]{:S(2)}) collective-permute-start(bf16[256,512]{1,0:T(8,128)(2,1)} %get-tuple-element.67.refs_4_), channel_id=1, source_target_pairs={{0,4},{2,6},{4,0},{6,2},{8,12},{10,14},{12,8},{14,10},{16,20},{18,... | collective-permute-start | bytes 786440 | tf_op jit(solution)/shard_map/ppermute | solution.py:409
  72.6 7.9 %collective-permute-start.15 = (bf16[256,512]{1,0:T(8,128)(2,1)}, bf16[256,512]{1,0:T(8,128)(2,1)S(1)}, u32[]{:S(2)}, u32[]{:S(2)}) collective-permute-start(bf16[256,512]{1,0:T(8,128)(2,1)} %get-tuple-element.67.refs_4_), channel_id=1, source_target_pairs={{0,2},{2,0},{4,6},{6,4},{8,10},{10,8},{12,14},{14,12},{16,18},{18,... | collective-permute-start | bytes 786440 | tf_op jit(solution)/shard_map/ppermute | solution.py:409
  72.6 11.4 %collective-permute-start.11 = (bf16[256,512]{1,0:T(8,128)(2,1)}, bf16[256,512]{1,0:T(8,128)(2,1)S(1)}, u32[]{:S(2)}, u32[]{:S(2)}) collective-permute-start(bf16[256,512]{1,0:T(8,128)(2,1)} %copy-done.11), channel_id=1, source_target_pairs={{0,6},{2,4},{4,2},{6,0},{8,14},{10,12},{12,10},{14,8},{16,22},{18,... | collective-permute-start | bytes 786440 | tf_op jit(solution)/shard_map/ppermute | solution.py:409
  76.3 23.2 %copy-start.1 = (bf16[256,1024]{1,0:T(8,128)(2,1)S(1)}, bf16[256,1024]{1,0:T(8,128)(2,1)}, u32[]{:S(2)}) copy-start(bf16[256,1024]{1,0:T(8,128)(2,1)} %q_ref.1) | copy-start | bytes 1572868
  76.3 23.2 %copy-start.2 = (bf16[256,1024]{1,0:T(8,128)(2,1)S(1)}, bf16[256,1024]{1,0:T(8,128)(2,1)}, u32[]{:S(2)}) copy-start(bf16[256,1024]{1,0:T(8,128)(2,1)} %k_ref.1) | copy-start | bytes 1572868
  76.3 23.2 %copy-start.3 = (bf16[256,1024]{1,0:T(8,128)(2,1)S(1)}, bf16[256,1024]{1,0:T(8,128)(2,1)}, u32[]{:S(2)}) copy-start(bf16[256,1024]{1,0:T(8,128)(2,1)} %do_ref.1) | copy-start | bytes 1572868
  76.3 23.2 %copy-start.4 = (bf16[8,256,256]{2,1,0:T(8,128)(2,1)S(1)}, bf16[8,256,256]{2,1,0:T(8,128)(2,1)}, u32[]{:S(2)}) copy-start(bf16[8,256,256]{2,1,0:T(8,128)(2,1)} %get-tuple-element.40.inv_ref) | copy-start | bytes 3145732
  76.3 23.2 %copy-start.6 = (bf16[256,1024]{1,0:T(8,128)(2,1)S(1)}, bf16[256,1024]{1,0:T(8,128)(2,1)}, u32[]{:S(2)}) copy-start(bf16[256,1024]{1,0:T(8,128)(2,1)} %get-tuple-element.41.dr_ref) | copy-start | bytes 1572868
  76.3 23.2 %copy-start.7 = (bf16[256,1024]{1,0:T(8,128)(2,1)S(1)}, bf16[256,1024]{1,0:T(8,128)(2,1)}, u32[]{:S(2)}) copy-start(bf16[256,1024]{1,0:T(8,128)(2,1)} %get-tuple-element.42.y_ref) | copy-start | bytes 1572868
  76.3 23.2 %copy-start.8 = (bf16[256,1024]{1,0:T(8,128)(2,1)S(1)}, bf16[256,1024]{1,0:T(8,128)(2,1)}, u32[]{:S(2)}) copy-start(bf16[256,1024]{1,0:T(8,128)(2,1)} %get-tuple-element.39.v_ref) | copy-start | bytes 1572868
  76.3 23.2 %copy-start.13 = (f32[256,8]{0,1:T(8,128)S(1)}, f32[256,8]{0,1:T(8,128)}, u32[]{:S(2)}) copy-start(f32[256,8]{0,1:T(8,128)} %param.12) | copy-start | bytes 24580
  78.0 30.8 %collective-permute-start.5 = (bf16[128,2048]{1,0:T(8,128)(2,1)S(1)}, bf16[128,2048]{1,0:T(8,128)(2,1)S(1)}, u32[]{:S(2)}, u32[]{:S(2)}) collective-permute-start(bf16[128,2048]{1,0:T(8,128)(2,1)S(1)} %get-tuple-element.57), channel_id=1, source_target_pairs={{0,1},{1,0},{2,3},{3,2},{4,5},{5,4},{6,7},{7,6},{8,9},{9,8},{10,11... | collective-permute-start | bytes 1572872 | tf_op jit(solution)/shard_map/ppermute | solution.py:498
  78.1 9.0 %collective-permute-start.10 = (bf16[256,512]{1,0:T(8,128)(2,1)S(1)}, bf16[256,512]{1,0:T(8,128)(2,1)S(1)}, u32[]{:S(2)}, u32[]{:S(2)}) collective-permute-start(bf16[256,512]{1,0:T(8,128)(2,1)S(1)} %copy-done.12), channel_id=1, source_target_pairs={{0,4},{2,6},{4,0},{6,2},{8,12},{10,14},{12,8},{14,10},{16,20},{18,... | collective-permute-start | bytes 786440 | tf_op jit(solution)/shard_map/ppermute | solution.py:409
  80.2 11.1 %collective-permute-start.9 = (bf16[256,512]{1,0:T(8,128)(2,1)S(1)}, bf16[256,512]{1,0:T(8,128)(2,1)S(1)}, u32[]{:S(2)}, u32[]{:S(2)}) collective-permute-start(bf16[256,512]{1,0:T(8,128)(2,1)S(1)} %copy-done.12), channel_id=1, source_target_pairs={{0,2},{2,0},{4,6},{6,4},{8,10},{10,8},{12,14},{14,12},{16,18},{18,... | collective-permute-start | bytes 786440 | tf_op jit(solution)/shard_map/ppermute | solution.py:409
  82.3 9.9 %collective-permute-start.18 = (bf16[128,512]{1,0:T(8,128)(2,1)S(1)}, bf16[128,512]{1,0:T(8,128)(2,1)S(1)}, u32[]{:S(2)}, u32[]{:S(2)}) collective-permute-start(bf16[128,512]{1,0:T(8,128)(2,1)S(1)} %get-tuple-element.69), channel_id=1, source_target_pairs={{0,8},{2,10},{4,12},{6,14},{8,0},{10,2},{12,4},{14,6},{16,24},{18,... | collective-permute-start | bytes 393224 | tf_op jit(solution)/shard_map/ppermute | solution.py:412
  84.0 12.1 %collective-permute-start.19 = (bf16[128,512]{1,0:T(8,128)(2,1)S(1)}, bf16[128,512]{1,0:T(8,128)(2,1)S(1)}, u32[]{:S(2)}, u32[]{:S(2)}) collective-permute-start(bf16[128,512]{1,0:T(8,128)(2,1)S(1)} %get-tuple-element.70), channel_id=1, source_target_pairs={{0,16},{2,18},{4,20},{6,22},{8,24},{10,26},{12,28},{14,30},{16,0},... | collective-permute-start | bytes 393224 | tf_op jit(solution)/shard_map/ppermute | solution.py:412
  87.1 20.7 %collective-permute-start.20 = (bf16[128,512]{1,0:T(8,128)(2,1)S(1)}, bf16[128,512]{1,0:T(8,128)(2,1)S(1)}, u32[]{:S(2)}, u32[]{:S(2)}) collective-permute-start(bf16[128,512]{1,0:T(8,128)(2,1)S(1)} %get-tuple-element.71), channel_id=1, source_target_pairs={{0,24},{2,26},{4,28},{6,30},{8,16},{10,18},{12,20},{14,22},{16,8},... | collective-permute-start | bytes 393224 | tf_op jit(solution)/shard_map/ppermute | solution.py:412
  92.1 15.8 %collective-permute-start.12 = (bf16[128,512]{1,0:T(8,128)(2,1)S(1)}, bf16[128,512]{1,0:T(8,128)(2,1)S(1)}, u32[]{:S(2)}, u32[]{:S(2)}) collective-permute-start(bf16[128,512]{1,0:T(8,128)(2,1)S(1)} %get-tuple-element.64), channel_id=1, source_target_pairs={{0,8},{2,10},{4,12},{6,14},{8,0},{10,2},{12,4},{14,6},{16,24},{18,... | collective-permute-start | bytes 393224 | tf_op jit(solution)/shard_map/ppermute | solution.py:412
  92.2 15.7 %collective-permute-start.13 = (bf16[128,512]{1,0:T(8,128)(2,1)S(1)}, bf16[128,512]{1,0:T(8,128)(2,1)S(1)}, u32[]{:S(2)}, u32[]{:S(2)}) collective-permute-start(bf16[128,512]{1,0:T(8,128)(2,1)S(1)} %get-tuple-element.65), channel_id=1, source_target_pairs={{0,16},{2,18},{4,20},{6,22},{8,24},{10,26},{12,28},{14,30},{16,0},... | collective-permute-start | bytes 393224 | tf_op jit(solution)/shard_map/ppermute | solution.py:412
  96.1 11.8 %collective-permute-start.14 = (bf16[128,512]{1,0:T(8,128)(2,1)S(1)}, bf16[128,512]{1,0:T(8,128)(2,1)S(1)}, u32[]{:S(2)}, u32[]{:S(2)}) collective-permute-start(bf16[128,512]{1,0:T(8,128)(2,1)S(1)} %get-tuple-element.66), channel_id=1, source_target_pairs={{0,24},{2,26},{4,28},{6,30},{8,16},{10,18},{12,20},{14,22},{16,8},... | collective-permute-start | bytes 393224 | tf_op jit(solution)/shard_map/ppermute | solution.py:412
  (5 other events, 51.2 us)
